TPU v7x, 256 devices: a whole 4x4x8 slice. The times are simulated.
256 devices in a mesh: sp: 64 (over z, y, core), tp: 4 (over x).
Axes of the slice: x: 4, y: 4, z: 8, core: 2. Of those that a mesh axis runs over, the one named last changes fastest.
Arguments:
- tokens: bfloat16 [49152, 2048], P('sp'), may hold values from -6 to 6
- input_gain: bfloat16 [2048], replicated, may hold values from 0.099609375 to 1.8984375
- gate_weight: bfloat16 [2048, 2048], P('sp', 'tp'), may hold values from -0.125 to 0.125
- value_weight: bfloat16 [2048, 2048], P('sp', 'tp'), may hold values from -0.125 to 0.125
- inflow_weight: bfloat16 [2048, 4, 128], P('sp', 'tp'), may hold values from -0.125 to 0.125
- readout_weight: bfloat16 [2048, 4, 128], P('sp', 'tp'), may hold values from -0.125 to 0.125
- step_weight: bfloat16 [2048, 2, 32], P('sp', None, 'tp'), may hold values from -0.125 to 0.125
- conv_values: bfloat16 [5, 2048], P(None, 'tp'), may hold values from -2.5 to 2.5
- conv_inflow: bfloat16 [5, 4, 128], P(None, 'tp'), may hold values from -2.5 to 2.5
- conv_readout: bfloat16 [5, 4, 128], P(None, 'tp'), may hold values from -2.5 to 2.5
- log_rate: float32 [2, 49152, 32], P(None, 'sp', 'tp'), may hold values from -20 to 0
- group_gain: bfloat16 [2048], P('tp'), may hold values from 0.099609375 to 1.8984375
- query_weight: bfloat16 [2048, 2048], P('sp', 'tp'), may hold values from -8 to 8
- key_weight: bfloat16 [2048, 512], P('sp', 'tp'), may hold values from -8 to 8
- vector_weight: bfloat16 [2048, 512], P('sp', 'tp'), may hold values from -0.125 to 0.125
- sink_logit: float32 [32], P('tp'), may hold values from 3 to 7
- state_out: bfloat16 [2048, 2048], P('tp', 'sp'), may hold values from -0.125 to 0.125
- window_out: bfloat16 [2048, 2048], P('tp', 'sp'), may hold values from -1 to 1
Outputs:
- mixed: bfloat16 [49152, 2048], P('sp', 'tp')
- log_total: float32 [49152, 32], P('sp', 'tp')
All inputs are finite; a program needn't handle non-finite values.
Results may differ from a plain program's by a relative error of at most 0.015.
The roundings to bfloat16 on the way count: a program that leaves them out, or rounds other values in their place, can miss the bound.
Values may be sent and summed in bfloat16 or wider, within the bound.
A program may use at most 128 MiB of HBM per device.

v0:
```python
import jax
import jax.numpy as jnp
from jax import lax
from jax.sharding import Mesh
from jax.sharding import PartitionSpec as P

HEAD_DIM = 64
CONV = 5
SSD_BLOCK = 128
WINDOW = 128
QBLOCK = 256
GRID_W = 64
SP = ("sp_0", "sp_1", "sp_2")


EPS = 1e-06
ROPE_BASE = 10000.0
HIGH = lax.Precision.HIGH


def turned_gather(arrays, axis, dims):
    turned = [jnp.moveaxis(a, dim, 0) for a, dim in zip(arrays, dims)]
    widths = [t[0].size for t in turned]
    both = jnp.concatenate([t.reshape(-1, w) for t, w in zip(turned, widths)], axis=1)
    out = lax.all_gather(both, axis, axis=0, tiled=True)
    parts = jnp.split(out, [sum(widths[:k]) for k in range(1, len(widths))], axis=1)
    return tuple(
        (
            jnp.moveaxis(b.reshape(-1, *t.shape[1:]), 0, dim)
            for b, t, dim in zip(parts, turned, dims)
        )
    )


def nothing_yet(value, identity):
    return jax.tree.map(
        lambda part, zero: jnp.zeros_like(part) + jnp.asarray(zero, part.dtype), value, identity
    )


def carried_in(value, axes, combine, identity, reverse):
    before = start = nothing_yet(value, identity)
    running = value
    for axis in reversed(axes):
        length, position = (lax.axis_size(axis), lax.axis_index(axis))
        pieces = jax.tree.map(
            lambda part, kind: lax.all_gather(part.astype(kind), axis),
            running,
            jax.tree.map(lambda a: jnp.bfloat16 if a.dtype == jnp.float32 else a.dtype, value),
        )
        inside, running = (start, start)
        for k in reversed(range(length)) if reverse else range(length):
            passed = k > position if reverse else k < position
            running = combine(
                running, jax.tree.map(lambda part, own: part[k].astype(own.dtype), pieces, value)
            )
            inside = jax.tree.map(lambda new, old: jnp.where(passed, new, old), running, inside)
        before = combine(inside, before)
    return before


def with_halo(cells, sides, width):
    for axis, dim in sides:
        count = lax.axis_size(axis)
        ends = count - 1
        head = lax.slice_in_dim(cells, 0, width, axis=dim)
        tail = lax.slice_in_dim(cells, cells.shape[dim] - width, cells.shape[dim], axis=dim)
        cells = jnp.concatenate(
            [
                lax.ppermute(tail, axis, [(i, (i + 1) % count) for i in range(ends)]),
                cells,
                lax.ppermute(head, axis, [((i + 1) % count, i) for i in range(ends)]),
            ],
            axis=dim,
        )
    return cells


def cut_along(value, dim, length):
    shape = value.shape
    parts = value.reshape(*shape[:dim], length, shape[dim] // length, *shape[dim + 1 :])
    return jnp.moveaxis(parts, dim, 0)


def sent_and_summed(value, axis, dim):
    parts = cut_along(value, dim, lax.axis_size(axis))
    arrived = lax.all_to_all(parts, axis, split_axis=0, concat_axis=0, tiled=True)
    return arrived.astype(jnp.float32).sum(axis=0)


def rope_pairs(part, angle):
    half = part.shape[-1] // 2
    cosine = jnp.cos(angle)[:, None, :]
    sine = jnp.sin(angle)[:, None, :]
    first = part[..., :half]
    second = part[..., half:]
    return jnp.concatenate(
        [first * cosine - second * sine, second * cosine + first * sine], axis=-1
    )


def axial_rope(heads, positions):
    width = heads.shape[-1]
    quarter = width // 4
    freqs = ROPE_BASE ** (-jnp.arange(quarter).astype(jnp.float32) / quarter)
    row_angle = (positions // GRID_W).astype(jnp.float32)[:, None] * freqs
    col_angle = (positions % GRID_W).astype(jnp.float32)[:, None] * freqs
    half = width // 2
    wide = heads.astype(jnp.float32)
    turned = jnp.concatenate(
        [rope_pairs(wide[..., :half], row_angle), rope_pairs(wide[..., half:], col_angle)], axis=-1
    )
    return turned.astype(jnp.bfloat16)


def block_ssd(state, inputs):
    xdt, decay, inflow, readout = inputs
    length = decay.shape[0]
    heads = xdt.shape[1]
    groups = inflow.shape[1]
    repeat = heads // groups
    cum = jnp.cumsum(decay, axis=0)
    seg = cum[:, None, :] - cum[None, :, :]
    lower = jnp.arange(length)[:, None] >= jnp.arange(length)[None, :]
    weight = jnp.exp(jnp.where(lower[:, :, None], seg, -jnp.inf))
    intersection = jnp.einsum("lgn,sgn->lsg", readout, inflow, preferred_element_type=jnp.float32)
    intersection = jnp.repeat(intersection, repeat, axis=2)
    final_result = jnp.einsum("lsh,shp->lhp", intersection * weight, xdt, precision=HIGH)
    read_heads = jnp.repeat(readout, repeat, axis=1).astype(jnp.float32)
    final_result = final_result + jnp.exp(cum)[:, :, None] * jnp.einsum(
        "lhn,hpn->lhp", read_heads, state, precision=HIGH
    )
    write_heads = jnp.repeat(inflow, repeat, axis=1).astype(jnp.float32)
    to_end = jnp.exp(cum[-1][None, :] - cum)
    fresh = jnp.einsum("shp,shn->hpn", xdt * to_end[:, :, None], write_heads, precision=HIGH)
    return (jnp.exp(cum[-1])[:, None, None] * state + fresh, final_result)


def chain(earlier, later):
    return (earlier[0] + later[0], jnp.exp(later[0])[:, None, None] * earlier[1] + later[1])


def flatten_rows(weight):
    return weight.reshape(weight.shape[0], -1)


def shards(
    tokens,
    input_gain,
    gate_weight,
    value_weight,
    inflow_weight,
    readout_weight,
    step_weight,
    conv_values,
    conv_inflow,
    conv_readout,
    log_rate,
    group_gain,
    query_weight,
    key_weight,
    vector_weight,
    sink_logit,
    state_out,
    window_out,
):
    count = tokens.shape[0]
    offset = lax.axis_index(SP) * count
    seq_total = count * lax.axis_size(SP)
    positions = offset + jnp.arange(count, dtype=jnp.int32)
    heads = step_weight.shape[2]
    groups = inflow_weight.shape[1]
    state_len = inflow_weight.shape[2]
    inner_local = value_weight.shape[1]
    q_count = query_weight.shape[1] // HEAD_DIM
    kv_count = key_weight.shape[1] // HEAD_DIM
    kv_width = key_weight.shape[1]
    wide = tokens.astype(jnp.float32)
    normed = (
        wide
        * lax.rsqrt(jnp.mean(wide * wide, axis=1, keepdims=True) + EPS)
        * input_gain.astype(jnp.float32)
    ).astype(jnp.bfloat16)
    out_stack = jnp.concatenate([state_out, window_out], axis=0)
    gathered = turned_gather(
        (
            gate_weight,
            value_weight,
            inflow_weight,
            readout_weight,
            step_weight,
            query_weight,
            key_weight,
            vector_weight,
            out_stack,
        ),
        SP,
        (0, 0, 0, 0, 0, 0, 0, 0, 1),
    )
    pieces = gathered[:8]
    matrices = (
        pieces[0],
        jnp.concatenate([pieces[1], flatten_rows(pieces[2]), flatten_rows(pieces[3])], axis=1),
        flatten_rows(pieces[4]),
        pieces[5],
        jnp.concatenate([pieces[6], pieces[7]], axis=1),
    )
    sums = tuple(
        (jnp.dot(normed, matrix, preferred_element_type=jnp.float32) for matrix in matrices)
    )
    out_whole = gathered[8]
    gate = sums[0].astype(jnp.bfloat16)
    conv_input = sums[1].astype(jnp.bfloat16)
    step = jax.nn.softplus(sums[2]).reshape(count, 2, heads)
    queries = sums[3].astype(jnp.bfloat16)
    keyvals = sums[4].astype(jnp.bfloat16)

    def direction(xdt, decay, inflow, readout, backward):
        if backward:
            xdt = jnp.flip(xdt, 0)
            decay = jnp.flip(decay, 0)
            inflow = jnp.flip(inflow, 0)
            readout = jnp.flip(readout, 0)
        blocks = count // SSD_BLOCK
        start_state = jnp.zeros((heads, HEAD_DIM, state_len), jnp.float32)
        shaped = (
            xdt.reshape(blocks, SSD_BLOCK, heads, HEAD_DIM),
            decay.reshape(blocks, SSD_BLOCK, heads),
            inflow.reshape(blocks, SSD_BLOCK, groups, state_len),
            readout.reshape(blocks, SSD_BLOCK, groups, state_len),
        )
        end_state, local = lax.scan(block_ssd, start_state, shaped)
        local = local.reshape(count, heads, HEAD_DIM)
        summary = (jnp.sum(decay, axis=0), end_state)
        identity = (jnp.zeros((heads,), jnp.float32), jnp.zeros_like(end_state))
        if backward:
            incoming = carried_in(summary, SP, chain, identity, True)
        else:
            incoming = carried_in(summary, SP, chain, identity, False)
        reach = jnp.exp(jnp.cumsum(decay, axis=0))
        per_head = jnp.repeat(readout, heads // groups, axis=1).astype(jnp.float32)
        local = local + reach[:, :, None] * jnp.einsum(
            "lhn,hpn->lhp", per_head, incoming[1], precision=HIGH
        )
        if backward:
            local = jnp.flip(local, 0)
        return local

    reach_rows = CONV // 2
    padded = with_halo(conv_input, ((SP, 0),), CONV // 2).astype(jnp.float32)
    taps = jnp.concatenate(
        [conv_values, flatten_rows(conv_inflow), flatten_rows(conv_readout)], axis=1
    ).astype(jnp.float32)
    conv_sum = padded[0:count] * taps[0]
    for tap in range(1, 2 * reach_rows + 1):
        conv_sum = conv_sum + padded[tap : tap + count] * taps[tap]
    conv_short = jax.nn.silu(conv_sum).astype(jnp.bfloat16)
    conv_out = conv_short.astype(jnp.float32)
    split_mid = inner_local + groups * state_len
    xs = conv_out[:, :inner_local].reshape(count, heads, HEAD_DIM)
    inflow = conv_short[:, inner_local:split_mid].reshape(count, groups, state_len)
    readout = conv_short[:, split_mid:].reshape(count, groups, state_len)
    decay = -jnp.exp(log_rate) * jnp.transpose(step, (1, 0, 2))
    forward = direction(xs * step[:, 0, :, None], decay[0], inflow, readout, False)
    backward = direction(xs * step[:, 1, :, None], decay[1], inflow, readout, True)
    combined = (forward + backward).reshape(count, -1) * jax.nn.silu(gate.astype(jnp.float32))
    grouped = combined.reshape(count, groups, -1)
    grouped = grouped * lax.rsqrt(jnp.mean(grouped * grouped, axis=2, keepdims=True) + EPS)
    state_features = (grouped.reshape(count, -1) * group_gain.astype(jnp.float32)).astype(
        jnp.bfloat16
    )
    q_heads = axial_rope(queries.reshape(count, q_count, HEAD_DIM), positions)
    k_heads = axial_rope(keyvals[:, :kv_width].reshape(count, kv_count, HEAD_DIM), positions)
    both = jnp.concatenate([k_heads.reshape(count, -1), keyvals[:, kv_width:]], axis=1)
    beside_all = with_halo(both, ((SP, 0),), WINDOW)
    repeat = q_count // kv_count
    band = QBLOCK + 2 * WINDOW
    sinks = sink_logit.reshape(kv_count, repeat, 1, 1)
    grouped_q = q_heads.reshape(count, kv_count, repeat, HEAD_DIM)

    def attend(index):
        start = index * QBLOCK
        block_q = lax.dynamic_slice_in_dim(grouped_q, start, QBLOCK, 0)
        block_kv = lax.dynamic_slice_in_dim(beside_all, start, band, 0)
        block_k = block_kv[:, :kv_width].reshape(band, kv_count, HEAD_DIM)
        block_v = block_kv[:, kv_width:].reshape(band, kv_count, HEAD_DIM)
        scores = jnp.einsum(
            "qkrd,skd->krqs", block_q, block_k, preferred_element_type=jnp.float32
        ) * HEAD_DIM ** (-0.5)
        query_pos = offset + start + jnp.arange(QBLOCK, dtype=jnp.int32)
        key_pos = offset + start - WINDOW + jnp.arange(band, dtype=jnp.int32)
        valid = (
            (jnp.abs(query_pos[:, None] - key_pos[None, :]) <= WINDOW)
            & (key_pos >= 0)[None, :]
            & (key_pos < seq_total)[None, :]
        )
        scores = jnp.where(valid, scores, -jnp.inf)
        top = jnp.maximum(jnp.max(scores, axis=-1, keepdims=True), sinks)
        expo = jnp.exp(scores - top)
        total = jnp.sum(expo, axis=-1, keepdims=True) + jnp.exp(sinks - top)
        probs = expo.astype(jnp.bfloat16)
        values = jnp.einsum("krqs,skd->qkrd", probs, block_v, preferred_element_type=jnp.float32)
        values = values / jnp.transpose(total, (2, 0, 1, 3))
        logs = jnp.transpose((top + jnp.log(total))[..., 0], (2, 0, 1)).reshape(QBLOCK, -1)
        return (values.astype(jnp.bfloat16).reshape(QBLOCK, -1), logs)

    feats, logs = lax.map(attend, jnp.arange(count // QBLOCK, dtype=jnp.int32))
    window_features = feats.reshape(count, -1)
    log_total = logs.reshape(count, -1)
    features = jnp.concatenate([state_features, window_features], axis=1)
    terms = jnp.dot(features, out_whole, preferred_element_type=jnp.float32)
    mixed = sent_and_summed(terms.astype(jnp.bfloat16), "tp", 1).astype(jnp.bfloat16)
    return (mixed, log_total)


def solution(mesh):
    torus = Mesh(mesh.devices.reshape(8, 4, 2, mesh.shape["tp"]), ("sp_0", "sp_1", "sp_2", "tp"))
    return jax.shard_map(
        shards,
        mesh=torus,
        in_specs=(
            P(SP, None),
            P(),
            P(SP, "tp"),
            P(SP, "tp"),
            P(SP, "tp", None),
            P(SP, "tp", None),
            P(SP, None, "tp"),
            P(None, "tp"),
            P(None, "tp", None),
            P(None, "tp", None),
            P(None, SP, "tp"),
            P("tp"),
            P(SP, "tp"),
            P(SP, "tp"),
            P(SP, "tp"),
            P("tp"),
            P("tp", SP),
            P("tp", SP),
        ),
        out_specs=(P(SP, "tp"), P(SP, "tp")),
        check_vma=False,
    )
```

profile of v0, /device:TPU:1, one launch (start us, length us, event | category | flops | bytes accessed | tf_op | source)
XLA Modules:
  0.0 517.7 jit_solution(13843516485455394829)
XLA Ops:
  19.3 86.2 %all-gather.12.cloned.1.call-done = bf16[2048,3088]{1,0:T(8,128)(2,1)} async-done(((bf16[32,3088]{1,0:T(8,128)(2,1)}), bf16[2048,3088]{1,0:T(8,128)(2,1)}) %all-gather.12.cloned.1.call-update) | async-done | bytes 12648464 | tf_op jit(solution)/shard_map/all_gather | solution.py:25
  124.1 5.5 %fusion.101 = bf16[768,768]{1,0:T(8,128)(2,1)S(1)} fusion(bf16[2048,3088]{1,0:T(8,128)(2,1)} %all-gather.12.cloned.1.call-done, bf16[768,2048]{1,0:T(8,128)(2,1)} %param.24, f32[2048]{0:T(1024)S(1)} %convert_element_type.661, f32[768]{0:T(1024)S(1)} %add_rsqrt_fusion.1), kind=kOutput, calls=%fused_computation.141 | convolution fusion | flops 2422800384 | bytes 7482368 | tf_op jit(solution)/shard_map/dot_general | solution.py:209
  141.8 10.0 %all-gather.6 = bf16[4,1,8]{2,1,0:T(2,128)(2,1)S(1)} all-gather(bf16[1,1,8]{2,1,0:T(2,128)(2,1)S(1)} %get-tuple-element.405), channel_id=1, replica_groups=mesh['sp_0'=8,'sp_1'=4,'sp_2'=2,'tp'=4] {'sp_1'}, dimensions={0}, use_global_device_ids=true | all-gather | bytes 80 | tf_op jit(solution)/shard_map/all_gather | solution.py:47
  153.6 12.3 %all-gather.7 = bf16[8,1,8]{2,1,0:T(2,128)(2,1)S(1)} all-gather(bf16[1,1,8]{2,1,0:T(2,128)(2,1)S(1)} %get-tuple-element.396), channel_id=1, replica_groups=mesh['sp_0'=8,'sp_1'=4,'sp_2'=2,'tp'=4] {'sp_0'}, dimensions={0}, use_global_device_ids=true | all-gather | bytes 144 | tf_op jit(solution)/shard_map/all_gather | solution.py:47
  169.9 5.2 %all-gather.4 = bf16[4,1,8]{2,1,0:T(2,128)(2,1)S(1)} all-gather(bf16[1,1,8]{2,1,0:T(2,128)(2,1)S(1)} %get-tuple-element.402), channel_id=1, replica_groups=mesh['sp_0'=8,'sp_1'=4,'sp_2'=2,'tp'=4] {'sp_1'}, dimensions={0}, use_global_device_ids=true | all-gather | bytes 80 | tf_op jit(solution)/shard_map/all_gather | solution.py:47
  177.0 10.0 %all-gather.5 = bf16[8,1,8]{2,1,0:T(2,128)(2,1)S(1)} all-gather(bf16[1,1,8]{2,1,0:T(2,128)(2,1)S(1)} %get-tuple-element.391), channel_id=1, replica_groups=mesh['sp_0'=8,'sp_1'=4,'sp_2'=2,'tp'=4] {'sp_0'}, dimensions={0}, use_global_device_ids=true | all-gather | bytes 144 | tf_op jit(solution)/shard_map/all_gather | solution.py:47
  212.2 74.4 %while.42 = (s32[]{:T(128)}, f32[8,64,128]{2,1,0:T(8,128)S(1)}, f32[6,128,8,64]{1,0,3,2:T(8,128)S(1)}, f32[6,128,8]{2,1,0:T(8,128)}, f32[6,128,8,64]{1,0,3,2:T(8...) while((s32[]{:T(128)}, f32[8,64,128]{2,1,0:T(8,128)S(1)}, ...), condition=%wide.region_9.10_spmd.clone, body=%wide.region_7.9_spmd.clone.sunk | while | flops 156188672 | bytes 3768652 | solution.py:232
  219.5 5.1 dynamic_update_slice.32
  231.9 5.1 dynamic_update_slice.32
  244.3 5.1 dynamic_update_slice.32
  256.7 5.1 dynamic_update_slice.32
  286.6 12.8 %all-gather.3 = bf16[16,64,128]{2,1,0:T(8,128)(2,1)S(1)} all-gather(bf16[8,64,128]{2,1,0:T(8,128)(2,1)S(1)} %convert_element_type.740), channel_id=5, replica_groups=mesh['sp_0'=8,'sp_1'=4,'sp_2'=2,'tp'=4] {'sp_2'}, dimensions={0}, use_global_device_ids=true | all-gather | bytes 393216 | tf_op jit(solution)/shard_map/all_gather | solution.py:47
  300.2 10.2 %all_gather.68 = bf16[4,8,64,128]{3,2,1,0:T(8,128)(2,1)S(1)} all-gather(bf16[1,8,64,128]{3,2,1,0:T(8,128)(2,1)S(1)} %fusion.172), channel_id=1, replica_groups=mesh['sp_0'=8,'sp_1'=4,'sp_2'=2,'tp'=4] {'sp_1'}, dimensions={0}, use_global_device_ids=true | all-gather | bytes 655360 | tf_op jit(solution)/shard_map/all_gather | solution.py:47
  317.4 80.1 %while.41 = (s32[]{:T(128)}, f32[8,64,128]{2,1,0:T(8,128)S(1)}, f32[6,128,8,64]{1,0,3,2:T(8,128)}, f32[6,128,8]{2,1,0:T(8,128)}, f32[6,128,8,64]{1,0,3,2:T(8,128...) while((s32[]{:T(128)}, f32[8,64,128]{2,1,0:T(8,128)S(1)}, ...), condition=%wide.region_3.4_spmd.clone, body=%wide.region_1.3_spmd.clone.sunk | while | flops 156188672 | bytes 3768652 | solution.py:232
  323.1 7.7 %dynamic_update_slice.31 = f32[6,128,8,64]{1,0,3,2:T(8,128)} dynamic-update-slice(f32[6,128,8,64]{1,0,3,2:T(8,128)} %get-tuple-element.665, f32[1,128,8,64]{1,0,3,2:T(1,128)S(1)} %bitcast.674, s32[]{:T(128)S(6)} %copy.178, s32[]{:T(128)} %constant.172.clone.1..sunk.1, s32[]{:T(128)} %constant.172.clone.1..sunk.1, s32[]{:T(128)} %constant.172.clone.1..sunk.1) | dynamic-update-slice | bytes 524292 | tf_op jit(solution)/shard_map/while/body/jit(dynamic_update_index_in_dim)/dynamic_update_slice | solution.py:232
  336.4 7.7 %dynamic_update_slice.31 = f32[6,128,8,64]{1,0,3,2:T(8,128)} dynamic-update-slice(f32[6,128,8,64]{1,0,3,2:T(8,128)} %get-tuple-element.665, f32[1,128,8,64]{1,0,3,2:T(1,128)S(1)} %bitcast.674, s32[]{:T(128)S(6)} %copy.178, s32[]{:T(128)} %constant.172.clone.1..sunk.1, s32[]{:T(128)} %constant.172.clone.1..sunk.1, s32[]{:T(128)} %constant.172.clone.1..sunk.1) | dynamic-update-slice | bytes 524292 | tf_op jit(solution)/shard_map/while/body/jit(dynamic_update_index_in_dim)/dynamic_update_slice | solution.py:232
  349.8 7.7 %dynamic_update_slice.31 = f32[6,128,8,64]{1,0,3,2:T(8,128)} dynamic-update-slice(f32[6,128,8,64]{1,0,3,2:T(8,128)} %get-tuple-element.665, f32[1,128,8,64]{1,0,3,2:T(1,128)S(1)} %bitcast.674, s32[]{:T(128)S(6)} %copy.178, s32[]{:T(128)} %constant.172.clone.1..sunk.1, s32[]{:T(128)} %constant.172.clone.1..sunk.1, s32[]{:T(128)} %constant.172.clone.1..sunk.1) | dynamic-update-slice | bytes 524292 | tf_op jit(solution)/shard_map/while/body/jit(dynamic_update_index_in_dim)/dynamic_update_slice | solution.py:232
  363.2 7.7 %dynamic_update_slice.31 = f32[6,128,8,64]{1,0,3,2:T(8,128)} dynamic-update-slice(f32[6,128,8,64]{1,0,3,2:T(8,128)} %get-tuple-element.665, f32[1,128,8,64]{1,0,3,2:T(1,128)S(1)} %bitcast.674, s32[]{:T(128)S(6)} %copy.178, s32[]{:T(128)} %constant.172.clone.1..sunk.1, s32[]{:T(128)} %constant.172.clone.1..sunk.1, s32[]{:T(128)} %constant.172.clone.1..sunk.1) | dynamic-update-slice | bytes 524292 | tf_op jit(solution)/shard_map/while/body/jit(dynamic_update_index_in_dim)/dynamic_update_slice | solution.py:232
  376.5 7.7 %dynamic_update_slice.31 = f32[6,128,8,64]{1,0,3,2:T(8,128)} dynamic-update-slice(f32[6,128,8,64]{1,0,3,2:T(8,128)} %get-tuple-element.665, f32[1,128,8,64]{1,0,3,2:T(1,128)S(1)} %bitcast.674, s32[]{:T(128)S(6)} %copy.178, s32[]{:T(128)} %constant.172.clone.1..sunk.1, s32[]{:T(128)} %constant.172.clone.1..sunk.1, s32[]{:T(128)} %constant.172.clone.1..sunk.1) | dynamic-update-slice | bytes 524292 | tf_op jit(solution)/shard_map/while/body/jit(dynamic_update_index_in_dim)/dynamic_update_slice | solution.py:232
  389.8 7.7 %dynamic_update_slice.31 = f32[6,128,8,64]{1,0,3,2:T(8,128)} dynamic-update-slice(f32[6,128,8,64]{1,0,3,2:T(8,128)} %get-tuple-element.665, f32[1,128,8,64]{1,0,3,2:T(1,128)S(1)} %bitcast.674, s32[]{:T(128)S(6)} %copy.178, s32[]{:T(128)} %constant.172.clone.1..sunk.1, s32[]{:T(128)} %constant.172.clone.1..sunk.1, s32[]{:T(128)} %constant.172.clone.1..sunk.1) | dynamic-update-slice | bytes 524292 | tf_op jit(solution)/shard_map/while/body/jit(dynamic_update_index_in_dim)/dynamic_update_slice | solution.py:232
  403.6 11.0 %all_gather.61 = bf16[4,8,64,128]{3,2,1,0:T(8,128)(2,1)S(1)} all-gather(bf16[1,8,64,128]{3,2,1,0:T(8,128)(2,1)S(1)} %fusion.168), channel_id=1, replica_groups=mesh['sp_0'=8,'sp_1'=4,'sp_2'=2,'tp'=4] {'sp_1'}, dimensions={0}, use_global_device_ids=true | all-gather | bytes 655360 | tf_op jit(solution)/shard_map/all_gather | solution.py:47
  421.6 19.3 %while.40 = (s32[]{:T(128)}, bf16[3,256,512]{2,1,0:T(8,128)(2,1)S(1)}, f32[3,256,8]{1,2,0:T(8,128)}, s32[3]{0:T(128)S(1)}, bf16[1024,256]{0,1:T(8,128)(2,1)S(1)}...) while((s32[]{:T(128)}, ...), condition=%wide.region_17.18_spmd, body=%wide.region_14.17_spmd.sunk | while | flops 280901888 | bytes 15614348 | solution.py:307
  465.1 8.7 %fusion.78 = bf16[768,2048]{1,0:T(8,128)(2,1)S(1)} fusion(bf16[2048,3088]{1,0:T(8,128)(2,1)} %all-gather.12.cloned.1.call-done, bf16[768,512]{0,1:T(8,128)(2,1)S(1)} %copy-done.11, bf16[768,512]{0,1:T(8,128)(2,1)S(1)} %multiply_convert_fusion.1), kind=kOutput, calls=%fused_computation.107 | convolution fusion | flops 3225944064 | bytes 8912896 | tf_op jit(solution)/shard_map/dot_general | solution.py:311
  474.1 35.5 %all_to_all.5 = bf16[4,768,512]{2,1,0:T(8,128)(2,1)S(1)} all-to-all(bf16[4,768,512]{2,1,0:T(8,128)(2,1)S(1)} %bitcast.677), channel_id=1, replica_groups=mesh['sp_0'=8,'sp_1'=4,'sp_2'=2,'tp'=4] {'tp'}, dimensions={0} | all-to-all | bytes 6291456 | tf_op jit(solution)/shard_map/all_to_all | solution.py:87
  (455 shorter events, 225.3 us)
Async XLA Ops:
  7.2 98.4 %all-gather.12.cloned.1.call-start = ((), (), s32[]{:S(2)}) async-start(), calls=%async_computation.1 | async-start | bytes 13312000 | tf_op jit(solution)/shard_map/all_gather | solution.py:25
  10.4 431.6 %all-gather.16.cloned.1.call-start = ((), (), s32[]{:S(2)}) async-start(), calls=%async_computation.3 | async-start | bytes 1179648 | tf_op jit(solution)/shard_map/all_gather | solution.py:47
  18.9 105.3 %copy-start.16 = (f32[768]{0:T(1024)}, f32[768]{0:T(1024)S(1)}, u32[]{:S(2)}) copy-start(f32[768]{0:T(1024)S(1)} %add_rsqrt_fusion.1) | copy-start | bytes 9220
  110.5 310.0 %collective-permute-start.3 = (bf16[128,256]{0,1:T(8,128)(2,1)}, bf16[128,256]{0,1:T(8,128)(2,1)}, u32[]{:S(2)}, u32[]{:S(2)}) collective-permute-start(bf16[128,256]{0,1:T(8,128)(2,1)} %get-tuple-element.360), channel_id=1, source_target_pairs={{4,0},{8,4},{12,8},{16,12},{20,16},{24,20},{28,24},{32,28},{36,32}... | collective-permute-start | bytes 196616 | tf_op jit(solution)/shard_map/ppermute | solution.py:72
  112.6 307.8 %collective-permute-start.2 = (bf16[128,256]{0,1:T(8,128)(2,1)}, bf16[128,256]{0,1:T(8,128)(2,1)}, u32[]{:S(2)}, u32[]{:S(2)}) collective-permute-start(bf16[128,256]{0,1:T(8,128)(2,1)} %get-tuple-element.359), channel_id=1, source_target_pairs={{0,4},{4,8},{8,12},{12,16},{16,20},{20,24},{24,28},{28,32},{32,36}... | collective-permute-start | bytes 196616 | tf_op jit(solution)/shard_map/ppermute | solution.py:70
  129.6 61.4 %collective-permute-start.1 = (bf16[2,768]{1,0:T(2,128)(2,1)S(1)}, bf16[2,768]{1,0:T(2,128)(2,1)S(1)}, u32[]{:S(2)}, u32[]{:S(2)}) collective-permute-start(bf16[2,768]{1,0:T(2,128)(2,1)S(1)} %get-tuple-element.354), channel_id=1, source_target_pairs={{4,0},{8,4},{12,8},{16,12},{20,16},{24,20},{28,24},{32,28},{36,32}... | collective-permute-start | bytes 9224 | tf_op jit(solution)/shard_map/ppermute | solution.py:72
  131.6 59.4 %collective-permute-start = (bf16[2,768]{1,0:T(2,128)(2,1)S(1)}, bf16[2,768]{1,0:T(2,128)(2,1)S(1)}, u32[]{:S(2)}, u32[]{:S(2)}) collective-permute-start(bf16[2,768]{1,0:T(2,128)(2,1)S(1)} %get-tuple-element.353), channel_id=1, source_target_pairs={{0,4},{4,8},{8,12},{12,16},{16,20},{20,24},{24,28},{28,32},{32,36}... | collective-permute-start | bytes 9224 | tf_op jit(solution)/shard_map/ppermute | solution.py:70
  286.6 26.3 %copy-start.12 = (f32[6,128,8]{1,0,2:T(8,128)S(1)}, f32[6,128,8]{1,0,2:T(8,128)}, u32[]{:S(2)}) copy-start(f32[6,128,8]{1,0,2:T(8,128)} %copy.92) | copy-start | bytes 73732
  312.8 143.6 %all-gather.14.cloned.1.call-start = ((), (), s32[]{:S(2)}) async-start(), calls=%async_computation.2 | async-start | bytes 1179648 | tf_op jit(solution)/shard_map/all_gather | solution.py:47
  421.4 20.7 %copy-start.7 = (bf16[16,64,128]{2,1,0:T(8,128)(2,1)S(1)}, bf16[16,64,128]{2,1,0:T(8,128)(2,1)}, u32[]{:S(2)}) copy-start(bf16[16,64,128]{2,1,0:T(8,128)(2,1)} %copy-done.6) | copy-start | bytes 786436
  421.4 20.6 %copy-start.13 = (f32[768,8]{0,1:T(8,128)S(1)}, f32[768,8]{0,1:T(8,128)}, u32[]{:S(2)}) copy-start(f32[768,8]{0,1:T(8,128)} %exponential_bitcast_fusion) | copy-start | bytes 73732
  421.4 20.6 %copy-start.20 = (f32[8]{0:T(128)S(1)}, f32[8]{0:T(128)}, u32[]{:S(2)}) copy-start(f32[8]{0:T(128)} %get-tuple-element.404) | copy-start | bytes 100
  421.5 20.6 %copy-start.21 = (f32[8]{0:T(128)S(1)}, f32[8]{0:T(128)}, u32[]{:S(2)}) copy-start(f32[8]{0:T(128)} %get-tuple-element.406) | copy-start | bytes 100
  421.5 20.6 %copy-start.23 = (f32[8]{0:T(128)S(1)}, f32[8]{0:T(128)}, u32[]{:S(2)}) copy-start(f32[8]{0:T(128)} %get-tuple-element.397) | copy-start | bytes 100
  421.5 20.6 %copy-start.27 = (f32[8]{0:T(128)S(1)}, f32[8]{0:T(128)}, u32[]{:S(2)}) copy-start(f32[8]{0:T(128)} %get-tuple-element.398) | copy-start | bytes 100
  421.5 20.6 %copy-start.28 = (f32[8]{0:T(128)S(1)}, f32[8]{0:T(128)}, u32[]{:S(2)}) copy-start(f32[8]{0:T(128)} %get-tuple-element.399) | copy-start | bytes 100
  421.5 20.6 %copy-start.29 = (f32[8]{0:T(128)S(1)}, f32[8]{0:T(128)}, u32[]{:S(2)}) copy-start(f32[8]{0:T(128)} %get-tuple-element.400) | copy-start | bytes 100
  421.5 20.6 %copy-start.31 = (f32[8]{0:T(128)S(1)}, f32[8]{0:T(128)}, u32[]{:S(2)}) copy-start(f32[8]{0:T(128)} %get-tuple-element.329) | copy-start | bytes 100
  421.5 20.6 %copy-start.40 = (f32[8]{0:T(128)S(1)}, f32[8]{0:T(128)}, u32[]{:S(2)}) copy-start(f32[8]{0:T(128)} %get-tuple-element.383) | copy-start | bytes 100
  421.5 20.6 %copy-start.41 = (f32[8]{0:T(128)S(1)}, f32[8]{0:T(128)}, u32[]{:S(2)}) copy-start(f32[8]{0:T(128)} %get-tuple-element.384) | copy-start | bytes 100
  421.5 20.6 %copy-start.42 = (f32[8]{0:T(128)S(1)}, f32[8]{0:T(128)}, u32[]{:S(2)}) copy-start(f32[8]{0:T(128)} %get-tuple-element.385) | copy-start | bytes 100
  421.5 20.6 %copy-start.43 = (f32[8]{0:T(128)S(1)}, f32[8]{0:T(128)}, u32[]{:S(2)}) copy-start(f32[8]{0:T(128)} %get-tuple-element.386) | copy-start | bytes 100
  421.6 20.6 %copy-start.44 = (f32[8]{0:T(128)S(1)}, f32[8]{0:T(128)}, u32[]{:S(2)}) copy-start(f32[8]{0:T(128)} %get-tuple-element.387) | copy-start | bytes 100
  421.6 20.6 %copy-start.45 = (f32[8]{0:T(128)S(1)}, f32[8]{0:T(128)}, u32[]{:S(2)}) copy-start(f32[8]{0:T(128)} %get-tuple-element.388) | copy-start | bytes 100
  (33 other events, 296.4 us)
Sparse Core Ops, SparseCore 0:
  10.7 94.7 all-gather.11
  313.0 35.8 all-gather.15
  420.6 35.8 all-gather.13
where the time goes:
time: 528 us; the launch traced here: 518 us
  local copies, waits for them, and re-layouts  168 us (32%)
  blocking collectives  114 us (22%)
  waiting for transfers between devices  90.9 us (17%)
  matrix products  74.4 us (14%)
  other arithmetic  41 us (8%)
  between operations  15.4 us (3%)
  starting transfers between devices  11.2 us (2%)
    all_gather x1, waiting for transfers between devices, turned_gather(): out = lax.all_gather(both, axis, axis=0, tiled=True)  86.2 us
    dynamic_update_slice x12, local copies, waits for them, and re-layouts, direction(): end_state, local = lax.scan(block_ssd, start_state, shaped)  76.7 us
    all_gather x8, blocking collectives, carried_in(): lax.all_gather(part.astype(kind), axis)  76.1 us
    all_to_all x1, blocking collectives, sent_and_summed(): lax.all_to_all(parts, axis, split_axis=0, concat_axis=0, tiled=True)  35.5 us
    dynamic_slice x12, local copies, waits for them, and re-layouts, direction(): end_state, local = lax.scan(block_ssd, start_state, shaped)  22.4 us
    dot_general x5, matrix products, shards(): jnp.dot(normed, matrix, preferred_element_type=jnp.float32)  20.3 us
    another operation x20, local copies, waits for them, and re-layouts  18.8 us
    dot_general x12, matrix products, block_ssd(): jnp.einsum('lsh,shp->lhp', intersection * weight, xdt, precision=HIGH)  12.7 us
  transfers between devices with their start and end apart: 7, of which 2 were waited for; matrix products, arithmetic and copies ran while one was open for 49% of the time, Pallas kernels for 0%

commit v1 on v0

v1 whole, which is shorter than its diff:
```python
import functools

import jax
import jax.numpy as jnp
from jax import lax
from jax.experimental import pallas as pl
from jax.experimental.pallas import tpu as pltpu
from jax.sharding import Mesh
from jax.sharding import PartitionSpec as P

HEAD_DIM = 64
STATE = 128
HEADS = 8
BLOCK = 128
WINDOW = 128
GRID_W = 64
HALO = 16
SP = ("sp_0", "sp_1", "sp_2")
EPS = 1e-06
ROPE_BASE = 10000.0
F32 = jnp.float32
BF16 = jnp.bfloat16
MSG = STATE + 16


def dot(a, b, dims=((1,), (0,)), precision=None):
    return lax.dot_general(
        a, b, (dims, ((), ())), preferred_element_type=F32, precision=precision
    )


def split_bf16(value, parts):
    pieces = []
    for _ in range(parts):
        piece = value.astype(BF16)
        pieces.append(piece)
        value = value - piece.astype(F32)
    return pieces


def spread(value, spread_matrix, parts):
    pieces = [p.astype(F32) for p in split_bf16(value, parts)]
    joined = jnp.concatenate(pieces, axis=1).astype(BF16)
    matrix = jnp.concatenate([spread_matrix] * parts, axis=0)
    return dot(joined, matrix)


def spread_matrix():
    rows = jnp.arange(2 * HEADS)[:, None]
    cols = jnp.arange(2 * HEADS * HEAD_DIM)[None, :] // HEAD_DIM
    return (rows == cols).astype(BF16)


def project_kernel(tok_ref, gain_ref, w_ref, ws_ref, out_ref, step_ref, normed):
    @pl.when(pl.program_id(0) == 0)
    def _():
        def one(i, carry):
            rows = pl.ds(i * BLOCK, BLOCK)
            wide = tok_ref[rows, :].astype(F32)
            scale = lax.rsqrt(jnp.mean(wide * wide, axis=1, keepdims=True) + EPS)
            normed[rows, :] = (wide * scale * gain_ref[...]).astype(BF16)
            return carry

        lax.fori_loop(0, tok_ref.shape[0] // BLOCK, one, 0)
        step_ref[...] = dot(normed[...], ws_ref[...])

    out_ref[...] = dot(normed[...], w_ref[...]).astype(BF16)


def project(tokens, gain, weights, step_weights):
    count, width = tokens.shape
    columns = weights.shape[1]
    tile = 256
    return pl.pallas_call(
        project_kernel,
        grid=(columns // tile,),
        in_specs=[
            pl.BlockSpec((count, width), lambda j: (0, 0), pipeline_mode=pl.Buffered(1)),
            pl.BlockSpec((1, width), lambda j: (0, 0)),
            pl.BlockSpec((width, tile), lambda j: (0, j)),
            pl.BlockSpec((width, 128), lambda j: (0, 0), pipeline_mode=pl.Buffered(1)),
        ],
        out_specs=[
            pl.BlockSpec((count, tile), lambda j: (0, j)),
            pl.BlockSpec((count, 128), lambda j: (0, 0)),
        ],
        out_shape=[
            jax.ShapeDtypeStruct((count, columns), BF16),
            jax.ShapeDtypeStruct((count, 128), F32),
        ],
        scratch_shapes=[pltpu.VMEM((count, width), BF16)],
        compiler_params=pltpu.CompilerParams(vmem_limit_bytes=16 << 20),
        cost_estimate=pl.CostEstimate(
            flops=2 * count * width * (columns + 128),
            bytes_accessed=2 * (count * width + width * columns + count * columns),
            transcendentals=0,
        ),
        name="project",
    )(tokens, gain, weights, step_weights)


def conv_state_kernel(
    cin_ref, before_ref, after_ref, taps_ref, step_ref, rate_ref, e_ref,
    conv_ref, col_ref, row_ref, piece_ref, etot_ref, msg_ref, win, near,
):
    count = cin_ref.shape[0]
    blocks = count // BLOCK
    channels = HEADS * HEAD_DIM
    spread_m = e_ref[...]
    lane16 = lax.broadcasted_iota(jnp.int32, (BLOCK, 2 * HEADS), 1)
    forward16 = lane16 < HEADS
    tri = (
        lax.broadcasted_iota(jnp.int32, (BLOCK, BLOCK), 0)
        >= lax.broadcasted_iota(jnp.int32, (BLOCK, BLOCK), 1)
    ).astype(F32)
    win[pl.ds(0, HALO), :] = before_ref[...].astype(F32)
    win[pl.ds(HALO + count, HALO), :] = after_ref[...].astype(F32)

    def fill(i, carry):
        start = pl.multiple_of(i * BLOCK, BLOCK)
        win[pl.ds(HALO + start, BLOCK), :] = cin_ref[pl.ds(start, BLOCK), :].astype(F32)
        return carry

    lax.fori_loop(0, blocks, fill, 0)

    def one(i, total):
        start = pl.multiple_of(i * BLOCK, BLOCK)
        rows = pl.ds(start, BLOCK)
        near[...] = win[pl.ds(start, BLOCK + 2 * HALO), :]
        acc = near[HALO - 2 : HALO - 2 + BLOCK, :] * taps_ref[0:1, :]
        for tap in range(1, 5):
            first = HALO - 2 + tap
            acc = acc + near[first : first + BLOCK, :] * taps_ref[tap : tap + 1, :]
        conv = (acc * jax.nn.sigmoid(acc)).astype(BF16)
        conv_ref[rows, :] = conv
        raw = step_ref[rows, 0 : 2 * HEADS]
        step = jnp.maximum(raw, 0.0) + jnp.log1p(jnp.exp(-jnp.abs(raw)))
        decay = -jnp.exp(rate_ref[rows, :]) * step
        cum = dot(tri, decay, precision=lax.Precision.HIGHEST)
        tot = cum[BLOCK - 1 : BLOCK, :]
        col = jnp.where(forward16, cum, cum - decay)
        col_ref[rows, 0 : 2 * HEADS] = col
        col_ref[rows, 2 * HEADS : 4 * HEADS] = jnp.broadcast_to(tot, (BLOCK, 2 * HEADS))
        both = jnp.concatenate([col, step, jnp.zeros((BLOCK, 128 - 4 * HEADS), F32)], axis=1)
        row_ref[i] = both.T[0 : 4 * HEADS, :]
        weight = jnp.exp(jnp.where(forward16, tot - col, col)) * step
        wide = spread(weight, spread_m, 2)
        xs = conv[:, 0:channels].astype(F32)
        scaled = (jnp.concatenate([xs, xs], axis=1) * wide).astype(BF16)
        inflow = conv[:, channels : channels + STATE]
        piece_ref[i] = dot(inflow, scaled, ((0,), (0,)))
        etot_ref[i] = spread(jnp.exp(jnp.broadcast_to(tot, (8, 2 * HEADS))), spread_m, 3)
        return total + tot

    total = lax.fori_loop(0, blocks, one, jnp.zeros((1, 2 * HEADS), F32))
    forward = piece_ref[0, :, 0:channels]
    backward = piece_ref[blocks - 1, :, channels : 2 * channels]
    for i in range(1, blocks):
        forward = etot_ref[i, 0:1, 0:channels] * forward + piece_ref[i, :, 0:channels]
        k = blocks - 1 - i
        backward = (
            etot_ref[k, 0:1, channels : 2 * channels] * backward
            + piece_ref[k, :, channels : 2 * channels]
        )
    spread_total = spread(jnp.broadcast_to(total, (16, 2 * HEADS)), spread_m, 3)
    hi, mid, lo = split_bf16(spread_total, 3)
    which = lax.broadcasted_iota(jnp.int32, (16, 2 * channels), 0)
    tail = jnp.where(
        which == 0, hi.astype(F32), jnp.where(which == 1, mid.astype(F32), lo.astype(F32))
    ).astype(BF16)
    for e, state in enumerate((forward, backward)):
        for pair in range(channels // 128):
            lanes = slice(pair * 128, pair * 128 + 128)
            msg_ref[e, pair, 0:STATE, :] = state[:, lanes].astype(BF16)
            msg_ref[e, pair, STATE:MSG, :] = tail[:, e * channels + pair * 128 : e * channels + pair * 128 + 128]


def conv_state(proj, before, after, taps, step_raw, rate, spread_m):
    count = proj.shape[0]
    width = before.shape[1]
    blocks = count // BLOCK
    channels = HEADS * HEAD_DIM
    whole = lambda shape: pl.BlockSpec(shape, lambda i: (0,) * len(shape))
    return pl.pallas_call(
        conv_state_kernel,
        grid=(1,),
        in_specs=[
            pl.BlockSpec((count, width), lambda i: (0, 0)),
            whole((HALO, width)),
            whole((HALO, width)),
            whole(taps.shape),
            whole(step_raw.shape),
            whole(rate.shape),
            whole(spread_m.shape),
        ],
        out_specs=[
            whole((count, width)),
            whole((count, 4 * HEADS)),
            whole((blocks, 4 * HEADS, BLOCK)),
            whole((blocks, STATE, 2 * channels)),
            whole((blocks, 8, 2 * channels)),
            whole((2, channels // 128, MSG, 128)),
        ],
        out_shape=[
            jax.ShapeDtypeStruct((count, width), BF16),
            jax.ShapeDtypeStruct((count, 4 * HEADS), F32),
            jax.ShapeDtypeStruct((blocks, 4 * HEADS, BLOCK), F32),
            jax.ShapeDtypeStruct((blocks, STATE, 2 * channels), F32),
            jax.ShapeDtypeStruct((blocks, 8, 2 * channels), F32),
            jax.ShapeDtypeStruct((2, channels // 128, MSG, 128), BF16),
        ],
        scratch_shapes=[
            pltpu.VMEM((count + 2 * HALO, width), F32),
            pltpu.VMEM((BLOCK + 2 * HALO, width), F32),
        ],
        compiler_params=pltpu.CompilerParams(vmem_limit_bytes=18 << 20),
        cost_estimate=pl.CostEstimate(
            flops=2 * count * STATE * 2 * channels, bytes_accessed=12 << 20, transcendentals=0
        ),
        name="conv_state",
    )(proj, before, after, taps, step_raw, rate, spread_m)


def mix_kernel(
    conv_ref, col_ref, row_ref, piece_ref, etot_ref, in_ref, gate_ref, gain_ref, e_ref,
    out_ref, held,
):
    count = conv_ref.shape[0]
    blocks = count // BLOCK
    channels = HEADS * HEAD_DIM
    spread_m = e_ref[...]
    for e in range(2):
        state = jnp.concatenate(
            [in_ref[e, p].astype(F32) for p in range(channels // 128)], axis=1
        )
        lanes = slice(e * channels, (e + 1) * channels)
        for i in range(blocks) if e == 0 else reversed(range(blocks)):
            held[i, :, lanes] = state.astype(BF16)
            state = etot_ref[i, 0:1, lanes] * state + piece_ref[i, :, lanes]
    row_at = lax.broadcasted_iota(jnp.int32, (BLOCK, BLOCK), 0)
    col_at = lax.broadcasted_iota(jnp.int32, (BLOCK, BLOCK), 1)
    lower = row_at >= col_at
    diagonal = row_at == col_at
    first_half = col_at < HEAD_DIM
    forward16 = lax.broadcasted_iota(jnp.int32, (BLOCK, 2 * HEADS), 1) < HEADS

    def one(i, carry):
        rows = pl.ds(pl.multiple_of(i * BLOCK, BLOCK), BLOCK)
        inflow = conv_ref[rows, channels : channels + STATE]
        readout = conv_ref[rows, channels + STATE : channels + 2 * STATE]
        inner = dot(readout, inflow, ((1,), (1,)))
        col = col_ref[rows, 0 : 2 * HEADS]
        tot = col_ref[rows, 2 * HEADS : 4 * HEADS]
        reach = spread(jnp.exp(jnp.where(forward16, col, tot - col)), spread_m, 2)
        far = dot(readout, held[i]) * reach
        parts = []
        for pair in range(HEADS // 2):
            weights = []
            for h in (2 * pair, 2 * pair + 1):
                b = HEADS + h
                arg = jnp.where(
                    lower,
                    col[:, h : h + 1] - row_ref[i, h : h + 1, :],
                    row_ref[i, b : b + 1, :] - col[:, b : b + 1],
                )
                step_f = row_ref[i, 2 * HEADS + h : 2 * HEADS + h + 1, :]
                step_b = row_ref[i, 2 * HEADS + b : 2 * HEADS + b + 1, :]
                step = jnp.where(lower, step_f, step_b) + jnp.where(diagonal, step_b, 0.0)
                weights.append((inner * jnp.exp(arg) * step).astype(BF16))
            xs = conv_ref[rows, pair * 128 : pair * 128 + 128]
            zero = jnp.zeros_like(xs)
            stacked = jnp.concatenate(
                [jnp.where(first_half, xs, zero), jnp.where(first_half, zero, xs)], axis=0
            )
            parts.append(dot(jnp.concatenate(weights, axis=1), stacked))
        y = jnp.concatenate(parts, axis=1) + far[:, 0:channels] + far[:, channels:]
        gate = gate_ref[rows, :].astype(F32)
        y = y * (gate * jax.nn.sigmoid(gate))
        y = y * lax.rsqrt(jnp.mean(y * y, axis=1, keepdims=True) + EPS)
        out_ref[rows, :] = (y * gain_ref[...]).astype(BF16)
        return carry

    lax.fori_loop(0, blocks, one, 0)


def mix(conv, col, row, piece, etot, incoming, proj, gate_block, gain, spread_m):
    count = conv.shape[0]
    blocks = count // BLOCK
    channels = HEADS * HEAD_DIM
    whole = lambda shape: pl.BlockSpec(shape, lambda i: (0,) * len(shape))
    return pl.pallas_call(
        mix_kernel,
        grid=(1,),
        in_specs=[
            whole(conv.shape), whole(col.shape), whole(row.shape), whole(piece.shape),
            whole(etot.shape), whole(incoming.shape),
            pl.BlockSpec((count, channels), lambda i: (0, gate_block)),
            whole(gain.shape), whole(spread_m.shape),
        ],
        out_specs=whole((count, channels)),
        out_shape=jax.ShapeDtypeStruct((count, channels), BF16),
        scratch_shapes=[pltpu.VMEM((blocks, STATE, 2 * channels), BF16)],
        compiler_params=pltpu.CompilerParams(vmem_limit_bytes=16 << 20),
        cost_estimate=pl.CostEstimate(
            flops=2 * count * BLOCK * 4 * channels, bytes_accessed=8 << 20, transcendentals=0
        ),
        name="mix",
    )(conv, col, row, piece, etot, incoming, proj, gain, spread_m)


def rope_tables(first_row, grid_rows):
    quarter = HEAD_DIM // 4
    lane = jnp.arange(2 * HEAD_DIM)
    freqs = ROPE_BASE ** (-(lane % quarter).astype(F32) / quarter)
    sign = jnp.where(lane % (2 * quarter) < quarter, -1.0, 1.0)
    row_angle = (first_row + jnp.arange(grid_rows, dtype=jnp.int32)).astype(F32)[:, None] * freqs
    col_angle = jnp.arange(GRID_W, dtype=jnp.int32).astype(F32)[:, None] * freqs
    return (
        jnp.stack([jnp.cos(row_angle), jnp.sin(row_angle) * sign]),
        jnp.stack([jnp.cos(col_angle), jnp.sin(col_angle) * sign]),
    )


def attend_kernel(
    at_ref, q_ref, kv_ref, before_ref, after_ref, by_row_ref, by_col_ref, sink_ref,
    out_ref, log_ref, keys, values,
):
    count = kv_ref.shape[0]
    blocks = count // BLOCK
    lane = lax.broadcasted_iota(jnp.int32, (BLOCK, 128), 1)
    low_quarter = lane % 32 < 16
    first_half = lane < HEAD_DIM
    row_lane = (lane % HEAD_DIM < 32)[0:GRID_W]

    def tables(slot):
        out = []
        for kind in range(2):
            parts = []
            for r in range(BLOCK // GRID_W):
                row = by_row_ref[kind, pl.ds(slot * (BLOCK // GRID_W) + r, 1), :]
                parts.append(jnp.where(row_lane, row, by_col_ref[kind]))
            out.append(jnp.concatenate(parts, axis=0))
        return out

    def turn(value, table):
        wide = value.astype(F32)
        other = jnp.where(low_quarter, pltpu.roll(wide, 112, 1), pltpu.roll(wide, 16, 1))
        return (wide * table[0] + other * table[1]).astype(BF16)

    def store(raw, slot):
        rows = pl.ds(pl.multiple_of(slot * BLOCK, BLOCK), BLOCK)
        key = turn(raw[:, 0:128], tables(slot)).astype(F32)
        swapped = pltpu.roll(key, 64, 1)
        keys[0, rows, :] = jnp.where(first_half, key, swapped).astype(BF16)
        keys[1, rows, :] = jnp.where(first_half, swapped, key).astype(BF16)
        values[:, rows] = raw[:, 128:256].astype(F32).T.astype(BF16)

    store(before_ref[...], 0)
    store(after_ref[...], blocks + 1)

    def fill(i, carry):
        store(kv_ref[pl.ds(pl.multiple_of(i * BLOCK, BLOCK), BLOCK), :], i + 1)
        return carry

    lax.fori_loop(0, blocks, fill, 0)
    key_at = lax.broadcasted_iota(jnp.int32, (3 * BLOCK, 2 * BLOCK), 0)
    query_at = lax.broadcasted_iota(jnp.int32, (3 * BLOCK, 2 * BLOCK), 1) % BLOCK
    in_band = (key_at >= query_at) & (key_at <= query_at + 2 * WINDOW)
    start_at = at_ref[0]
    end_at = at_ref[1]

    def one(i, carry):
        start = pl.multiple_of(i * BLOCK, BLOCK)
        rows = pl.ds(start, BLOCK)
        here = key_at + (start - WINDOW)
        valid = in_band & (here >= start_at) & (here < end_at)
        table = tables(i + 1)
        band = pl.ds(start, 3 * BLOCK)
        for pair in range(HEADS // 2):
            group = pair // 2
            lanes = slice(pair * 128, pair * 128 + 128)
            q = (turn(q_ref[rows, lanes], table).astype(F32) * HEAD_DIM ** (-0.5)).astype(BF16)
            zero = jnp.zeros_like(q)
            both = jnp.concatenate(
                [jnp.where(first_half, q, zero), jnp.where(first_half, zero, q)], axis=0
            )
            scores = dot(keys[group, band, :], both, ((1,), (1,)))
            scores = jnp.where(valid, scores, -1e30)
            sink = sink_ref[pair : pair + 1, :]
            top = jnp.maximum(jnp.max(scores, axis=0, keepdims=True), sink)
            expo = jnp.exp(scores - top)
            total = jnp.sum(expo, axis=0, keepdims=True) + jnp.exp(sink - top)
            mine = values[group * HEAD_DIM : (group + 1) * HEAD_DIM, band]
            o = dot(mine, expo.astype(BF16)) / total
            turned = jnp.concatenate([o[:, 0:BLOCK], o[:, BLOCK:]], axis=0).T
            out_ref[rows, lanes] = turned.astype(BF16)
            log = top + jnp.log(total)
            log_ref[2 * pair : 2 * pair + 1, rows] = log[:, 0:BLOCK]
            log_ref[2 * pair + 1 : 2 * pair + 2, rows] = log[:, BLOCK:]
        return carry

    lax.fori_loop(0, blocks, one, 0)


def attend(limits, proj, q_block, kv_block, before, after, tables, sinks):
    count = proj.shape[0]
    channels = HEADS * HEAD_DIM
    whole = lambda shape: pl.BlockSpec(shape, lambda i, *_: (0,) * len(shape))
    smem = pl.BlockSpec(memory_space=pltpu.SMEM)
    by_row, by_col = tables
    wide_sinks = jnp.repeat(sinks.reshape(HEADS // 2, 2), BLOCK, axis=1)
    return pl.pallas_call(
        attend_kernel,
        grid=(1,),
        in_specs=[
            smem,
            pl.BlockSpec((count, channels), lambda i: (0, q_block)),
            pl.BlockSpec((count, 256), lambda i: (0, kv_block)),
            whole(before.shape), whole(after.shape), whole(by_row.shape), whole(by_col.shape),
            whole(wide_sinks.shape),
        ],
        out_specs=[whole((count, channels)), whole((HEADS, count))],
        out_shape=[
            jax.ShapeDtypeStruct((count, channels), BF16),
            jax.ShapeDtypeStruct((HEADS, count), F32),
        ],
        scratch_shapes=[
            pltpu.VMEM((2, count + 2 * BLOCK, 128), BF16),
            pltpu.VMEM((128, count + 2 * BLOCK), BF16),
        ],
        compiler_params=pltpu.CompilerParams(vmem_limit_bytes=12 << 20),
        cost_estimate=pl.CostEstimate(
            flops=4 * count * 3 * BLOCK * channels, bytes_accessed=4 << 20, transcendentals=0
        ),
        name="attend",
    )(limits, proj, proj, before, after, by_row, by_col, wide_sinks)


def exchange_kernel(
    msg_ref, out_ref, part, turned, by_y, summed, by_z, back, arrived, nxt, final, carry,
    part_sem, y_sem, z_sem, back_sem, final_sem,
):
    z, y, c = (lax.axis_index(a) for a in SP)
    length_z, length_y = lax.axis_size(SP[0]), lax.axis_size(SP[1])
    forward = c == 0
    other = 1 - c
    order_z = jnp.where(forward, z, length_z - 1 - z)
    mesh_id = pl.DeviceIdType.MESH
    peers = [{SP[2]: other}]
    peers += [{SP[1]: lax.rem(y + k, length_y)} for k in range(1, length_y)]
    peers += [{SP[0]: lax.rem(z + k, length_z)} for k in range(1, length_z)]
    barrier = pltpu.get_barrier_semaphore()
    for peer in peers:
        pl.semaphore_signal(barrier, inc=1, device_id=peer, device_id_type=mesh_id)
    pl.semaphore_wait(barrier, len(peers))

    def send(src, dst, sems, peer):
        copy = pltpu.make_async_remote_copy(
            src_ref=src, dst_ref=dst, send_sem=sems.at[0], recv_sem=sems.at[1],
            device_id=peer, device_id_type=mesh_id,
        )
        copy.start()
        return copy

    def state_of(ref, *at):
        return ref[(*at, slice(0, STATE), slice(None))].astype(F32)

    def decay_of(ref, *at):
        tail = ref[(*at, slice(STATE, MSG), slice(None))].astype(F32)
        return tail[0:1] + tail[1:2] + tail[2:3]

    def put(ref, state, decay, *at):
        ref[(*at, slice(0, STATE), slice(None))] = state.astype(BF16)
        hi, mid, lo = (p.astype(F32) for p in split_bf16(decay, 3))
        which = lax.broadcasted_iota(jnp.int32, (MSG - STATE, 128), 0)
        tail = jnp.where(which == 0, hi, jnp.where(which == 1, mid, lo))
        ref[(*at, slice(STATE, MSG), slice(None))] = tail.astype(BF16)

    pairs = msg_ref.shape[1]
    copy = send(msg_ref.at[other], part, part_sem, {SP[2]: other})
    copy.wait()
    for j in range(pairs):
        decay = decay_of(part, j)
        put(
            turned,
            jnp.exp(decay) * state_of(msg_ref, c, j) + state_of(part, j),
            decay + decay_of(msg_ref, c, j),
            j,
        )
    copies = []
    for k in range(1, length_y):
        to = lax.rem(y + k, length_y)
        copies.append(send(turned.at[to], by_y.at[k], y_sem.at[k], {SP[1]: to}))
    by_y[0] = turned[y]
    for copy in copies:
        copy.wait()
    before = []
    state = jnp.zeros((STATE, 128), F32)
    decay = jnp.zeros((1, 128), F32)
    for q in range(length_y):
        before.append((state, decay))
        slot = jnp.where(forward, lax.rem(y - q + length_y, length_y), lax.rem(y + 1 + q, length_y))
        step = decay_of(by_y, slot)
        state = jnp.exp(step) * state + state_of(by_y, slot)
        decay = decay + step
    put(summed, state, decay)
    for k in range(1, length_z):
        to = lax.rem(z + k, length_z)

        @pl.when((z + k >= length_z) == (c == 1))
        def _():
            send(summed, by_z.at[k], z_sem.at[k], {SP[0]: to})

    carry[...] = jnp.zeros_like(carry)
    for distance in reversed(range(1, length_z)):
        slot = jnp.where(forward, distance, length_z - distance)

        @pl.when(order_z >= distance)
        def _():
            pltpu.make_async_remote_copy(
                src_ref=summed, dst_ref=by_z.at[slot], send_sem=z_sem.at[slot, 0],
                recv_sem=z_sem.at[slot, 1], device_id={SP[0]: z}, device_id_type=mesh_id,
            ).wait_recv()
            carry[...] = jnp.exp(decay_of(by_z, slot)) * carry[...] + state_of(by_z, slot)

    for k in range(1, length_z):
        to = lax.rem(z + k, length_z)

        @pl.when((z + k >= length_z) == (c == 1))
        def _():
            pltpu.make_async_remote_copy(
                src_ref=summed, dst_ref=by_z.at[k], send_sem=z_sem.at[k, 0],
                recv_sem=z_sem.at[k, 1], device_id={SP[0]: to}, device_id_type=mesh_id,
            ).wait_send()

    incoming = carry[...]
    for q in range(length_y):
        to = jnp.where(forward, q, length_y - 1 - q)
        state, decay = before[q]
        back[to] = (jnp.exp(decay) * incoming + state).astype(BF16)
    copies = []
    for k in range(1, length_y):
        to = lax.rem(y + k, length_y)
        copies.append(send(back.at[to], arrived.at[k], back_sem.at[k], {SP[1]: to}))
    arrived[0] = back[y]
    for copy in copies:
        copy.wait()
    for j in range(pairs):
        state = arrived[lax.rem(y - j + length_y, length_y)]
        out_ref[c, j] = state
        nxt[j] = (
            jnp.exp(decay_of(msg_ref, c, j)) * state.astype(F32) + state_of(msg_ref, c, j)
        ).astype(BF16)
    send(nxt, final, final_sem, {SP[2]: other}).wait()
    out_ref[other] = final[...]


def exchange(message, length_z, length_y):
    pairs = message.shape[1]
    tile = (STATE, 128)
    full = (MSG, 128)
    dma = pltpu.SemaphoreType.DMA
    return pl.pallas_call(
        exchange_kernel,
        in_specs=[pl.BlockSpec(memory_space=pltpu.VMEM)],
        out_specs=pl.BlockSpec(memory_space=pltpu.VMEM),
        out_shape=jax.ShapeDtypeStruct((2, pairs, *tile), BF16),
        scratch_shapes=[
            pltpu.VMEM((pairs, *full), BF16),
            pltpu.VMEM((pairs, *full), BF16),
            pltpu.VMEM((length_y, *full), BF16),
            pltpu.VMEM(full, BF16),
            pltpu.VMEM((length_z, *full), BF16),
            pltpu.VMEM((length_y, *tile), BF16),
            pltpu.VMEM((length_y, *tile), BF16),
            pltpu.VMEM((pairs, *tile), BF16),
            pltpu.VMEM((pairs, *tile), BF16),
            pltpu.VMEM(tile, F32),
            dma((2,)), dma((length_y, 2)), dma((length_z, 2)), dma((length_y, 2)), dma((2,)),
        ],
        compiler_params=pltpu.CompilerParams(
            collective_id=1, has_side_effects=True, vmem_limit_bytes=8 << 20
        ),
        cost_estimate=pl.CostEstimate(flops=1 << 24, bytes_accessed=1 << 20, transcendentals=0),
        name="exchange",
    )(message)


def neighbours(tail, head):
    count = lax.axis_size(SP)
    up = [(i, i + 1) for i in range(count - 1)]
    down = [(i + 1, i) for i in range(count - 1)]
    return lax.ppermute(tail, SP, up), lax.ppermute(head, SP, down)


def flatten_rows(weight):
    return weight.reshape(weight.shape[0], -1)


def shards(
    tokens, input_gain, gate_weight, value_weight, inflow_weight, readout_weight, step_weight,
    conv_values, conv_inflow, conv_readout, log_rate, group_gain, query_weight, key_weight,
    vector_weight, sink_logit, state_out, window_out,
):
    count = tokens.shape[0]
    place = lax.axis_index(SP)
    total = count * lax.axis_size(SP)
    length_z, length_y = lax.axis_size(SP[0]), lax.axis_size(SP[1])
    out_stack = jnp.concatenate([state_out, window_out], axis=0).T
    shard = jnp.concatenate(
        [
            value_weight, flatten_rows(inflow_weight), flatten_rows(readout_weight),
            key_weight, vector_weight, gate_weight, query_weight,
            jnp.pad(flatten_rows(step_weight), ((0, 0), (0, 128 - 2 * HEADS))), out_stack,
        ],
        axis=1,
    )
    gathered = lax.all_gather(shard, SP, axis=0, tiled=True)
    weights = gathered[:, 0:2048]
    step_weights = gathered[:, 2048:2176]
    out_weights = gathered[:, 2176:3200]
    proj, step_raw = project(tokens, input_gain.astype(F32)[None], weights, step_weights)
    conv_before, conv_after = neighbours(proj[-HALO:, 0:768], proj[:HALO, 0:768])
    kv_before, kv_after = neighbours(proj[-WINDOW:, 768:1024], proj[:WINDOW, 768:1024])
    spread_m = spread_matrix()
    rate = jnp.concatenate([log_rate[0], log_rate[1]], axis=1)
    taps = jnp.concatenate(
        [conv_values, flatten_rows(conv_inflow), flatten_rows(conv_readout)], axis=1
    )
    taps = jnp.pad(taps.astype(F32), ((0, 3), (0, 0)))
    conv, col, row, piece, etot, message = conv_state(
        proj, conv_before, conv_after, taps, step_raw, rate, spread_m
    )
    incoming = exchange(message, length_z, length_y)
    limits = jnp.stack([-place * count, total - place * count]).astype(jnp.int32)
    tables = rope_tables((place * count - WINDOW) // GRID_W, (count + 2 * WINDOW) // GRID_W)
    window, logs = attend(limits, proj, 3, 3, kv_before, kv_after, tables, sink_logit)
    state = mix(
        conv, col, row, piece, etot, incoming, proj, 2, group_gain.astype(F32)[None], spread_m
    )
    half = HEADS * HEAD_DIM
    terms = dot(state, out_weights[:, :half], ((1,), (1,))) + dot(
        window, out_weights[:, half:], ((1,), (1,))
    )
    n = lax.axis_size("tp")
    parts = jnp.moveaxis(terms.astype(BF16).reshape(count, n, -1), 1, 0)
    arrived = lax.all_to_all(parts, "tp", split_axis=0, concat_axis=0, tiled=True)
    mixed = arrived.astype(F32).sum(axis=0).astype(BF16)
    return mixed, logs.T


def solution(mesh):
    torus = Mesh(mesh.devices.reshape(8, 4, 2, mesh.shape["tp"]), (*SP, "tp"))
    return jax.shard_map(
        shards,
        mesh=torus,
        in_specs=(
            P(SP, None), P(), P(SP, "tp"), P(SP, "tp"), P(SP, "tp", None), P(SP, "tp", None),
            P(SP, None, "tp"), P(None, "tp"), P(None, "tp", None), P(None, "tp", None),
            P(None, SP, "tp"), P("tp"), P(SP, "tp"), P(SP, "tp"), P(SP, "tp"), P("tp"),
            P("tp", SP), P("tp", SP),
        ),
        out_specs=(P(SP, "tp"), P(SP, "tp")),
        check_vma=False,
    )
```

time: 528 us -> 262 us (0.50); the launches traced: 518 us -> 260 us
  local copies, waits for them, and re-layouts: 168 us -> 28 us
  blocking collectives: 114 us -> 41 us
  matrix products: 74.4 us -> 6.84 us
  Pallas kernels: 0 us -> 63.9 us
  other arithmetic: 41 us -> 7.87 us
    dynamic_update_slice x21 -> x0, local copies, waits for them, and re-layouts: 79 us -> none  [the longest x12 76.7 us: direction(): end_state, local = lax.scan(block_ssd, start_state, shaped)]
    all_gather x8 -> x0, blocking collectives: 76.1 us -> none  [carried_in(): lax.all_gather(part.astype(kind), axis)]
    dot_general x62 -> x2, matrix products: 74.4 us -> 6.84 us  [dot(): lax.dot_general(a, b, (dims, ((), ())), preferred_element_type=F32, preci...]
    pallas_call x0 -> x5, Pallas kernels: none -> 63.9 us  [the longest x1 26.7 us: exchange(): pl.pallas_call(exchange_kernel, in_specs=[pl.BlockSpec(memory_space=pltpu...]
    dynamic_slice x15 -> x0, local copies, waits for them, and re-layouts: 24.1 us -> none  [the longest x12 22.4 us: direction(): end_state, local = lax.scan(block_ssd, start_state, shaped)]
    another operation x32 -> x0, local copies, waits for them, and re-layouts: 19.3 us -> none
    rev x4 -> x0, local copies, waits for them, and re-layouts: 9.78 us -> none  [the longest x1 5 us: direction(): local = jnp.flip(local, 0)]
    squeeze x24 -> x1, local copies, waits for them, and re-layouts: 10.3 us -> 0.76 us  [shards(): rate = jnp.concatenate([log_rate[0], log_rate[1]], axis=1)]
  transfers between devices with their start and end apart: 7 -> 5, of which waited for: 2 -> 1; matrix products, arithmetic and copies ran while one was open for 49% -> 4% of each run, Pallas kernels for 0% -> 15%
where the time goes in v1:
time: 262 us; the launch traced here: 260 us
  waiting for transfers between devices  88.5 us (34%)
  Pallas kernels  63.9 us (24%)
  blocking collectives  41 us (16%)
  local copies, waits for them, and re-layouts  28 us (11%)
  between operations  14.3 us (5%)
  starting transfers between devices  9.86 us (4%)
  other arithmetic  7.87 us (3%)
  matrix products  6.84 us (3%)
    all_gather x1, waiting for transfers between devices, shards(): gathered = lax.all_gather(shard, SP, axis=0, tiled=True)  88.5 us
    all_to_all x1, blocking collectives, shards(): lax.all_to_all(parts, 'tp', split_axis=0, concat_axis=0, tiled=True)  41 us
    pallas_call x1, Pallas kernels, exchange(): pl.pallas_call(exchange_kernel, in_specs=[pl.BlockSpec(memory_space=pltpu...  26.7 us
    unnamed x30, local copies, waits for them, and re-layouts  13.7 us
    pallas_call x1, Pallas kernels, attend(): pl.pallas_call(attend_kernel, grid=(1,), in_specs=[smem, pl.BlockSpec((co...  13.3 us
    pallas_call x1, Pallas kernels, project(): pl.pallas_call(project_kernel, grid=(columns // tile,), in_specs=[pl.Bloc...  11.7 us
    ppermute x4, starting transfers between devices, neighbours(): return (lax.ppermute(tail, SP, up), lax.ppermute(head, SP, down))  9.83 us
    slice x1, local copies, waits for them, and re-layouts, shards(): weights = gathered[:, 0:2048]  8.43 us
  transfers between devices with their start and end apart: 5, of which 1 were waited for; matrix products, arithmetic and copies ran while one was open for 4% of the time, Pallas kernels for 15%

profile of v1, /device:TPU:1, one launch (start us, length us, event | category | flops | bytes accessed | tf_op | source)
XLA Modules:
  0.0 260.3 jit_solution(9738829189816976525)
XLA Ops:
  7.2 0.8 constant_dynamic-update-slice_fusion.7
  8.0 0.8 copy.26
  11.6 0.8 constant_dynamic-update-slice_fusion.2
  13.1 0.8 fusion.3
  16.2 1.4 fusion.11.taps_ref
  21.0 88.5 %all-gather.2.cloned.1.call-done = bf16[2048,3200]{1,0:T(8,128)(2,1)} async-done(((bf16[32,3200]{1,0:T(8,128)(2,1)}), bf16[2048,3200]{1,0:T(8,128)(2,1)}) %all-gather.2.cloned.1.call-update) | async-done | bytes 13107216 | tf_op jit(solution)/shard_map/all_gather | solution.py:618
  109.5 8.4 %slice.43.w_ref = bf16[2048,2048]{1,0:T(8,128)(2,1)} slice(bf16[2048,3200]{1,0:T(8,128)(2,1)} %all-gather.2.cloned.1.call-done), slice={[0:2048], [0:2048]} | slice | bytes 16777216 | tf_op jit(solution)/shard_map/slice | solution.py:619
  117.9 1.1 slice.44.ws_ref
  119.0 3.4 %copy-done = bf16[2048,2048]{1,0:T(8,128)(2,1)S(1)} copy-done((bf16[2048,2048]{1,0:T(8,128)(2,1)S(1)}, bf16[2048,2048]{1,0:T(8,128)(2,1)}, u32[]{:S(2)}) %copy-start) | copy-done | bytes 8388632
  122.4 11.7 %project.1 = (bf16[768,2048]{1,0:T(8,128)(2,1)S(1)}, f32[768,128]{1,0:T(8,128)S(1)}) custom-call(bf16[768,2048]{1,0:T(8,128)(2,1)S(1)} %copy-done.8, f32[1,2048]{1,0:T(1,128)S(1)} %bitcast.36, bf16[2048,2048]{1,0:T(8,128)(2,1)S(1)} %copy-done, bf16[2048,128]{1,0:T(8,128)(2,1)S(1)} %slice.44.ws_ref), custom_call_target="tpu_custom_call" | custom-call | flops 6845104128 | bytes 14680064 | tf_op jit(solution)/shard_map/project/pallas_call | solution.py:74
  136.2 2.0 collective-permute-start
  138.2 2.9 %collective-permute-start.1 = (bf16[16,768]{1,0:T(8,128)(2,1)}, bf16[16,768]{1,0:T(8,128)(2,1)}, u32[]{:S(2)}, u32[]{:S(2)}) collective-permute-start(bf16[16,768]{1,0:T(8,128)(2,1)} %get-tuple-element.22), channel_id=1, source_target_pairs={{4,0},{8,4},{12,8},{16,12},{20,16},{24,20},{28,24},{32,28},{36,32}... | collective-permute-start | bytes 73736 | tf_op jit(solution)/shard_map/ppermute | solution.py:593
  141.1 2.6 %collective-permute-start.2 = (bf16[128,256]{1,0:T(8,128)(2,1)}, bf16[128,256]{1,0:T(8,128)(2,1)}, u32[]{:S(2)}, u32[]{:S(2)}) collective-permute-start(bf16[128,256]{1,0:T(8,128)(2,1)} %get-tuple-element.25), channel_id=1, source_target_pairs={{0,4},{4,8},{8,12},{12,16},{16,20},{20,24},{24,28},{28,32},{32,36}... | collective-permute-start | bytes 196616 | tf_op jit(solution)/shard_map/ppermute | solution.py:593
  143.7 2.3 collective-permute-start.3
  146.6 1.0 copy.27.rate_ref
  149.0 1.0 copy-done.2
  151.5 7.0 %conv_state.1 = (bf16[768,768]{1,0:T(8,128)(2,1)S(1)}, f32[768,32]{1,0:T(8,128)S(1)}, f32[6,32,128]{2,1,0:T(8,128)S(1)}, f32[6,128,1024]{2,1,0:T(8,128)S(1)}, f3...) custom-call(bf16[768,2048]{1,0:T(8,128)(2,1)S(1)} %get-tuple-element.12.cin_ref.gate_ref.q_ref.kv_ref, ...), custom_call_target="tpu_custom_call" | custom-call | flops 201326592 | bytes 12582912 | tf_op jit(solution)/shard_map/conv_state/pallas_call | solution.py:184
  158.5 26.7 %exchange.1.in_ref = bf16[2,4,128,128]{3,2,1,0:T(8,128)(2,1)S(1)} custom-call(bf16[2,4,144,128]{3,2,1,0:T(8,128)(2,1)S(1)} %get-tuple-element.19.msg_ref), custom_call_target="tpu_custom_call" | custom-call | flops 16777216 | bytes 1048576 | tf_op jit(solution)/shard_map/exchange/pallas_call | solution.py:563
  185.2 5.2 %mix.1 = bf16[768,512]{1,0:T(8,128)(2,1)S(1)} custom-call(bf16[768,768]{1,0:T(8,128)(2,1)S(1)} %get-tuple-element.14.conv_ref, f32[768,32]{1,0:T(8,128)S(1)} %get-tuple-element.15.col_ref, f32[6,32,128]{2,1,0:T(8,128)S(1)} %get-tuple-element.16.row_ref, f32[6,128,1024]{2,1,0:T(8,128)S(1)} %get-tuple-element.17.piece_ref, ...), custom_call_target="tpu_custom_call" | custom-call | flops 402653184 | bytes 8388608 | tf_op jit(solution)/shard_map/mix/pallas_call | solution.py:291
  190.5 13.3 %attend.1 = (bf16[768,512]{1,0:T(8,128)(2,1)S(1)}, f32[8,768]{1,0:T(8,128)}) custom-call(s32[2]{0:T(128)S(1)} %copy-done.7, bf16[768,2048]{1,0:T(8,128)(2,1)S(1)} %get-tuple-element.12.cin_ref.gate_ref.q_ref.kv_ref, bf16[768,2048]{1,0:T(8,128)(2,1)S(1)} %get-tuple-element.12.cin_ref.gate_ref.q_ref.kv_ref, ...), custom_call_target="tpu_custom_call" | custom-call | flops 603979776 | bytes 4194304 | tf_op jit(solution)/shard_map/attend/pallas_call | solution.py:412
  203.7 3.4 %fusion = f32[768,2048]{1,0:T(8,128)S(1)} fusion(bf16[768,512]{1,0:T(8,128)(2,1)S(1)} %get-tuple-element.20, bf16[2048,3200]{1,0:T(8,128)(2,1)} %all-gather.2.cloned.1.call-done), kind=kOutput, calls=%fused_computation.2 | convolution fusion | flops 1610612736 | bytes 9175040 | tf_op jit(solution)/shard_map/dot_general | solution.py:27
  207.1 3.4 %add_convert_fusion = bf16[768,2048]{1,0:T(8,128)(2,1)S(1)} fusion(f32[768,2048]{1,0:T(8,128)S(1)} %fusion, bf16[768,512]{1,0:T(8,128)(2,1)S(1)} %mix.1, bf16[2048,3200]{1,0:T(8,128)(2,1)} %all-gather.2.cloned.1.call-done), kind=kOutput, calls=%fused_computation | convolution fusion | flops 1613758464 | bytes 12320768 | tf_op jit(solution)/shard_map/dot_general | solution.py:27
  210.9 41.0 %all_to_all.5 = bf16[4,768,512]{2,1,0:T(8,128)(2,1)S(1)} all-to-all(bf16[4,768,512]{2,1,0:T(8,128)(2,1)S(1)} %bitcast.37), channel_id=1, replica_groups=mesh['sp_0'=8,'sp_1'=4,'sp_2'=2,'tp'=4] {'tp'}, dimensions={0} | all-to-all | bytes 6291456 | tf_op jit(solution)/shard_map/all_to_all | solution.py:647
  251.9 1.6 reduce_sum.12
  (50 shorter events, 15.1 us)
Async XLA Ops:
  7.2 102.3 %all-gather.2.cloned.1.call-start = ((), (), s32[]{:S(2)}) async-start(), calls=%async_computation.1 | async-start | bytes 13312000 | tf_op jit(solution)/shard_map/all_gather | solution.py:618
  13.9 0.7 copy-start.9
  109.5 9.5 %copy-start.8 = (bf16[768,2048]{1,0:T(8,128)(2,1)S(1)}, bf16[768,2048]{1,0:T(8,128)(2,1)}, u32[]{:S(2)}) copy-start(bf16[768,2048]{1,0:T(8,128)(2,1)} %tok_ref.1) | copy-start | bytes 9437188
  119.0 3.4 %copy-start = (bf16[2048,2048]{1,0:T(8,128)(2,1)S(1)}, bf16[2048,2048]{1,0:T(8,128)(2,1)}, u32[]{:S(2)}) copy-start(bf16[2048,2048]{1,0:T(8,128)(2,1)} %slice.43.w_ref) | copy-start | bytes 25165828
  134.2 0.7 copy-start.1
  136.2 12.8 %collective-permute-start = (bf16[16,768]{1,0:T(8,128)(2,1)}, bf16[16,768]{1,0:T(8,128)(2,1)}, u32[]{:S(2)}, u32[]{:S(2)}) collective-permute-start(bf16[16,768]{1,0:T(8,128)(2,1)} %get-tuple-element.23), channel_id=1, source_target_pairs={{0,4},{4,8},{8,12},{12,16},{16,20},{20,24},{24,28},{28,32},{32,36}... | collective-permute-start | bytes 73736 | tf_op jit(solution)/shard_map/ppermute | solution.py:593
  138.2 10.8 %collective-permute-start.1 = (bf16[16,768]{1,0:T(8,128)(2,1)}, bf16[16,768]{1,0:T(8,128)(2,1)}, u32[]{:S(2)}, u32[]{:S(2)}) collective-permute-start(bf16[16,768]{1,0:T(8,128)(2,1)} %get-tuple-element.22), channel_id=1, source_target_pairs={{4,0},{8,4},{12,8},{16,12},{20,16},{24,20},{28,24},{32,28},{36,32}... | collective-permute-start | bytes 73736 | tf_op jit(solution)/shard_map/ppermute | solution.py:593
  141.1 49.3 %collective-permute-start.2 = (bf16[128,256]{1,0:T(8,128)(2,1)}, bf16[128,256]{1,0:T(8,128)(2,1)}, u32[]{:S(2)}, u32[]{:S(2)}) collective-permute-start(bf16[128,256]{1,0:T(8,128)(2,1)} %get-tuple-element.25), channel_id=1, source_target_pairs={{0,4},{4,8},{8,12},{12,16},{16,20},{20,24},{24,28},{28,32},{32,36}... | collective-permute-start | bytes 196616 | tf_op jit(solution)/shard_map/ppermute | solution.py:593
  143.7 46.7 %collective-permute-start.3 = (bf16[128,256]{1,0:T(8,128)(2,1)}, bf16[128,256]{1,0:T(8,128)(2,1)}, u32[]{:S(2)}, u32[]{:S(2)}) collective-permute-start(bf16[128,256]{1,0:T(8,128)(2,1)} %get-tuple-element.24), channel_id=1, source_target_pairs={{4,0},{8,4},{12,8},{16,12},{20,16},{24,20},{28,24},{32,28},{36,32}... | collective-permute-start | bytes 196616 | tf_op jit(solution)/shard_map/ppermute | solution.py:593
  149.0 1.0 copy-start.2
  150.0 0.8 copy-start.3
  150.7 0.7 copy-start.6
  151.5 33.7 %copy-start.4 = (bf16[16,1024]{1,0:T(8,128)(2,1)S(1)}, bf16[16,1024]{1,0:T(8,128)(2,1)}, u32[]{:S(2)}) copy-start(bf16[16,1024]{1,0:T(8,128)(2,1)} %fusion.4.e_ref) | copy-start | bytes 98308
  185.2 5.2 %copy-start.5 = (f32[2,64,128]{2,1,0:T(8,128)S(1)}, f32[2,64,128]{2,1,0:T(8,128)}, u32[]{:S(2)}) copy-start(f32[2,64,128]{2,1,0:T(8,128)} %pad_maximum_fusion.by_col_ref) | copy-start | bytes 196612
  185.2 5.2 %copy-start.7 = (s32[2]{0:T(128)S(1)}, s32[2]{0:T(128)}, u32[]{:S(2)}) copy-start(s32[2]{0:T(128)} %pad_add_fusion.at_ref) | copy-start | bytes 28
Sparse Core Ops, SparseCore 0:
  14.7 94.7 all-gather.1

commit v2 on v1

--- a/solution.py
+++ b/solution.py
@@ -21,6 +21,7 @@
 F32 = jnp.float32
 BF16 = jnp.bfloat16
 MSG = STATE + 16
+KV_AT = 768
 
 
 def dot(a, b, dims=((1,), (0,)), precision=None):
@@ -51,59 +52,68 @@
     return (rows == cols).astype(BF16)
 
 
-def project_kernel(tok_ref, gain_ref, w_ref, ws_ref, out_ref, step_ref, normed):
-    @pl.when(pl.program_id(0) == 0)
-    def _():
-        def one(i, carry):
-            rows = pl.ds(i * BLOCK, BLOCK)
-            wide = tok_ref[rows, :].astype(F32)
-            scale = lax.rsqrt(jnp.mean(wide * wide, axis=1, keepdims=True) + EPS)
-            normed[rows, :] = (wide * scale * gain_ref[...]).astype(BF16)
-            return carry
-
-        lax.fori_loop(0, tok_ref.shape[0] // BLOCK, one, 0)
-        step_ref[...] = dot(normed[...], ws_ref[...])
-
-    out_ref[...] = dot(normed[...], w_ref[...]).astype(BF16)
-
-
-def project(tokens, gain, weights, step_weights):
+def project_kernel(tok_ref, before_ref, after_ref, gain_ref, a_ref, b_ref, out_ref, step_ref, normed):
+    count = tok_ref.shape[0]
+    place = lax.axis_index(SP)
+    tile = 256
+
+    def norm(value):
+        wide = value.astype(F32)
+        scale = lax.rsqrt(jnp.mean(wide * wide, axis=1, keepdims=True) + EPS)
+        return wide * scale * gain_ref[...]
+
+    def one(i, carry):
+        rows = pl.ds(pl.multiple_of(i * BLOCK, BLOCK), BLOCK)
+        normed[rows, :] = norm(tok_ref[rows, :]).astype(BF16)
+        return carry
+
+    lax.fori_loop(0, count // BLOCK, one, 0)
+    before = jnp.where(place > 0, norm(before_ref[...]), 0.0)
+    normed[count : count + HALO, :] = before.astype(BF16)
+    after = jnp.where(place < lax.axis_size(SP) - 1, norm(after_ref[...]), 0.0)
+    normed[count + HALO : count + 2 * HALO, :] = after.astype(BF16)
+
+    def column(j, carry):
+        cols = pl.ds(pl.multiple_of(j * tile, tile), tile)
+        out_ref[:, cols] = dot(normed[...], a_ref[:, cols]).astype(BF16)
+        return carry
+
+    tiles = WIDTH_A // tile
+    lax.fori_loop(0, tiles, column, 0)
+    step_ref[...] = dot(normed[0:count, :], a_ref[:, tiles * tile : WIDTH_A])
+    out_ref[:, tiles * tile : (tiles + 1) * tile] = dot(
+        normed[...], b_ref[:, WIDTH_B - tile : WIDTH_B]
+    ).astype(BF16)
+
+
+def project(tokens, before, after, gain, a, b):
     count, width = tokens.shape
-    columns = weights.shape[1]
-    tile = 256
+    columns = 2048
+    vmem = pl.BlockSpec(memory_space=pltpu.VMEM)
     return pl.pallas_call(
         project_kernel,
-        grid=(columns // tile,),
-        in_specs=[
-            pl.BlockSpec((count, width), lambda j: (0, 0), pipeline_mode=pl.Buffered(1)),
-            pl.BlockSpec((1, width), lambda j: (0, 0)),
-            pl.BlockSpec((width, tile), lambda j: (0, j)),
-            pl.BlockSpec((width, 128), lambda j: (0, 0), pipeline_mode=pl.Buffered(1)),
-        ],
-        out_specs=[
-            pl.BlockSpec((count, tile), lambda j: (0, j)),
-            pl.BlockSpec((count, 128), lambda j: (0, 0)),
-        ],
+        in_specs=[vmem] * 6,
+        out_specs=[vmem] * 2,
         out_shape=[
-            jax.ShapeDtypeStruct((count, columns), BF16),
+            jax.ShapeDtypeStruct((count + 2 * HALO, columns), BF16),
             jax.ShapeDtypeStruct((count, 128), F32),
         ],
-        scratch_shapes=[pltpu.VMEM((count, width), BF16)],
-        compiler_params=pltpu.CompilerParams(vmem_limit_bytes=16 << 20),
+        scratch_shapes=[pltpu.VMEM((count + 2 * HALO, width), BF16)],
+        compiler_params=pltpu.CompilerParams(vmem_limit_bytes=12 << 20),
         cost_estimate=pl.CostEstimate(
             flops=2 * count * width * (columns + 128),
             bytes_accessed=2 * (count * width + width * columns + count * columns),
             transcendentals=0,
         ),
         name="project",
-    )(tokens, gain, weights, step_weights)
+    )(tokens, before, after, gain, a, b)
 
 
 def conv_state_kernel(
-    cin_ref, before_ref, after_ref, taps_ref, step_ref, rate_ref, e_ref,
+    cin_ref, taps_ref, step_ref, rate_ref, e_ref,
     conv_ref, col_ref, row_ref, piece_ref, etot_ref, msg_ref, win, near,
 ):
-    count = cin_ref.shape[0]
+    count = cin_ref.shape[0] - 2 * HALO
     blocks = count // BLOCK
     channels = HEADS * HEAD_DIM
     spread_m = e_ref[...]
@@ -113,8 +123,8 @@
         lax.broadcasted_iota(jnp.int32, (BLOCK, BLOCK), 0)
         >= lax.broadcasted_iota(jnp.int32, (BLOCK, BLOCK), 1)
     ).astype(F32)
-    win[pl.ds(0, HALO), :] = before_ref[...].astype(F32)
-    win[pl.ds(HALO + count, HALO), :] = after_ref[...].astype(F32)
+    win[pl.ds(0, HALO), :] = cin_ref[pl.ds(count, HALO), :].astype(F32)
+    win[pl.ds(HALO + count, HALO), :] = cin_ref[pl.ds(count + HALO, HALO), :].astype(F32)
 
     def fill(i, carry):
         start = pl.multiple_of(i * BLOCK, BLOCK)
@@ -175,9 +185,9 @@
             msg_ref[e, pair, STATE:MSG, :] = tail[:, e * channels + pair * 128 : e * channels + pair * 128 + 128]
 
 
-def conv_state(proj, before, after, taps, step_raw, rate, spread_m):
-    count = proj.shape[0]
-    width = before.shape[1]
+def conv_state(proj, taps, step_raw, rate, spread_m):
+    count = step_raw.shape[0]
+    width = taps.shape[1]
     blocks = count // BLOCK
     channels = HEADS * HEAD_DIM
     whole = lambda shape: pl.BlockSpec(shape, lambda i: (0,) * len(shape))
@@ -185,9 +195,7 @@
         conv_state_kernel,
         grid=(1,),
         in_specs=[
-            pl.BlockSpec((count, width), lambda i: (0, 0)),
-            whole((HALO, width)),
-            whole((HALO, width)),
+            pl.BlockSpec((proj.shape[0], width), lambda i: (0, 0)),
             whole(taps.shape),
             whole(step_raw.shape),
             whole(rate.shape),
@@ -218,7 +226,7 @@
             flops=2 * count * STATE * 2 * channels, bytes_accessed=12 << 20, transcendentals=0
         ),
         name="conv_state",
-    )(proj, before, after, taps, step_raw, rate, spread_m)
+    )(proj, taps, step_raw, rate, spread_m)
 
 
 def mix_kernel(
@@ -322,11 +330,12 @@
 
 
 def attend_kernel(
-    at_ref, q_ref, kv_ref, before_ref, after_ref, by_row_ref, by_col_ref, sink_ref,
+    q_ref, kv_ref, before_ref, after_ref, by_row_ref, by_col_ref, sink_ref,
     out_ref, log_ref, keys, values,
 ):
-    count = kv_ref.shape[0]
+    count = q_ref.shape[0]
     blocks = count // BLOCK
+    place = lax.axis_index(SP)
     lane = lax.broadcasted_iota(jnp.int32, (BLOCK, 128), 1)
     low_quarter = lane % 32 < 16
     first_half = lane < HEAD_DIM
@@ -366,8 +375,8 @@
     key_at = lax.broadcasted_iota(jnp.int32, (3 * BLOCK, 2 * BLOCK), 0)
     query_at = lax.broadcasted_iota(jnp.int32, (3 * BLOCK, 2 * BLOCK), 1) % BLOCK
     in_band = (key_at >= query_at) & (key_at <= query_at + 2 * WINDOW)
-    start_at = at_ref[0]
-    end_at = at_ref[1]
+    start_at = -place * count
+    end_at = start_at + count * lax.axis_size(SP)
 
     def one(i, carry):
         start = pl.multiple_of(i * BLOCK, BLOCK)
@@ -402,18 +411,15 @@
     lax.fori_loop(0, blocks, one, 0)
 
 
-def attend(limits, proj, q_block, kv_block, before, after, tables, sinks):
-    count = proj.shape[0]
+def attend(count, proj, q_block, kv_block, before, after, tables, sinks):
     channels = HEADS * HEAD_DIM
     whole = lambda shape: pl.BlockSpec(shape, lambda i, *_: (0,) * len(shape))
-    smem = pl.BlockSpec(memory_space=pltpu.SMEM)
     by_row, by_col = tables
     wide_sinks = jnp.repeat(sinks.reshape(HEADS // 2, 2), BLOCK, axis=1)
     return pl.pallas_call(
         attend_kernel,
         grid=(1,),
         in_specs=[
-            smem,
             pl.BlockSpec((count, channels), lambda i: (0, q_block)),
             pl.BlockSpec((count, 256), lambda i: (0, kv_block)),
             whole(before.shape), whole(after.shape), whole(by_row.shape), whole(by_col.shape),
@@ -433,12 +439,267 @@
             flops=4 * count * 3 * BLOCK * channels, bytes_accessed=4 << 20, transcendentals=0
         ),
         name="attend",
-    )(limits, proj, proj, before, after, by_row, by_col, wide_sinks)
+    )(proj, proj, before, after, by_row, by_col, wide_sinks)
+
+
+LINKS = ("z+", "z-", "y+", "y-")
+WIDTH_A = 1920
+WIDTH_B = 1280
+
+
+def ring(kind, link_axis, other_at, length, total, cut):
+    out = []
+    for sign in (1, -1):
+        previous = None
+        for step in range(length // 2):
+            last = step == length // 2 - 1
+            cols = (0, total)
+            if last:
+                cols = (0, cut) if sign == 1 else (cut, total)
+            name = (kind, link_axis, other_at, sign, step)
+            out.append(dict(
+                name=name, kind=kind, axis=link_axis, sign=sign,
+                along=-sign * step, other=other_at, cols=cols, after=previous,
+            ))
+            previous = name
+    return out
+
+
+def transfers(length_z, length_y):
+    sends = []
+    for kind, first, length, second, length2, total, cut in (
+        ("A", "z", length_z, "y", length_y, WIDTH_A, 1024),
+        ("B", "y", length_y, "z", length_z, WIDTH_B, 640),
+    ):
+        sends += ring(kind, first, 0, length, total, cut)
+        for offset in range(-(length // 2) + 1, length // 2 + 1):
+            sends += ring(kind, second, offset, length2, total, cut)
+    for s in sends:
+        length, first = (length_z, "z") if s["kind"] == "A" else (length_y, "y")
+        s["needs"] = []
+        if s["after"] is not None:
+            s["needs"] = [s["after"]]
+        elif s["axis"] != first and s["other"] != 0:
+            d = s["other"]
+            if abs(d) == length // 2:
+                s["needs"] = [(s["kind"], first, 0, sign, length // 2 - 1) for sign in (1, -1)]
+            else:
+                s["needs"] = [(s["kind"], first, 0, -1 if d > 0 else 1, abs(d) - 1)]
+    return sends
+
+
+def arrival_order(sends):
+    import heapq
+
+    rate, hop = 46.6e3, 1.9
+    free = dict.fromkeys(LINKS, 0.0)
+    left = {s["name"]: len(s["needs"]) for s in sends}
+    followers = {}
+    for s in sends:
+        for need in s["needs"]:
+            followers.setdefault(need, []).append(s)
+    heap, order, first = [], [], []
+
+    def start(s, now):
+        link = s["axis"] + ("+" if s["sign"] == 1 else "-")
+        size = 32 * 2 * (s["cols"][1] - s["cols"][0])
+        free[link] = max(free[link], now) + size / rate
+        heapq.heappush(heap, (free[link] + hop, len(order), str(s["name"]), s["name"]))
+
+    def rank(s):
+        return (s["axis"] != ("z" if s["kind"] == "A" else "y"), s["kind"] != "A")
+
+    for s in sorted((s for s in sends if not s["needs"]), key=rank):
+        first.append(s)
+        start(s, 0.0)
+    end = 0.0
+    while heap:
+        now, _, _, name = heapq.heappop(heap)
+        ready = []
+        for s in sorted(followers.get(name, []), key=rank):
+            left[s["name"]] -= 1
+            if left[s["name"]] == 0:
+                ready.append(s)
+                start(s, now)
+        order.append((name, ready))
+        end = now
+    return first, order, end
+
+
+def gather_kernel(
+    lengths, edges_ref, value_ref, inflow_ref, readout_ref, key_ref, vector_ref, gate_ref,
+    query_ref, step_ref, turned_ref,
+    a_ref, b_ref, before_ref, after_ref, send_sem, recv_sem, core_send, core_recv, edge_sem,
+):
+    length_z, length_y = lengths
+    z, y, c = (lax.axis_index(a) for a in SP)
+    other = 1 - c
+    mesh_id = pl.DeviceIdType.MESH
+
+    def wrap(value, length):
+        return lax.rem(value + length, length)
+
+    steps = {"z": (SP[0], z, length_z), "y": (SP[1], y, length_y)}
+
+    def towards(axis, sign):
+        name, at, length = steps[axis]
+        return {name: wrap(at + sign, length)}
+
+    flat = (z * length_y + y) * 2 + c
+    count = length_z * length_y * 2
+
+    def device_at(index):
+        index = wrap(index, count)
+        return {
+            SP[0]: index // (2 * length_y),
+            SP[1]: lax.rem(index // 2, length_y),
+            SP[2]: lax.rem(index, 2),
+        }
+
+    peers = [{SP[2]: other}] + [towards(a, s) for a in ("z", "y") for s in (1, -1)]
+    peers += [device_at(flat + 1), device_at(flat - 1)]
+    barrier = pltpu.get_barrier_semaphore()
+    for peer in peers:
+        pl.semaphore_signal(barrier, inc=1, device_id=peer, device_id_type=mesh_id)
+
+    own_a, own_b = a_ref.at[z, y, c], b_ref.at[z, y, c]
+    column = 0
+    for ref in (value_ref, inflow_ref, readout_ref, key_ref, vector_ref, gate_ref):
+        own_a[:, column : column + ref.shape[1]] = ref[...]
+        column += ref.shape[1]
+    half = query_ref.shape[1] // 2
+    own_a[:, column : column + half] = query_ref[:, 0:half]
+    own_a[:, column + half : WIDTH_A] = step_ref[...]
+    own_b[:, 0 : turned_ref.shape[1]] = turned_ref[...]
+    own_b[:, turned_ref.shape[1] : WIDTH_B] = query_ref[:, half : 2 * half]
+    pl.semaphore_wait(barrier, len(peers))
+
+    sends = transfers(length_z, length_y)
+    number = {s["name"]: i for i, s in enumerate(sends)}
+    by_name = {s["name"]: s for s in sends}
+
+    def block(s, shift):
+        along = s["along"] - shift * s["sign"]
+        dz, dy = (along, s["other"]) if s["axis"] == "z" else (s["other"], along)
+        ref = a_ref if s["kind"] == "A" else b_ref
+        cols = pl.ds(s["cols"][0], s["cols"][1] - s["cols"][0])
+        return ref.at[wrap(z + dz, length_z), wrap(y + dy, length_y), c, :, cols]
+
+    def copy_of(s, shift):
+        i = number[s["name"]]
+        ref = block(s, shift)
+        return pltpu.make_async_remote_copy(
+            src_ref=ref, dst_ref=ref, send_sem=send_sem.at[i], recv_sem=recv_sem.at[i],
+            device_id=towards(s["axis"], s["sign"]), device_id_type=mesh_id,
+        )
+
+    edge_rows = edges_ref.shape[0] // 2
+    edge_copies = []
+    for k, (index, dst) in enumerate(((flat - 1, after_ref), (flat + 1, before_ref))):
+        edge_copies.append(pltpu.make_async_remote_copy(
+            src_ref=edges_ref.at[pl.ds(k * edge_rows, edge_rows)], dst_ref=dst,
+            send_sem=edge_sem.at[k, 0], recv_sem=edge_sem.at[k, 1],
+            device_id=device_at(index), device_id_type=mesh_id,
+        ))
+
+    first, order, _ = arrival_order(sends)
+    started = []
+    for s in first:
+        copy = copy_of(s, 0)
+        copy.start()
+        started.append(copy)
+    for copy in edge_copies:
+        copy.start()
+
+    waiting = {}
+    for kind, first_axis, length, second in (("A", "z", length_z, "y"), ("B", "y", length_y, "z")):
+        for offset in range(-(length // 2) + 1, length // 2 + 1):
+            names = [s["name"] for s in sends
+                     if s["kind"] == kind and s["axis"] == second and s["other"] == offset]
+            waiting[(kind, offset)] = set(names)
+    keys = list(waiting)
+
+    def core_copy(key):
+        kind, offset = key
+        i = keys.index(key)
+        if kind == "A":
+            src = a_ref.at[wrap(z + offset, length_z), :, c]
+        else:
+            src = b_ref.at[:, wrap(y + offset, length_y), c]
+        return src, i
+
+    def send_core(key):
+        src, i = core_copy(key)
+        copy = pltpu.make_async_remote_copy(
+            src_ref=src, dst_ref=src, send_sem=core_send.at[i], recv_sem=core_recv.at[i],
+            device_id={SP[2]: other}, device_id_type=mesh_id,
+        )
+        copy.start()
+        started.append(copy)
+
+    def wait_core(key):
+        kind, offset = key
+        i = keys.index(key)
+        if kind == "A":
+            dst = a_ref.at[wrap(z + offset, length_z), :, other]
+        else:
+            dst = b_ref.at[:, wrap(y + offset, length_y), other]
+        pltpu.make_async_remote_copy(
+            src_ref=dst, dst_ref=dst, send_sem=core_send.at[i], recv_sem=core_recv.at[i],
+            device_id={SP[2]: other}, device_id_type=mesh_id,
+        ).wait_recv()
+
+    for name, ready in order:
+        copy_of(by_name[name], 1).wait_recv()
+        for s in ready:
+            copy = copy_of(s, 0)
+            copy.start()
+            started.append(copy)
+        for key in keys:
+            if name in waiting[key]:
+                waiting[key].remove(name)
+                if not waiting[key]:
+                    send_core(key)
+    for copy in started:
+        copy.wait_send()
+    for key in keys:
+        wait_core(key)
+    for copy in edge_copies:
+        copy.wait()
+
+
+def gather(length_z, length_y, edges, *shards):
+    sends = transfers(length_z, length_y)
+    groups = length_z + length_y
+    vmem = pl.BlockSpec(memory_space=pltpu.VMEM)
+    dma = pltpu.SemaphoreType.DMA
+    lead = (length_z, length_y, 2, 32)
+    edge = (edges.shape[0] // 2, edges.shape[1])
+    a, b, before, after = pl.pallas_call(
+        functools.partial(gather_kernel, (length_z, length_y)),
+        in_specs=[vmem] * (1 + len(shards)),
+        out_specs=[vmem] * 4,
+        out_shape=[
+            jax.ShapeDtypeStruct((*lead, WIDTH_A), BF16),
+            jax.ShapeDtypeStruct((*lead, WIDTH_B), BF16),
+            jax.ShapeDtypeStruct(edge, BF16),
+            jax.ShapeDtypeStruct(edge, BF16),
+        ],
+        scratch_shapes=[
+            dma((len(sends),)), dma((len(sends),)), dma((groups,)), dma((groups,)), dma((2, 2)),
+        ],
+        compiler_params=pltpu.CompilerParams(
+            collective_id=2, has_side_effects=True, vmem_limit_bytes=20 << 20
+        ),
+        cost_estimate=pl.CostEstimate(flops=1 << 24, bytes_accessed=24 << 20, transcendentals=0),
+        name="gather",
+    )(edges, *shards)
+    return a.reshape(-1, WIDTH_A), b.reshape(-1, WIDTH_B), before, after
 
 
 def exchange_kernel(
-    msg_ref, out_ref, part, turned, by_y, summed, by_z, back, arrived, nxt, final, carry,
-    part_sem, y_sem, z_sem, back_sem, final_sem,
+    rows, msg_ref, proj_ref, out_ref, kv_before_ref, kv_after_ref, part, turned, by_y, summed, by_z, back, arrived, nxt, final, carry,
+    part_sem, y_sem, z_sem, back_sem, final_sem, kv_sem,
 ):
     z, y, c = (lax.axis_index(a) for a in SP)
     length_z, length_y = lax.axis_size(SP[0]), lax.axis_size(SP[1])
@@ -449,6 +710,18 @@
     peers = [{SP[2]: other}]
     peers += [{SP[1]: lax.rem(y + k, length_y)} for k in range(1, length_y)]
     peers += [{SP[0]: lax.rem(z + k, length_z)} for k in range(1, length_z)]
+    flat = (z * length_y + y) * 2 + c
+    count = length_z * length_y * 2
+
+    def device_at(index):
+        index = lax.rem(index + count, count)
+        return {
+            SP[0]: index // (2 * length_y),
+            SP[1]: lax.rem(index // 2, length_y),
+            SP[2]: lax.rem(index, 2),
+        }
+
+    peers += [device_at(flat + 1), device_at(flat - 1)]
     barrier = pltpu.get_barrier_semaphore()
     for peer in peers:
         pl.semaphore_signal(barrier, inc=1, device_id=peer, device_id_type=mesh_id)
@@ -478,6 +751,14 @@
 
     pairs = msg_ref.shape[1]
     copy = send(msg_ref.at[other], part, part_sem, {SP[2]: other})
+    kv_cols = pl.ds(KV_AT, kv_before_ref.shape[1])
+    kv_copies = [
+        send(
+            proj_ref.at[pl.ds(rows - WINDOW, WINDOW), kv_cols], kv_before_ref, kv_sem.at[0],
+            device_at(flat + 1),
+        ),
+        send(proj_ref.at[pl.ds(0, WINDOW), kv_cols], kv_after_ref, kv_sem.at[1], device_at(flat - 1)),
+    ]
     copy.wait()
     for j in range(pairs):
         decay = decay_of(part, j)
@@ -553,18 +834,24 @@
         ).astype(BF16)
     send(nxt, final, final_sem, {SP[2]: other}).wait()
     out_ref[other] = final[...]
-
-
-def exchange(message, length_z, length_y):
+    for copy in kv_copies:
+        copy.wait()
+
+
+def exchange(message, proj, rows, length_z, length_y):
     pairs = message.shape[1]
     tile = (STATE, 128)
     full = (MSG, 128)
     dma = pltpu.SemaphoreType.DMA
     return pl.pallas_call(
-        exchange_kernel,
-        in_specs=[pl.BlockSpec(memory_space=pltpu.VMEM)],
-        out_specs=pl.BlockSpec(memory_space=pltpu.VMEM),
-        out_shape=jax.ShapeDtypeStruct((2, pairs, *tile), BF16),
+        functools.partial(exchange_kernel, rows),
+        in_specs=[pl.BlockSpec(memory_space=pltpu.VMEM)] * 2,
+        out_specs=[pl.BlockSpec(memory_space=pltpu.VMEM)] * 3,
+        out_shape=[
+            jax.ShapeDtypeStruct((2, pairs, *tile), BF16),
+            jax.ShapeDtypeStruct((WINDOW, 256), BF16),
+            jax.ShapeDtypeStruct((WINDOW, 256), BF16),
+        ],
         scratch_shapes=[
             pltpu.VMEM((pairs, *full), BF16),
             pltpu.VMEM((pairs, *full), BF16),
@@ -577,20 +864,119 @@
             pltpu.VMEM((pairs, *tile), BF16),
             pltpu.VMEM(tile, F32),
             dma((2,)), dma((length_y, 2)), dma((length_z, 2)), dma((length_y, 2)), dma((2,)),
+            dma((2, 2)),
         ],
         compiler_params=pltpu.CompilerParams(
             collective_id=1, has_side_effects=True, vmem_limit_bytes=8 << 20
         ),
         cost_estimate=pl.CostEstimate(flops=1 << 24, bytes_accessed=1 << 20, transcendentals=0),
         name="exchange",
-    )(message)
-
-
-def neighbours(tail, head):
-    count = lax.axis_size(SP)
-    up = [(i, i + 1) for i in range(count - 1)]
-    down = [(i + 1, i) for i in range(count - 1)]
-    return lax.ppermute(tail, SP, up), lax.ppermute(head, SP, down)
+    )(message, proj)
+
+
+def finish_kernel(state_ref, window_ref, w_ref, out_ref, *refs):
+    far_out, far_in, near_out, near_in, far_sem, near_sem = refs
+    n = lax.axis_size("tp")
+    me = lax.axis_index("tp")
+    mesh_id = pl.DeviceIdType.MESH
+    sides = (1, -1)
+    count, channels = state_ref.shape
+    width = w_ref.shape[0] // n
+    half = width // 2
+    chunk = far_out.shape[2]
+    chunks = count // chunk
+
+    def at(step):
+        return lax.rem(me + step + n, n)
+
+    barrier = pltpu.get_barrier_semaphore()
+    for side in sides:
+        pl.semaphore_signal(barrier, inc=1, device_id={"tp": at(side)}, device_id_type=mesh_id)
+    pl.semaphore_wait(barrier, 2)
+
+    def terms(rows, to):
+        outs = pl.ds(pl.multiple_of(to * width, width), width)
+        return dot(state_ref[rows, :], w_ref[outs, 0:channels], ((1,), (1,))) + dot(
+            window_ref[rows, :], w_ref[outs, channels : 2 * channels], ((1,), (1,))
+        )
+
+    def far_copy(i, k):
+        return pltpu.make_async_remote_copy(
+            src_ref=far_out.at[k, i], dst_ref=far_in.at[k, i], send_sem=far_sem.at[k, i, 0],
+            recv_sem=far_sem.at[k, i, 1], device_id={"tp": at(sides[k])}, device_id_type=mesh_id,
+        )
+
+    def near_copy(i, k):
+        return pltpu.make_async_remote_copy(
+            src_ref=near_out.at[k, i], dst_ref=near_in.at[k, i], send_sem=near_sem.at[k, i, 0],
+            recv_sem=near_sem.at[k, i, 1], device_id={"tp": at(sides[k])}, device_id_type=mesh_id,
+        )
+
+    def send_far(i, carry):
+        rows = pl.ds(pl.multiple_of(i * chunk, chunk), chunk)
+        value = terms(rows, at(2)).astype(BF16)
+        for k in range(2):
+            far_out[k, i] = value[:, k * half : (k + 1) * half]
+            far_copy(i, k).start()
+        return carry
+
+    lax.fori_loop(0, chunks, send_far, 0)
+
+    def send_near(i, carry):
+        rows = pl.ds(pl.multiple_of(i * chunk, chunk), chunk)
+        for k in range(2):
+            value = terms(rows, at(sides[k])).astype(BF16).astype(F32)
+            lanes = slice(k * half, (k + 1) * half)
+            far_copy(i, k).wait_recv()
+            near_out[k, i] = value.astype(BF16)
+            near_out[k, i, :, lanes] = (value[:, lanes] + far_in[k, i].astype(F32)).astype(BF16)
+            near_copy(i, k).start()
+        return carry
+
+    lax.fori_loop(0, chunks, send_near, 0)
+
+    def collect(i, carry):
+        rows = pl.ds(pl.multiple_of(i * chunk, chunk), chunk)
+        value = terms(rows, me).astype(BF16).astype(F32)
+        for k in range(2):
+            near_copy(i, k).wait_recv()
+            value = value + near_in[k, i].astype(F32)
+        out_ref[rows, :] = value.astype(BF16)
+        for k in range(2):
+            far_copy(i, k).wait_send()
+            near_copy(i, k).wait_send()
+        return carry
+
+    lax.fori_loop(0, chunks, collect, 0)
+
+
+def finish(state, window, weights, n):
+    count, channels = state.shape
+    width = weights.shape[0] // n
+    chunk = 128
+    chunks = count // chunk
+    vmem = pl.BlockSpec(memory_space=pltpu.VMEM)
+    dma = pltpu.SemaphoreType.DMA
+    return pl.pallas_call(
+        finish_kernel,
+        in_specs=[vmem] * 3,
+        out_specs=vmem,
+        out_shape=jax.ShapeDtypeStruct((count, width), BF16),
+        scratch_shapes=[
+            pltpu.VMEM((2, chunks, chunk, width // 2), BF16),
+            pltpu.VMEM((2, chunks, chunk, width // 2), BF16),
+            pltpu.VMEM((2, chunks, chunk, width), BF16),
+            pltpu.VMEM((2, chunks, chunk, width), BF16),
+            dma((2, chunks, 2)), dma((2, chunks, 2)),
+        ],
+        compiler_params=pltpu.CompilerParams(
+            collective_id=3, has_side_effects=True, vmem_limit_bytes=24 << 20
+        ),
+        cost_estimate=pl.CostEstimate(
+            flops=4 * count * channels * width * n, bytes_accessed=8 << 20, transcendentals=0
+        ),
+        name="finish",
+    )(state, window, weights)
 
 
 def flatten_rows(weight):
@@ -604,48 +990,29 @@
 ):
     count = tokens.shape[0]
     place = lax.axis_index(SP)
-    total = count * lax.axis_size(SP)
     length_z, length_y = lax.axis_size(SP[0]), lax.axis_size(SP[1])
-    out_stack = jnp.concatenate([state_out, window_out], axis=0).T
-    shard = jnp.concatenate(
-        [
-            value_weight, flatten_rows(inflow_weight), flatten_rows(readout_weight),
-            key_weight, vector_weight, gate_weight, query_weight,
-            jnp.pad(flatten_rows(step_weight), ((0, 0), (0, 128 - 2 * HEADS))), out_stack,
-        ],
-        axis=1,
-    )
-    gathered = lax.all_gather(shard, SP, axis=0, tiled=True)
-    weights = gathered[:, 0:2048]
-    step_weights = gathered[:, 2048:2176]
-    out_weights = gathered[:, 2176:3200]
-    proj, step_raw = project(tokens, input_gain.astype(F32)[None], weights, step_weights)
-    conv_before, conv_after = neighbours(proj[-HALO:, 0:768], proj[:HALO, 0:768])
-    kv_before, kv_after = neighbours(proj[-WINDOW:, 768:1024], proj[:WINDOW, 768:1024])
     spread_m = spread_matrix()
     rate = jnp.concatenate([log_rate[0], log_rate[1]], axis=1)
     taps = jnp.concatenate(
         [conv_values, flatten_rows(conv_inflow), flatten_rows(conv_readout)], axis=1
     )
     taps = jnp.pad(taps.astype(F32), ((0, 3), (0, 0)))
-    conv, col, row, piece, etot, message = conv_state(
-        proj, conv_before, conv_after, taps, step_raw, rate, spread_m
+    tables = rope_tables((place * count - WINDOW) // GRID_W, (count + 2 * WINDOW) // GRID_W)
+    edges = jnp.concatenate([tokens[:HALO], tokens[-HALO:]], axis=0)
+    a, b, before, after = gather(
+        length_z, length_y, edges, value_weight, flatten_rows(inflow_weight),
+        flatten_rows(readout_weight), key_weight, vector_weight, gate_weight, query_weight,
+        jnp.pad(flatten_rows(step_weight), ((0, 0), (0, 128 - 2 * HEADS))),
+        jnp.concatenate([state_out, window_out], axis=0).T,
     )
-    incoming = exchange(message, length_z, length_y)
-    limits = jnp.stack([-place * count, total - place * count]).astype(jnp.int32)
-    tables = rope_tables((place * count - WINDOW) // GRID_W, (count + 2 * WINDOW) // GRID_W)
-    window, logs = attend(limits, proj, 3, 3, kv_before, kv_after, tables, sink_logit)
+    proj, step_raw = project(tokens, before, after, input_gain.astype(F32)[None], a, b)
+    conv, col, row, piece, etot, message = conv_state(proj, taps, step_raw, rate, spread_m)
+    incoming, kv_before, kv_after = exchange(message, proj, count, length_z, length_y)
+    window, logs = attend(count, proj, 3, 3, kv_before, kv_after, tables, sink_logit)
     state = mix(
         conv, col, row, piece, etot, incoming, proj, 2, group_gain.astype(F32)[None], spread_m
     )
-    half = HEADS * HEAD_DIM
-    terms = dot(state, out_weights[:, :half], ((1,), (1,))) + dot(
-        window, out_weights[:, half:], ((1,), (1,))
-    )
-    n = lax.axis_size("tp")
-    parts = jnp.moveaxis(terms.astype(BF16).reshape(count, n, -1), 1, 0)
-    arrived = lax.all_to_all(parts, "tp", split_axis=0, concat_axis=0, tiled=True)
-    mixed = arrived.astype(F32).sum(axis=0).astype(BF16)
+    mixed = finish(state, window, b, lax.axis_size("tp"))
     return mixed, logs.T
 
 

time: 262 us -> 159 us (0.61)
  waiting for transfers between devices: 88.5 us -> 0 us
  Pallas kernels: 63.9 us -> 138 us
  blocking collectives: 41 us -> 0 us
  between operations: 14.3 us -> 0.84 us
  local copies, waits for them, and re-layouts: 28 us -> 17.8 us
  starting transfers between devices: 9.86 us -> 0 us
  matrix products: 6.84 us -> 0 us
  other arithmetic: 7.87 us -> 1.89 us
    all_gather x1 -> x0, waiting for transfers between devices: 88.5 us -> none  [shards(): gathered = lax.all_gather(shard, SP, axis=0, tiled=True)]
    pallas_call x4 -> x6, Pallas kernels: 58.7 us -> 132 us  [the longest x1 54.8 us: gather(): pl.pallas_call(functools.partial(gather_kernel, (length_z, length_y)), in...]
    all_to_all x1 -> x0, blocking collectives: 41 us -> none  [shards(): lax.all_to_all(parts, 'tp', split_axis=0, concat_axis=0, tiled=True)]
    slice x4 -> x1, local copies, waits for them, and re-layouts: 10.8 us -> 0.88 us  [shards(): edges = jnp.concatenate([tokens[:HALO], tokens[-HALO:]], axis=0)]
    ppermute x4 -> x0, starting transfers between devices: 9.83 us -> none  [neighbours(): return (lax.ppermute(tail, SP, up), lax.ppermute(head, SP, down))]
    dot_general x2 -> x0, matrix products: 6.84 us -> none  [dot(): lax.dot_general(a, b, (dims, ((), ())), preferred_element_type=F32, preci...]
    unnamed x30 -> x45, local copies, waits for them, and re-layouts: 13.7 us -> 15.2 us
  transfers between devices with their start and end apart: 5 -> 0, of which waited for: 1 -> 0; matrix products, arithmetic and copies ran while one was open for 4% -> 0% of each run, Pallas kernels for 15% -> 0%
where the time goes in v2:
time: 159 us; the launch traced here: 158 us
  Pallas kernels  138 us (87%)
  local copies, waits for them, and re-layouts  17.8 us (11%)
  other arithmetic  1.89 us (1%)
    pallas_call x1, Pallas kernels, gather(): pl.pallas_call(functools.partial(gather_kernel, (length_z, length_y)), in...  54.8 us
    pallas_call x1, Pallas kernels, finish(): pl.pallas_call(finish_kernel, in_specs=[vmem] * 3, out_specs=vmem, out_sh...  29.9 us
    pallas_call x1, Pallas kernels, exchange(): pl.pallas_call(functools.partial(exchange_kernel, rows), in_specs=[pl.Blo...  18.6 us
    unnamed x45, local copies, waits for them, and re-layouts  15.2 us
    pallas_call x1, Pallas kernels, attend(): pl.pallas_call(attend_kernel, grid=(1,), in_specs=[pl.BlockSpec((count, c...  12.3 us
    pallas_call x1, Pallas kernels, project(): pl.pallas_call(project_kernel, in_specs=[vmem] * 6, out_specs=[vmem] * 2,...  10.5 us
    pallas_call x1, Pallas kernels, conv_state(): pl.pallas_call(conv_state_kernel, grid=(1,), in_specs=[pl.BlockSpec((proj...  6.26 us
    pallas_call x1, Pallas kernels, mix(): pl.pallas_call(mix_kernel, grid=(1,), in_specs=[whole(conv.shape), whole(...  5.21 us

profile of v2, /device:TPU:1, one launch (start us, length us, event | category | flops | bytes accessed | tf_op | source)
XLA Modules:
  0.0 158.1 jit_solution(2432281111004386964)
XLA Ops:
  0.6 0.9 fusion.16
  1.5 0.8 copy.26
  2.3 0.8 maximum_bitcast_fusion.turned_ref
  3.1 0.8 copy-done.5
  3.9 0.8 copy-done.6
  4.6 0.8 copy-done.7
  5.4 0.7 copy-done.8
  6.1 0.7 copy-done.9
  8.2 54.8 %gather.1 = (bf16[8,4,2,32,1920]{4,3,2,1,0:T(8,128)(2,1)S(1)}, bf16[8,4,2,32,1280]{4,3,2,1,0:T(8,128)(2,1)S(1)}, bf16[16,2048]{1,0:T(8,128)(2,1)S(1)}, bf16[16,2048]{1,0:T(8,128)(2,1)S(1)}) custom-call(bf16[32,2048]{1,0:T(8,128)(2,1)S(1)} %pad_maximum_fusion.edges_ref, bf16[32,512]{1,0:T(8,128)(2,1)S(1)} %copy-done.5, bf16[32,128]{1,0:T(8,128)(2,1)S(1)} %bitcast.24, ...), custom_call_target="tpu_custom_call" | custom-call | flops 16777216 | bytes 25165824 | tf_op jit(solution)/shard_map/gather/pallas_call | solution.py:678
  63.0 0.7 broadcast_in_dim.36
  63.7 3.0 %copy-done.12 = bf16[768,2048]{1,0:T(8,128)(2,1)S(1)} copy-done((bf16[768,2048]{1,0:T(8,128)(2,1)S(1)}, bf16[768,2048]{1,0:T(8,128)(2,1)}, u32[]{:S(2)}) %copy-start.12) | copy-done | bytes 3145752
  66.7 10.5 %project.1 = (bf16[800,2048]{1,0:T(8,128)(2,1)S(1)}, f32[768,128]{1,0:T(8,128)S(1)}) custom-call(bf16[768,2048]{1,0:T(8,128)(2,1)S(1)} %copy-done.12, bf16[16,2048]{1,0:T(8,128)(2,1)S(1)} %get-tuple-element.19.before_ref, bf16[16,2048]{1,0:T(8,128)(2,1)S(1)} %get-tuple-element.20.after_ref, f32[1,2048]{1,0:T(1,128)S(1)} %bitcast.23, ...), custom_call_target="tpu_custom_call" | custom-call | flops 6845104128 | bytes 14680064 | tf_op jit(solution)/shard_map/project/pallas_call | solution.py:93
  77.2 0.7 copy-done.3
  78.0 0.9 copy.27.rate_ref
  79.0 1.0 copy-done
  80.0 1.0 copy-done.4
  81.0 6.3 %conv_state.1 = (bf16[768,768]{1,0:T(8,128)(2,1)S(1)}, f32[768,32]{1,0:T(8,128)S(1)}, f32[6,32,128]{2,1,0:T(8,128)S(1)}, f32[6,128,1024]{2,1,0:T(8,128)S(1)}, f3...) custom-call(bf16[800,2048]{1,0:T(8,128)(2,1)S(1)} %get-tuple-element.23.cin_ref.proj_ref.gate_ref.q_ref.kv_ref, ...), custom_call_target="tpu_custom_call" | custom-call | flops 201326592 | bytes 12582912 | tf_op jit(solution)/shard_map/conv_state/pallas_call | solution.py:194
  87.2 18.6 %exchange.1 = (bf16[2,4,128,128]{3,2,1,0:T(8,128)(2,1)S(1)}, bf16[128,256]{1,0:T(8,128)(2,1)S(1)}, bf16[128,256]{1,0:T(8,128)(2,1)S(1)}) custom-call(bf16[2,4,144,128]{3,2,1,0:T(8,128)(2,1)S(1)} %get-tuple-element.30.msg_ref, bf16[800,2048]{1,0:T(8,128)(2,1)S(1)} %get-tuple-element.23.cin_ref.proj_ref.gate_ref.q_ref.kv_ref), custom_call_target="tpu_custom_call" | custom-call | flops 16777216 | bytes 1048576 | tf_op jit(solution)/shard_map/exchange/pallas_call | solution.py:846
  105.8 5.2 %mix.1.state_ref = bf16[768,512]{1,0:T(8,128)(2,1)S(1)} custom-call(bf16[768,768]{1,0:T(8,128)(2,1)S(1)} %get-tuple-element.25.conv_ref, f32[768,32]{1,0:T(8,128)S(1)} %get-tuple-element.26.col_ref, f32[6,32,128]{2,1,0:T(8,128)S(1)} %get-tuple-element.27.row_ref, f32[6,128,1024]{2,1,0:T(8,128)S(1)} %get-tuple-element.28.piece_ref, ...), custom_call_target="tpu_custom_call" | custom-call | flops 402653184 | bytes 8388608 | tf_op jit(solution)/shard_map/mix/pallas_call | solution.py:299
  111.1 0.9 copy-done.1
  112.5 12.3 %attend.1 = (bf16[768,512]{1,0:T(8,128)(2,1)S(1)}, f32[8,768]{1,0:T(8,128)}) custom-call(bf16[800,2048]{1,0:T(8,128)(2,1)S(1)} %get-tuple-element.23.cin_ref.proj_ref.gate_ref.q_ref.kv_ref, bf16[800,2048]{1,0:T(8,128)(2,1)S(1)} %get-tuple-element.23.cin_ref.proj_ref.gate_ref.q_ref.kv_ref, bf16[128,256]{1,0:T(8,128)(2,1)S(1)} %get-tuple-element.32.before_ref, ...), custom_call_target="tpu_custom_call" | custom-call | flops 603979776 | bytes 4194304 | tf_op jit(solution)/shard_map/attend/pallas_call | solution.py:419
  124.8 2.5 %copy-done.14 = bf16[8,4,2,32,1280]{4,3,2,1,0:T(8,128)(2,1)S(1)} copy-done((bf16[8,4,2,32,1280]{4,3,2,1,0:T(8,128)(2,1)S(1)}, bf16[8,4,2,32,1280]{4,3,2,1,0:T(8,128)(2,1)}, u32[]{:S(2)}) %copy-start.14) | copy-done | bytes 5242904
  127.3 29.9 %finish.1 = bf16[768,512]{1,0:T(8,128)(2,1)S(1)} custom-call(bf16[768,512]{1,0:T(8,128)(2,1)S(1)} %copy-done.2, bf16[768,512]{1,0:T(8,128)(2,1)S(1)} %get-tuple-element.34.window_ref, bf16[2048,1280]{1,0:T(8,128)(2,1)S(1)} %bitcast.28), custom_call_target="tpu_custom_call" | custom-call | flops 3221225472 | bytes 8388608 | tf_op jit(solution)/shard_map/finish/pallas_call | solution.py:960
  157.2 0.9 copy.32
  (49 shorter events, 2.0 us)
Async XLA Ops:
  3.1 0.8 copy-start.5
  3.9 0.8 copy-start.6
  4.6 0.8 copy-start.7
  5.4 0.7 copy-start.8
  6.1 0.7 copy-start.9
  6.8 0.7 copy-start.10
  7.5 0.7 copy-start.11
  63.0 14.2 %copy-start.13 = (bf16[8,4,2,32,1280]{4,3,2,1,0:T(8,128)(2,1)}, bf16[8,4,2,32,1280]{4,3,2,1,0:T(8,128)(2,1)S(1)}, u32[]{:S(2)}) copy-start(bf16[8,4,2,32,1280]{4,3,2,1,0:T(8,128)(2,1)S(1)} %get-tuple-element.22) | copy-start | bytes 15728644
  63.7 3.0 %copy-start.12 = (bf16[768,2048]{1,0:T(8,128)(2,1)S(1)}, bf16[768,2048]{1,0:T(8,128)(2,1)}, u32[]{:S(2)}) copy-start(bf16[768,2048]{1,0:T(8,128)(2,1)} %tok_ref.1) | copy-start | bytes 9437188
  66.7 11.2 %copy-start.16 = (bf16[5,512]{1,0:T(8,128)(2,1)S(1)}, bf16[5,512]{1,0:T(8,128)(2,1)}, u32[]{:S(2)}) copy-start(bf16[5,512]{1,0:T(8,128)(2,1)} %param.25) | copy-start | bytes 15364
  66.7 11.3 %copy-start.17 = (bf16[5,1,128]{2,0,1:T(8,128)(2,1)S(1)}, bf16[5,1,128]{2,0,1:T(8,128)(2,1)}, u32[]{:S(2)}) copy-start(bf16[5,1,128]{2,0,1:T(8,128)(2,1)} %param.27) | copy-start | bytes 3844
  66.7 11.3 %copy-start.18 = (bf16[5,1,128]{2,0,1:T(8,128)(2,1)S(1)}, bf16[5,1,128]{2,0,1:T(8,128)(2,1)}, u32[]{:S(2)}) copy-start(bf16[5,1,128]{2,0,1:T(8,128)(2,1)} %param.26) | copy-start | bytes 3844
  66.7 11.3 %copy-start.15 = (f32[2,768,8]{1,2,0:T(8,128)S(1)}, f32[2,768,8]{1,2,0:T(8,128)}, u32[]{:S(2)}) copy-start(f32[2,768,8]{1,2,0:T(8,128)} %param.28) | copy-start | bytes 147460
  77.2 0.7 copy-start.3
  79.0 1.0 copy-start
  80.0 1.0 copy-start.4
  81.0 24.8 %copy-start.19 = (bf16[512]{0:T(512)(128)(2,1)S(1)}, bf16[512]{0:T(512)(128)(2,1)}, u32[]{:S(2)}) copy-start(bf16[512]{0:T(512)(128)(2,1)} %param.29) | copy-start | bytes 3076
  105.8 6.5 %copy-start.20 = (f32[8]{0:T(128)S(1)}, f32[8]{0:T(128)}, u32[]{:S(2)}) copy-start(f32[8]{0:T(128)} %param.33) | copy-start | bytes 100
  111.1 0.9 copy-start.1
  112.5 12.3 %copy-start.2 = (bf16[768,512]{1,0:T(8,128)(2,1)S(1)}, bf16[768,512]{1,0:T(8,128)(2,1)}, u32[]{:S(2)}) copy-start(bf16[768,512]{1,0:T(8,128)(2,1)} %copy-done.1) | copy-start | bytes 2359300
  124.8 2.5 %copy-start.14 = (bf16[8,4,2,32,1280]{4,3,2,1,0:T(8,128)(2,1)S(1)}, bf16[8,4,2,32,1280]{4,3,2,1,0:T(8,128)(2,1)}, u32[]{:S(2)}) copy-start(bf16[8,4,2,32,1280]{4,3,2,1,0:T(8,128)(2,1)} %copy-done.13) | copy-start | bytes 15728644

commit v3 on v2

--- a/solution.py
+++ b/solution.py
@@ -22,6 +22,8 @@
 BF16 = jnp.bfloat16
 MSG = STATE + 16
 KV_AT = 768
+GATE_AT = 1024
+Q_AT = 1536
 
 
 def dot(a, b, dims=((1,), (0,)), precision=None):
@@ -47,31 +49,15 @@
 
 
 def spread_matrix():
-    rows = jnp.arange(2 * HEADS)[:, None]
-    cols = jnp.arange(2 * HEADS * HEAD_DIM)[None, :] // HEAD_DIM
-    return (rows == cols).astype(BF16)
-
-
-def project_kernel(tok_ref, before_ref, after_ref, gain_ref, a_ref, b_ref, out_ref, step_ref, normed):
-    count = tok_ref.shape[0]
-    place = lax.axis_index(SP)
+    shape = (2 * HEADS, 2 * HEADS * HEAD_DIM)
+    rows = lax.broadcasted_iota(jnp.int32, shape, 0)
+    first = lax.broadcasted_iota(jnp.int32, shape, 1) - rows * HEAD_DIM
+    return jnp.where((first >= 0) & (first < HEAD_DIM), 1.0, 0.0).astype(BF16)
+
+
+def project_kernel(normed, a_ref, b_ref, out_ref, step_ref):
+    count = step_ref.shape[0]
     tile = 256
-
-    def norm(value):
-        wide = value.astype(F32)
-        scale = lax.rsqrt(jnp.mean(wide * wide, axis=1, keepdims=True) + EPS)
-        return wide * scale * gain_ref[...]
-
-    def one(i, carry):
-        rows = pl.ds(pl.multiple_of(i * BLOCK, BLOCK), BLOCK)
-        normed[rows, :] = norm(tok_ref[rows, :]).astype(BF16)
-        return carry
-
-    lax.fori_loop(0, count // BLOCK, one, 0)
-    before = jnp.where(place > 0, norm(before_ref[...]), 0.0)
-    normed[count : count + HALO, :] = before.astype(BF16)
-    after = jnp.where(place < lax.axis_size(SP) - 1, norm(after_ref[...]), 0.0)
-    normed[count + HALO : count + 2 * HALO, :] = after.astype(BF16)
 
     def column(j, carry):
         cols = pl.ds(pl.multiple_of(j * tile, tile), tile)
@@ -86,37 +72,37 @@
     ).astype(BF16)
 
 
-def project(tokens, before, after, gain, a, b):
-    count, width = tokens.shape
+def project(normed, count, a, b):
+    rows, width = normed.shape
     columns = 2048
     vmem = pl.BlockSpec(memory_space=pltpu.VMEM)
     return pl.pallas_call(
         project_kernel,
-        in_specs=[vmem] * 6,
+        in_specs=[vmem] * 3,
         out_specs=[vmem] * 2,
         out_shape=[
-            jax.ShapeDtypeStruct((count + 2 * HALO, columns), BF16),
+            jax.ShapeDtypeStruct((rows, columns), BF16),
             jax.ShapeDtypeStruct((count, 128), F32),
         ],
-        scratch_shapes=[pltpu.VMEM((count + 2 * HALO, width), BF16)],
         compiler_params=pltpu.CompilerParams(vmem_limit_bytes=12 << 20),
         cost_estimate=pl.CostEstimate(
-            flops=2 * count * width * (columns + 128),
-            bytes_accessed=2 * (count * width + width * columns + count * columns),
+            flops=2 * rows * width * (columns + 128),
+            bytes_accessed=2 * (rows * width + width * columns + rows * columns),
             transcendentals=0,
         ),
         name="project",
-    )(tokens, before, after, gain, a, b)
+    )(normed, a, b)
 
 
 def conv_state_kernel(
-    cin_ref, taps_ref, step_ref, rate_ref, e_ref,
+    cin_ref, taps_x_ref, taps_b_ref, taps_c_ref, step_ref, rate_ref,
     conv_ref, col_ref, row_ref, piece_ref, etot_ref, msg_ref, win, near,
 ):
     count = cin_ref.shape[0] - 2 * HALO
     blocks = count // BLOCK
     channels = HEADS * HEAD_DIM
-    spread_m = e_ref[...]
+    spread_m = spread_matrix()
+    taps = jnp.concatenate([t[...].astype(F32) for t in (taps_x_ref, taps_b_ref, taps_c_ref)], axis=1)
     lane16 = lax.broadcasted_iota(jnp.int32, (BLOCK, 2 * HEADS), 1)
     forward16 = lane16 < HEADS
     tri = (
@@ -137,15 +123,16 @@
         start = pl.multiple_of(i * BLOCK, BLOCK)
         rows = pl.ds(start, BLOCK)
         near[...] = win[pl.ds(start, BLOCK + 2 * HALO), :]
-        acc = near[HALO - 2 : HALO - 2 + BLOCK, :] * taps_ref[0:1, :]
+        acc = near[HALO - 2 : HALO - 2 + BLOCK, :] * taps[0:1, :]
         for tap in range(1, 5):
             first = HALO - 2 + tap
-            acc = acc + near[first : first + BLOCK, :] * taps_ref[tap : tap + 1, :]
+            acc = acc + near[first : first + BLOCK, :] * taps[tap : tap + 1, :]
         conv = (acc * jax.nn.sigmoid(acc)).astype(BF16)
         conv_ref[rows, :] = conv
         raw = step_ref[rows, 0 : 2 * HEADS]
         step = jnp.maximum(raw, 0.0) + jnp.log1p(jnp.exp(-jnp.abs(raw)))
-        decay = -jnp.exp(rate_ref[rows, :]) * step
+        rate = jnp.concatenate([rate_ref[:, rows], jnp.zeros((BLOCK - 2 * HEADS, BLOCK), F32)], axis=0)
+        decay = -jnp.exp(rate.T[:, 0 : 2 * HEADS]) * step
         cum = dot(tri, decay, precision=lax.Precision.HIGHEST)
         tot = cum[BLOCK - 1 : BLOCK, :]
         col = jnp.where(forward16, cum, cum - decay)
@@ -185,9 +172,9 @@
             msg_ref[e, pair, STATE:MSG, :] = tail[:, e * channels + pair * 128 : e * channels + pair * 128 + 128]
 
 
-def conv_state(proj, taps, step_raw, rate, spread_m):
+def conv_state(proj, taps, step_raw, rate):
     count = step_raw.shape[0]
-    width = taps.shape[1]
+    width = sum(t.shape[1] for t in taps)
     blocks = count // BLOCK
     channels = HEADS * HEAD_DIM
     whole = lambda shape: pl.BlockSpec(shape, lambda i: (0,) * len(shape))
@@ -196,10 +183,9 @@
         grid=(1,),
         in_specs=[
             pl.BlockSpec((proj.shape[0], width), lambda i: (0, 0)),
-            whole(taps.shape),
+            *(whole(t.shape) for t in taps),
             whole(step_raw.shape),
             whole(rate.shape),
-            whole(spread_m.shape),
         ],
         out_specs=[
             whole((count, width)),
@@ -226,17 +212,15 @@
             flops=2 * count * STATE * 2 * channels, bytes_accessed=12 << 20, transcendentals=0
         ),
         name="conv_state",
-    )(proj, taps, step_raw, rate, spread_m)
-
-
-def mix_kernel(
-    conv_ref, col_ref, row_ref, piece_ref, etot_ref, in_ref, gate_ref, gain_ref, e_ref,
-    out_ref, held,
-):
+    )(proj, *taps, step_raw, rate)
+
+
+def mixer(conv_ref, col_ref, row_ref, piece_ref, etot_ref, in_ref, proj_ref, gain_ref, out_ref, held):
     count = conv_ref.shape[0]
     blocks = count // BLOCK
     channels = HEADS * HEAD_DIM
-    spread_m = e_ref[...]
+    spread_m = spread_matrix()
+    gain = gain_ref[...].astype(F32)
     for e in range(2):
         state = jnp.concatenate(
             [in_ref[e, p].astype(F32) for p in range(channels // 128)], axis=1
@@ -252,7 +236,7 @@
     first_half = col_at < HEAD_DIM
     forward16 = lax.broadcasted_iota(jnp.int32, (BLOCK, 2 * HEADS), 1) < HEADS
 
-    def one(i, carry):
+    def one(i):
         rows = pl.ds(pl.multiple_of(i * BLOCK, BLOCK), BLOCK)
         inflow = conv_ref[rows, channels : channels + STATE]
         readout = conv_ref[rows, channels + STATE : channels + 2 * STATE]
@@ -282,58 +266,18 @@
             )
             parts.append(dot(jnp.concatenate(weights, axis=1), stacked))
         y = jnp.concatenate(parts, axis=1) + far[:, 0:channels] + far[:, channels:]
-        gate = gate_ref[rows, :].astype(F32)
+        gate = proj_ref[rows, GATE_AT : GATE_AT + channels].astype(F32)
         y = y * (gate * jax.nn.sigmoid(gate))
         y = y * lax.rsqrt(jnp.mean(y * y, axis=1, keepdims=True) + EPS)
-        out_ref[rows, :] = (y * gain_ref[...]).astype(BF16)
-        return carry
-
-    lax.fori_loop(0, blocks, one, 0)
-
-
-def mix(conv, col, row, piece, etot, incoming, proj, gate_block, gain, spread_m):
-    count = conv.shape[0]
-    blocks = count // BLOCK
-    channels = HEADS * HEAD_DIM
-    whole = lambda shape: pl.BlockSpec(shape, lambda i: (0,) * len(shape))
-    return pl.pallas_call(
-        mix_kernel,
-        grid=(1,),
-        in_specs=[
-            whole(conv.shape), whole(col.shape), whole(row.shape), whole(piece.shape),
-            whole(etot.shape), whole(incoming.shape),
-            pl.BlockSpec((count, channels), lambda i: (0, gate_block)),
-            whole(gain.shape), whole(spread_m.shape),
-        ],
-        out_specs=whole((count, channels)),
-        out_shape=jax.ShapeDtypeStruct((count, channels), BF16),
-        scratch_shapes=[pltpu.VMEM((blocks, STATE, 2 * channels), BF16)],
-        compiler_params=pltpu.CompilerParams(vmem_limit_bytes=16 << 20),
-        cost_estimate=pl.CostEstimate(
-            flops=2 * count * BLOCK * 4 * channels, bytes_accessed=8 << 20, transcendentals=0
-        ),
-        name="mix",
-    )(conv, col, row, piece, etot, incoming, proj, gain, spread_m)
-
-
-def rope_tables(first_row, grid_rows):
-    quarter = HEAD_DIM // 4
-    lane = jnp.arange(2 * HEAD_DIM)
-    freqs = ROPE_BASE ** (-(lane % quarter).astype(F32) / quarter)
-    sign = jnp.where(lane % (2 * quarter) < quarter, -1.0, 1.0)
-    row_angle = (first_row + jnp.arange(grid_rows, dtype=jnp.int32)).astype(F32)[:, None] * freqs
-    col_angle = jnp.arange(GRID_W, dtype=jnp.int32).astype(F32)[:, None] * freqs
-    return (
-        jnp.stack([jnp.cos(row_angle), jnp.sin(row_angle) * sign]),
-        jnp.stack([jnp.cos(col_angle), jnp.sin(col_angle) * sign]),
-    )
-
-
-def attend_kernel(
-    q_ref, kv_ref, before_ref, after_ref, by_row_ref, by_col_ref, sink_ref,
-    out_ref, log_ref, keys, values,
+        out_ref[rows, :] = (y * gain).astype(BF16)
+
+    return one
+
+
+def attention(
+    count, proj_ref, before_ref, after_ref, freq_ref, sink_ref,
+    out_ref, log_ref, keys, values, by_row, by_col,
 ):
-    count = q_ref.shape[0]
     blocks = count // BLOCK
     place = lax.axis_index(SP)
     lane = lax.broadcasted_iota(jnp.int32, (BLOCK, 128), 1)
@@ -341,13 +285,22 @@
     first_half = lane < HEAD_DIM
     row_lane = (lane % HEAD_DIM < 32)[0:GRID_W]
 
+    grid_rows = by_row.shape[1]
+    first_row = place * (count // GRID_W) - WINDOW // GRID_W
+    sign = jnp.where(low_quarter, -1.0, 1.0)
+    for ref, first, length in ((by_row, first_row, grid_rows), (by_col, 0, GRID_W)):
+        at = lax.broadcasted_iota(jnp.int32, (length, 128), 0) + first
+        angle = at.astype(F32) * freq_ref[0:1, :]
+        ref[0] = jnp.cos(angle)
+        ref[1] = jnp.sin(angle) * sign[0:length]
+
     def tables(slot):
         out = []
         for kind in range(2):
             parts = []
             for r in range(BLOCK // GRID_W):
-                row = by_row_ref[kind, pl.ds(slot * (BLOCK // GRID_W) + r, 1), :]
-                parts.append(jnp.where(row_lane, row, by_col_ref[kind]))
+                row = by_row[kind, pl.ds(slot * (BLOCK // GRID_W) + r, 1), :]
+                parts.append(jnp.where(row_lane, row, by_col[kind]))
             out.append(jnp.concatenate(parts, axis=0))
         return out
 
@@ -364,21 +317,26 @@
         keys[1, rows, :] = jnp.where(first_half, swapped, key).astype(BF16)
         values[:, rows] = raw[:, 128:256].astype(F32).T.astype(BF16)
 
-    store(before_ref[...], 0)
-    store(after_ref[...], blocks + 1)
-
-    def fill(i, carry):
-        store(kv_ref[pl.ds(pl.multiple_of(i * BLOCK, BLOCK), BLOCK), :], i + 1)
-        return carry
-
-    lax.fori_loop(0, blocks, fill, 0)
+    def own_keys():
+        def fill(i, carry):
+            rows = pl.ds(pl.multiple_of(i * BLOCK, BLOCK), BLOCK)
+            store(proj_ref[rows, KV_AT : KV_AT + 256], i + 1)
+            return carry
+
+        lax.fori_loop(0, blocks, fill, 0)
+
+    def edge_keys():
+        store(before_ref[...], 0)
+        store(after_ref[...], blocks + 1)
+
     key_at = lax.broadcasted_iota(jnp.int32, (3 * BLOCK, 2 * BLOCK), 0)
     query_at = lax.broadcasted_iota(jnp.int32, (3 * BLOCK, 2 * BLOCK), 1) % BLOCK
     in_band = (key_at >= query_at) & (key_at <= query_at + 2 * WINDOW)
+    first_row_half = lax.broadcasted_iota(jnp.int32, (1, 2 * BLOCK), 1) < BLOCK
     start_at = -place * count
     end_at = start_at + count * lax.axis_size(SP)
 
-    def one(i, carry):
+    def one(i):
         start = pl.multiple_of(i * BLOCK, BLOCK)
         rows = pl.ds(start, BLOCK)
         here = key_at + (start - WINDOW)
@@ -388,14 +346,14 @@
         for pair in range(HEADS // 2):
             group = pair // 2
             lanes = slice(pair * 128, pair * 128 + 128)
-            q = (turn(q_ref[rows, lanes], table).astype(F32) * HEAD_DIM ** (-0.5)).astype(BF16)
+            q = (turn(proj_ref[rows, Q_AT + pair * 128 : Q_AT + pair * 128 + 128], table).astype(F32) * HEAD_DIM ** (-0.5)).astype(BF16)
             zero = jnp.zeros_like(q)
             both = jnp.concatenate(
                 [jnp.where(first_half, q, zero), jnp.where(first_half, zero, q)], axis=0
             )
             scores = dot(keys[group, band, :], both, ((1,), (1,)))
             scores = jnp.where(valid, scores, -1e30)
-            sink = sink_ref[pair : pair + 1, :]
+            sink = jnp.where(first_row_half, sink_ref[2 * pair], sink_ref[2 * pair + 1])
             top = jnp.maximum(jnp.max(scores, axis=0, keepdims=True), sink)
             expo = jnp.exp(scores - top)
             total = jnp.sum(expo, axis=0, keepdims=True) + jnp.exp(sink - top)
@@ -406,40 +364,8 @@
             log = top + jnp.log(total)
             log_ref[2 * pair : 2 * pair + 1, rows] = log[:, 0:BLOCK]
             log_ref[2 * pair + 1 : 2 * pair + 2, rows] = log[:, BLOCK:]
-        return carry
-
-    lax.fori_loop(0, blocks, one, 0)
-
-
-def attend(count, proj, q_block, kv_block, before, after, tables, sinks):
-    channels = HEADS * HEAD_DIM
-    whole = lambda shape: pl.BlockSpec(shape, lambda i, *_: (0,) * len(shape))
-    by_row, by_col = tables
-    wide_sinks = jnp.repeat(sinks.reshape(HEADS // 2, 2), BLOCK, axis=1)
-    return pl.pallas_call(
-        attend_kernel,
-        grid=(1,),
-        in_specs=[
-            pl.BlockSpec((count, channels), lambda i: (0, q_block)),
-            pl.BlockSpec((count, 256), lambda i: (0, kv_block)),
-            whole(before.shape), whole(after.shape), whole(by_row.shape), whole(by_col.shape),
-            whole(wide_sinks.shape),
-        ],
-        out_specs=[whole((count, channels)), whole((HEADS, count))],
-        out_shape=[
-            jax.ShapeDtypeStruct((count, channels), BF16),
-            jax.ShapeDtypeStruct((HEADS, count), F32),
-        ],
-        scratch_shapes=[
-            pltpu.VMEM((2, count + 2 * BLOCK, 128), BF16),
-            pltpu.VMEM((128, count + 2 * BLOCK), BF16),
-        ],
-        compiler_params=pltpu.CompilerParams(vmem_limit_bytes=12 << 20),
-        cost_estimate=pl.CostEstimate(
-            flops=4 * count * 3 * BLOCK * channels, bytes_accessed=4 << 20, transcendentals=0
-        ),
-        name="attend",
-    )(proj, proj, before, after, by_row, by_col, wide_sinks)
+
+    return own_keys, edge_keys, one
 
 
 LINKS = ("z+", "z-", "y+", "y-")
@@ -527,9 +453,10 @@
 
 
 def gather_kernel(
-    lengths, edges_ref, value_ref, inflow_ref, readout_ref, key_ref, vector_ref, gate_ref,
-    query_ref, step_ref, turned_ref,
-    a_ref, b_ref, before_ref, after_ref, send_sem, recv_sem, core_send, core_recv, edge_sem,
+    lengths, tok_ref, gain_ref, step_ref, value_ref, inflow_ref, readout_ref, key_ref, vector_ref,
+    gate_ref, query_ref, state_ref, window_ref,
+    a_ref, b_ref, normed, before, after, held, send_sem, recv_sem, core_send, core_recv, edge_sem,
+    own_sem,
 ):
     length_z, length_y = lengths
     z, y, c = (lax.axis_index(a) for a in SP)
@@ -562,16 +489,33 @@
     for peer in peers:
         pl.semaphore_signal(barrier, inc=1, device_id=peer, device_id_type=mesh_id)
 
-    own_a, own_b = a_ref.at[z, y, c], b_ref.at[z, y, c]
-    column = 0
-    for ref in (value_ref, inflow_ref, readout_ref, key_ref, vector_ref, gate_ref):
-        own_a[:, column : column + ref.shape[1]] = ref[...]
-        column += ref.shape[1]
+    count_rows = tok_ref.shape[0]
     half = query_ref.shape[1] // 2
-    own_a[:, column : column + half] = query_ref[:, 0:half]
-    own_a[:, column + half : WIDTH_A] = step_ref[...]
-    own_b[:, 0 : turned_ref.shape[1]] = turned_ref[...]
-    own_b[:, turned_ref.shape[1] : WIDTH_B] = query_ref[:, half : 2 * half]
+    moves = []
+    for array, refs in (
+        (a_ref, (value_ref, inflow_ref, readout_ref, key_ref, vector_ref, gate_ref, query_ref)),
+        (b_ref, (state_ref, window_ref, query_ref)),
+    ):
+        column = 0
+        for ref in refs:
+            width = ref.shape[1]
+            src = ref
+            if ref is query_ref:
+                src = ref.at[:, pl.ds(0 if array is a_ref else half, half)]
+                width = half
+            moves.append((src, array.at[z, y, c, :, pl.ds(column, width)]))
+            column += width
+    moves.append((tok_ref, held))
+    moves = [pltpu.make_async_copy(*move, own_sem.at[i]) for i, move in enumerate(moves)]
+    for move in moves:
+        move.start()
+    step = step_ref[...].astype(F32)
+    rows, cols = step.shape
+    step = jnp.concatenate([step, jnp.zeros((rows, 128 - cols), F32)], axis=1)
+    step = jnp.concatenate([step, jnp.zeros((128 - rows, 128), F32)], axis=0)
+    a_ref[z, y, c, :, WIDTH_A - 128 : WIDTH_A] = step.T[0:cols, :].astype(BF16)
+    for move in moves[:-1]:
+        move.wait()
     pl.semaphore_wait(barrier, len(peers))
 
     sends = transfers(length_z, length_y)
@@ -593,14 +537,25 @@
             device_id=towards(s["axis"], s["sign"]), device_id_type=mesh_id,
         )
 
-    edge_rows = edges_ref.shape[0] // 2
     edge_copies = []
-    for k, (index, dst) in enumerate(((flat - 1, after_ref), (flat + 1, before_ref))):
+    for k, (index, dst) in enumerate(((flat - 1, after), (flat + 1, before))):
         edge_copies.append(pltpu.make_async_remote_copy(
-            src_ref=edges_ref.at[pl.ds(k * edge_rows, edge_rows)], dst_ref=dst,
+            src_ref=tok_ref.at[pl.ds(k * (count_rows - HALO), HALO)], dst_ref=dst,
             send_sem=edge_sem.at[k, 0], recv_sem=edge_sem.at[k, 1],
             device_id=device_at(index), device_id_type=mesh_id,
         ))
+
+    gain = gain_ref[...].astype(F32)
+
+    def norm(value):
+        wide = value.astype(F32)
+        scale = lax.rsqrt(jnp.mean(wide * wide, axis=1, keepdims=True) + EPS)
+        return wide * scale * gain
+
+    def norm_block(i, carry):
+        rows = pl.ds(pl.multiple_of(i * BLOCK, BLOCK), BLOCK)
+        normed[rows, :] = norm(held[rows, :]).astype(BF16)
+        return carry
 
     first, order, _ = arrival_order(sends)
     started = []
@@ -610,6 +565,8 @@
         started.append(copy)
     for copy in edge_copies:
         copy.start()
+    moves[-1].wait()
+    lax.fori_loop(0, count_rows // BLOCK, norm_block, 0)
 
     waiting = {}
     for kind, first_axis, length, second in (("A", "z", length_z, "y"), ("B", "y", length_y, "z")):
@@ -666,39 +623,47 @@
         wait_core(key)
     for copy in edge_copies:
         copy.wait()
-
-
-def gather(length_z, length_y, edges, *shards):
+    normed[count_rows : count_rows + HALO, :] = jnp.where(flat > 0, norm(before[...]), 0.0).astype(BF16)
+    normed[count_rows + HALO : count_rows + 2 * HALO, :] = jnp.where(
+        flat < count - 1, norm(after[...]), 0.0
+    ).astype(BF16)
+
+
+def gather(length_z, length_y, tokens, gain, step, *shards):
     sends = transfers(length_z, length_y)
     groups = length_z + length_y
     vmem = pl.BlockSpec(memory_space=pltpu.VMEM)
+    hbm = pl.BlockSpec(memory_space=pl.ANY)
     dma = pltpu.SemaphoreType.DMA
     lead = (length_z, length_y, 2, 32)
-    edge = (edges.shape[0] // 2, edges.shape[1])
-    a, b, before, after = pl.pallas_call(
+    rows, width = tokens.shape
+    edge = pltpu.VMEM((HALO, width), BF16)
+    a, b, normed = pl.pallas_call(
         functools.partial(gather_kernel, (length_z, length_y)),
-        in_specs=[vmem] * (1 + len(shards)),
-        out_specs=[vmem] * 4,
+        in_specs=[hbm, vmem, vmem] + [hbm] * len(shards),
+        out_specs=[vmem] * 3,
         out_shape=[
             jax.ShapeDtypeStruct((*lead, WIDTH_A), BF16),
             jax.ShapeDtypeStruct((*lead, WIDTH_B), BF16),
-            jax.ShapeDtypeStruct(edge, BF16),
-            jax.ShapeDtypeStruct(edge, BF16),
+            jax.ShapeDtypeStruct((rows + 2 * HALO, width), BF16),
         ],
         scratch_shapes=[
+            edge, edge, pltpu.VMEM((rows, width), BF16),
             dma((len(sends),)), dma((len(sends),)), dma((groups,)), dma((groups,)), dma((2, 2)),
+            dma((len(shards) + 2,)),
         ],
         compiler_params=pltpu.CompilerParams(
-            collective_id=2, has_side_effects=True, vmem_limit_bytes=20 << 20
+            collective_id=2, has_side_effects=True, vmem_limit_bytes=28 << 20
         ),
         cost_estimate=pl.CostEstimate(flops=1 << 24, bytes_accessed=24 << 20, transcendentals=0),
         name="gather",
-    )(edges, *shards)
-    return a.reshape(-1, WIDTH_A), b.reshape(-1, WIDTH_B), before, after
+    )(tokens, gain, step, *shards)
+    return a.reshape(-1, WIDTH_A), b.reshape(-1, WIDTH_B), normed
 
 
 def exchange_kernel(
-    rows, msg_ref, proj_ref, out_ref, kv_before_ref, kv_after_ref, part, turned, by_y, summed, by_z, back, arrived, nxt, final, carry,
+    rows, msg_ref, proj_ref, freq_ref, sink_ref, out_ref, window_ref, log_ref,
+    kv_before_ref, kv_after_ref, keys, values, by_row, by_col, part, turned, by_y, summed, by_z, back, arrived, nxt, final, carry,
     part_sem, y_sem, z_sem, back_sem, final_sem, kv_sem,
 ):
     z, y, c = (lax.axis_index(a) for a in SP)
@@ -759,6 +724,20 @@
         ),
         send(proj_ref.at[pl.ds(0, WINDOW), kv_cols], kv_after_ref, kv_sem.at[1], device_at(flat - 1)),
     ]
+    own_keys, edge_keys, attend = attention(
+        rows, proj_ref, kv_before_ref, kv_after_ref, freq_ref, sink_ref,
+        window_ref, log_ref, keys, values, by_row, by_col,
+    )
+
+    def attend_blocks(first, last):
+        def one(i, carry):
+            attend(i)
+            return carry
+
+        lax.fori_loop(first, last, one, 0)
+
+    blocks = rows // BLOCK
+    own_keys()
     copy.wait()
     for j in range(pairs):
         decay = decay_of(part, j)
@@ -773,6 +752,7 @@
         to = lax.rem(y + k, length_y)
         copies.append(send(turned.at[to], by_y.at[k], y_sem.at[k], {SP[1]: to}))
     by_y[0] = turned[y]
+    attend_blocks(1, 2)
     for copy in copies:
         copy.wait()
     before = []
@@ -793,6 +773,7 @@
             send(summed, by_z.at[k], z_sem.at[k], {SP[0]: to})
 
     carry[...] = jnp.zeros_like(carry)
+    attend_blocks(2, blocks - 1)
     for distance in reversed(range(1, length_z)):
         slot = jnp.where(forward, distance, length_z - distance)
 
@@ -824,6 +805,10 @@
         to = lax.rem(y + k, length_y)
         copies.append(send(back.at[to], arrived.at[k], back_sem.at[k], {SP[1]: to}))
     arrived[0] = back[y]
+    for copy in kv_copies:
+        copy.wait()
+    edge_keys()
+    attend(0)
     for copy in copies:
         copy.wait()
     for j in range(pairs):
@@ -832,27 +817,35 @@
         nxt[j] = (
             jnp.exp(decay_of(msg_ref, c, j)) * state.astype(F32) + state_of(msg_ref, c, j)
         ).astype(BF16)
-    send(nxt, final, final_sem, {SP[2]: other}).wait()
+    copy = send(nxt, final, final_sem, {SP[2]: other})
+    attend(blocks - 1)
+    copy.wait()
     out_ref[other] = final[...]
-    for copy in kv_copies:
-        copy.wait()
-
-
-def exchange(message, proj, rows, length_z, length_y):
+
+
+def exchange(message, proj, rows, freqs, sinks, length_z, length_y):
     pairs = message.shape[1]
+    channels = HEADS * HEAD_DIM
     tile = (STATE, 128)
     full = (MSG, 128)
     dma = pltpu.SemaphoreType.DMA
+    vmem = pl.BlockSpec(memory_space=pltpu.VMEM)
     return pl.pallas_call(
         functools.partial(exchange_kernel, rows),
-        in_specs=[pl.BlockSpec(memory_space=pltpu.VMEM)] * 2,
-        out_specs=[pl.BlockSpec(memory_space=pltpu.VMEM)] * 3,
+        in_specs=[vmem, vmem, vmem, pl.BlockSpec(memory_space=pltpu.SMEM)],
+        out_specs=[vmem] * 3,
         out_shape=[
             jax.ShapeDtypeStruct((2, pairs, *tile), BF16),
-            jax.ShapeDtypeStruct((WINDOW, 256), BF16),
-            jax.ShapeDtypeStruct((WINDOW, 256), BF16),
+            jax.ShapeDtypeStruct((rows, channels), BF16),
+            jax.ShapeDtypeStruct((HEADS, rows), F32),
         ],
         scratch_shapes=[
+            pltpu.VMEM((WINDOW, 256), BF16),
+            pltpu.VMEM((WINDOW, 256), BF16),
+            pltpu.VMEM((2, rows + 2 * BLOCK, 128), BF16),
+            pltpu.VMEM((128, rows + 2 * BLOCK), BF16),
+            pltpu.VMEM((2, (rows + 2 * WINDOW) // GRID_W, 128), F32),
+            pltpu.VMEM((2, GRID_W, 128), F32),
             pltpu.VMEM((pairs, *full), BF16),
             pltpu.VMEM((pairs, *full), BF16),
             pltpu.VMEM((length_y, *full), BF16),
@@ -867,20 +860,28 @@
             dma((2, 2)),
         ],
         compiler_params=pltpu.CompilerParams(
-            collective_id=1, has_side_effects=True, vmem_limit_bytes=8 << 20
+            collective_id=1, has_side_effects=True, vmem_limit_bytes=16 << 20
         ),
-        cost_estimate=pl.CostEstimate(flops=1 << 24, bytes_accessed=1 << 20, transcendentals=0),
+        cost_estimate=pl.CostEstimate(
+            flops=4 * rows * 3 * BLOCK * channels, bytes_accessed=8 << 20, transcendentals=0
+        ),
         name="exchange",
-    )(message, proj)
-
-
-def finish_kernel(state_ref, window_ref, w_ref, out_ref, *refs):
-    far_out, far_in, near_out, near_in, far_sem, near_sem = refs
+    )(message, proj, freqs, sinks)
+
+
+def finish_kernel(
+    window_ref, w_ref, conv_ref, col_ref, row_ref, piece_ref, etot_ref, in_ref, proj_ref, gain_ref,
+    out_ref, *refs
+):
+    state_ref, held, far_out, far_in, near_out, near_in, far_sem, near_sem = refs
     n = lax.axis_size("tp")
     me = lax.axis_index("tp")
     mesh_id = pl.DeviceIdType.MESH
     sides = (1, -1)
     count, channels = state_ref.shape
+    mix = mixer(
+        conv_ref, col_ref, row_ref, piece_ref, etot_ref, in_ref, proj_ref, gain_ref, state_ref, held
+    )
     width = w_ref.shape[0] // n
     half = width // 2
     chunk = far_out.shape[2]
@@ -914,6 +915,7 @@
 
     def send_far(i, carry):
         rows = pl.ds(pl.multiple_of(i * chunk, chunk), chunk)
+        mix(i)
         value = terms(rows, at(2)).astype(BF16)
         for k in range(2):
             far_out[k, i] = value[:, k * half : (k + 1) * half]
@@ -950,19 +952,21 @@
     lax.fori_loop(0, chunks, collect, 0)
 
 
-def finish(state, window, weights, n):
-    count, channels = state.shape
+def finish(window, weights, mixed_from, n):
+    count, channels = window.shape
     width = weights.shape[0] // n
-    chunk = 128
+    chunk = BLOCK
     chunks = count // chunk
     vmem = pl.BlockSpec(memory_space=pltpu.VMEM)
     dma = pltpu.SemaphoreType.DMA
     return pl.pallas_call(
         finish_kernel,
-        in_specs=[vmem] * 3,
+        in_specs=[vmem] * (2 + len(mixed_from)),
         out_specs=vmem,
         out_shape=jax.ShapeDtypeStruct((count, width), BF16),
         scratch_shapes=[
+            pltpu.VMEM((count, channels), BF16),
+            pltpu.VMEM((chunks, STATE, 2 * channels), BF16),
             pltpu.VMEM((2, chunks, chunk, width // 2), BF16),
             pltpu.VMEM((2, chunks, chunk, width // 2), BF16),
             pltpu.VMEM((2, chunks, chunk, width), BF16),
@@ -970,13 +974,13 @@
             dma((2, chunks, 2)), dma((2, chunks, 2)),
         ],
         compiler_params=pltpu.CompilerParams(
-            collective_id=3, has_side_effects=True, vmem_limit_bytes=24 << 20
+            collective_id=3, has_side_effects=True, vmem_limit_bytes=28 << 20
         ),
         cost_estimate=pl.CostEstimate(
             flops=4 * count * channels * width * n, bytes_accessed=8 << 20, transcendentals=0
         ),
         name="finish",
-    )(state, window, weights)
+    )(window, weights, *mixed_from)
 
 
 def flatten_rows(weight):
@@ -989,30 +993,27 @@
     vector_weight, sink_logit, state_out, window_out,
 ):
     count = tokens.shape[0]
-    place = lax.axis_index(SP)
     length_z, length_y = lax.axis_size(SP[0]), lax.axis_size(SP[1])
-    spread_m = spread_matrix()
-    rate = jnp.concatenate([log_rate[0], log_rate[1]], axis=1)
-    taps = jnp.concatenate(
-        [conv_values, flatten_rows(conv_inflow), flatten_rows(conv_readout)], axis=1
+    quarter = HEAD_DIM // 4
+    freqs = ROPE_BASE ** (-(jnp.arange(128) % quarter).astype(F32) / quarter)
+    freqs = jnp.broadcast_to(freqs, (8, 128))
+    step_turned = step_weight.transpose(1, 2, 0).reshape(2 * HEADS, -1)
+    a, b, normed = gather(
+        length_z, length_y, tokens, input_gain[None], step_turned, value_weight,
+        flatten_rows(inflow_weight), flatten_rows(readout_weight), key_weight, vector_weight,
+        gate_weight, query_weight, state_out.T, window_out.T,
     )
-    taps = jnp.pad(taps.astype(F32), ((0, 3), (0, 0)))
-    tables = rope_tables((place * count - WINDOW) // GRID_W, (count + 2 * WINDOW) // GRID_W)
-    edges = jnp.concatenate([tokens[:HALO], tokens[-HALO:]], axis=0)
-    a, b, before, after = gather(
-        length_z, length_y, edges, value_weight, flatten_rows(inflow_weight),
-        flatten_rows(readout_weight), key_weight, vector_weight, gate_weight, query_weight,
-        jnp.pad(flatten_rows(step_weight), ((0, 0), (0, 128 - 2 * HEADS))),
-        jnp.concatenate([state_out, window_out], axis=0).T,
+    proj, step_raw = project(normed, count, a, b)
+    taps = (conv_values, flatten_rows(conv_inflow), flatten_rows(conv_readout))
+    rate = log_rate.transpose(0, 2, 1).reshape(2 * HEADS, count)
+    conv, col, row, piece, etot, message = conv_state(proj, taps, step_raw, rate)
+    incoming, window, logs = exchange(
+        message, proj, count, freqs, sink_logit, length_z, length_y
     )
-    proj, step_raw = project(tokens, before, after, input_gain.astype(F32)[None], a, b)
-    conv, col, row, piece, etot, message = conv_state(proj, taps, step_raw, rate, spread_m)
-    incoming, kv_before, kv_after = exchange(message, proj, count, length_z, length_y)
-    window, logs = attend(count, proj, 3, 3, kv_before, kv_after, tables, sink_logit)
-    state = mix(
-        conv, col, row, piece, etot, incoming, proj, 2, group_gain.astype(F32)[None], spread_m
+    mixed = finish(
+        window, b, (conv, col, row, piece, etot, incoming, proj, group_gain[None]),
+        lax.axis_size("tp"),
     )
-    mixed = finish(state, window, b, lax.axis_size("tp"))
     return mixed, logs.T
 
 

time: 159 us -> 135 us (0.85)
  Pallas kernels: 138 us -> 122 us
  local copies, waits for them, and re-layouts: 17.8 us -> 11.4 us
  other arithmetic: 1.89 us -> 0.01 us
    pallas_call x5 -> x3, Pallas kernels: 76.5 us -> 60.3 us  [the longest x1 30.9 us: finish(): pl.pallas_call(finish_kernel, in_specs=[vmem] * (2 + len(mixed_from)), ou...]
    unnamed x45 -> x36, local copies, waits for them, and re-layouts: 15.2 us -> 10.7 us
where the time goes in v3:
time: 135 us; the launch traced here: 134 us
  Pallas kernels  122 us (90%)
  local copies, waits for them, and re-layouts  11.4 us (8%)
    pallas_call x1, Pallas kernels, gather(): pl.pallas_call(functools.partial(gather_kernel, (length_z, length_y)), in...  55.1 us
    pallas_call x1, Pallas kernels, finish(): pl.pallas_call(finish_kernel, in_specs=[vmem] * (2 + len(mixed_from)), ou...  30.9 us
    pallas_call x1, Pallas kernels, exchange(): pl.pallas_call(functools.partial(exchange_kernel, rows), in_specs=[vmem,...  20.4 us
    unnamed x36, local copies, waits for them, and re-layouts  10.7 us
    pallas_call x1, Pallas kernels, project(): pl.pallas_call(project_kernel, in_specs=[vmem] * 3, out_specs=[vmem] * 2,...  8.96 us
    pallas_call x1, Pallas kernels, conv_state(): pl.pallas_call(conv_state_kernel, grid=(1,), in_specs=[pl.BlockSpec((proj...  6.65 us

profile of v3, /device:TPU:1, one launch (start us, length us, event | category | flops | bytes accessed | tf_op | source)
XLA Modules:
  0.0 134.2 jit_solution(936962184370837258)
XLA Ops:
  0.6 0.7 broadcast_in_dim.9.gain_ref
  1.3 1.9 %copy-done = bf16[768,2048]{1,0:T(8,128)(2,1)S(1)} copy-done((bf16[768,2048]{1,0:T(8,128)(2,1)S(1)}, bf16[768,2048]{1,0:T(8,128)(2,1)}, u32[]{:S(2)}) %copy-start) | copy-done | bytes 3145752
  3.2 0.8 copy-done.2
  4.0 0.8 copy-done.3
  4.7 0.8 copy-done.4
  5.5 0.8 copy-done.5
  6.2 0.8 copy-done.6
  7.0 0.7 copy-done.7
  7.7 0.7 copy-done.8
  8.4 0.7 copy-done.9
  9.1 0.7 copy-done.10
  9.8 0.7 copy-done.12
  10.5 55.1 %gather.1 = (bf16[8,4,2,32,1920]{4,3,2,1,0:T(8,128)(2,1)S(1)}, bf16[8,4,2,32,1280]{4,3,2,1,0:T(8,128)(2,1)S(1)}, bf16[800,2048]{1,0:T(8,128)(2,1)S(1)}) custom-call(bf16[768,2048]{1,0:T(8,128)(2,1)S(1)} %copy-done, bf16[1,2048]{1,0:T(2,128)(2,1)S(1)} %broadcast_in_dim.9.gain_ref, bf16[16,32]{1,0:T(8,128)(2,1)S(1)} %bitcast.23, ...), custom_call_target="tpu_custom_call" | custom-call | flops 16777216 | bytes 25165824 | tf_op jit(solution)/shard_map/gather/pallas_call | solution.py:641
  65.6 0.0 copy-start.1
  65.6 0.0 copy-start.11
  65.6 0.0 copy-start.13
  65.6 0.0 copy-start.14
  65.6 9.0 %project.1 = (bf16[800,2048]{1,0:T(8,128)(2,1)S(1)}, f32[768,128]{1,0:T(8,128)S(1)}) custom-call(bf16[800,2048]{1,0:T(8,128)(2,1)S(1)} %get-tuple-element.16.normed, bf16[2048,1920]{1,0:T(8,128)(2,1)S(1)} %bitcast.26, bf16[2048,1280]{1,0:T(8,128)(2,1)S(1)} %bitcast.15), custom_call_target="tpu_custom_call" | custom-call | flops 7130316800 | bytes 14942208 | tf_op jit(solution)/shard_map/project/pallas_call | solution.py:79
  74.6 0.0 copy-start.15
  74.6 6.7 %conv_state.1 = (bf16[768,768]{1,0:T(8,128)(2,1)S(1)}, f32[768,32]{1,0:T(8,128)S(1)}, f32[6,32,128]{2,1,0:T(8,128)S(1)}, f32[6,128,1024]{2,1,0:T(8,128)S(1)}, f3...) custom-call(bf16[800,2048]{1,0:T(8,128)(2,1)S(1)} %get-tuple-element.19.cin_ref.proj_ref, ...), custom_call_target="tpu_custom_call" | custom-call | flops 201326592 | bytes 12582912 | tf_op jit(solution)/shard_map/conv_state/pallas_call | solution.py:181
  81.3 20.4 %exchange.1 = (bf16[2,4,128,128]{3,2,1,0:T(8,128)(2,1)S(1)}, bf16[768,512]{1,0:T(8,128)(2,1)S(1)}, f32[8,768]{1,0:T(8,128)S(1)}) custom-call(bf16[2,4,144,128]{3,2,1,0:T(8,128)(2,1)S(1)} %get-tuple-element.21.msg_ref, bf16[800,2048]{1,0:T(8,128)(2,1)S(1)} %get-tuple-element.19.cin_ref.proj_ref, f32[8,128]{1,0:T(8,128)S(1)} %broadcast_in_dim.10.freq_ref, ...), custom_call_target="tpu_custom_call" | custom-call | flops 603979776 | bytes 8388608 | tf_op jit(solution)/shard_map/exchange/pallas_call | solution.py:833
  101.8 30.9 %finish.1 = bf16[768,512]{1,0:T(8,128)(2,1)S(1)} custom-call(bf16[768,512]{1,0:T(8,128)(2,1)S(1)} %get-tuple-element.22.window_ref, bf16[2048,1280]{1,0:T(8,128)(2,1)S(1)} %bitcast.16, bf16[768,768]{1,0:T(8,128)(2,1)S(1)} %get-tuple-element.23.conv_ref, f32[768,32]{1,0:T(8,128)S(1)} %get-tuple-element.24.col_ref, ...), custom_call_target="tpu_custom_call" | custom-call | flops 3221225472 | bytes 8388608 | tf_op jit(solution)/shard_map/finish/pallas_call | solution.py:962
  132.7 0.9 copy.22
  133.6 0.6 copy.23
  (21 shorter events, 0.0 us)
Async XLA Ops:
  1.3 1.9 %copy-start = (bf16[768,2048]{1,0:T(8,128)(2,1)S(1)}, bf16[768,2048]{1,0:T(8,128)(2,1)}, u32[]{:S(2)}) copy-start(bf16[768,2048]{1,0:T(8,128)(2,1)} %tok_ref.1) | copy-start | bytes 9437188
  3.2 0.8 copy-start.2
  4.0 0.8 copy-start.3
  4.7 0.8 copy-start.4
  5.5 0.8 copy-start.5
  6.2 0.8 copy-start.6
  7.0 0.7 copy-start.7
  7.7 0.7 copy-start.8
  8.4 0.7 copy-start.9
  9.1 0.7 copy-start.10
  9.8 0.7 copy-start.12
  65.6 9.0 %copy-start.1 = (f32[2,768,8]{1,2,0:T(8,128)S(1)}, f32[2,768,8]{1,2,0:T(8,128)}, u32[]{:S(2)}) copy-start(f32[2,768,8]{1,2,0:T(8,128)} %param.28) | copy-start | bytes 147460
  65.6 9.0 %copy-start.11 = (bf16[5,512]{1,0:T(8,128)(2,1)S(1)}, bf16[5,512]{1,0:T(8,128)(2,1)}, u32[]{:S(2)}) copy-start(bf16[5,512]{1,0:T(8,128)(2,1)} %taps_x_ref.1) | copy-start | bytes 15364
  65.6 9.0 %copy-start.13 = (bf16[5,1,128]{2,0,1:T(8,128)(2,1)S(1)}, bf16[5,1,128]{2,0,1:T(8,128)(2,1)}, u32[]{:S(2)}) copy-start(bf16[5,1,128]{2,0,1:T(8,128)(2,1)} %param.26) | copy-start | bytes 3844
  65.6 9.0 %copy-start.14 = (bf16[5,1,128]{2,0,1:T(8,128)(2,1)S(1)}, bf16[5,1,128]{2,0,1:T(8,128)(2,1)}, u32[]{:S(2)}) copy-start(bf16[5,1,128]{2,0,1:T(8,128)(2,1)} %param.27) | copy-start | bytes 3844
  74.6 6.8 %copy-start.15 = (f32[8]{0:T(128)S(1)}, f32[8]{0:T(128)}, u32[]{:S(2)}) copy-start(f32[8]{0:T(128)} %sink_ref.1) | copy-start | bytes 100
  74.6 27.1 %copy-start.16 = (bf16[512]{0:T(512)(128)(2,1)S(1)}, bf16[512]{0:T(512)(128)(2,1)}, u32[]{:S(2)}) copy-start(bf16[512]{0:T(512)(128)(2,1)} %param.29) | copy-start | bytes 3076

commit v4 on v3

--- a/solution.py
+++ b/solution.py
@@ -2,6 +2,7 @@
 
 import jax
 import jax.numpy as jnp
+import numpy as np
 from jax import lax
 from jax.experimental import pallas as pl
 from jax.experimental.pallas import tpu as pltpu
@@ -48,6 +49,11 @@
     return dot(joined, matrix)
 
 
+def as_row(ref):
+    wide = ref[...].astype(F32)
+    return jnp.concatenate([wide[i : i + 1, :] for i in range(wide.shape[0])], axis=1)
+
+
 def spread_matrix():
     shape = (2 * HEADS, 2 * HEADS * HEAD_DIM)
     rows = lax.broadcasted_iota(jnp.int32, shape, 0)
@@ -55,46 +61,7 @@
     return jnp.where((first >= 0) & (first < HEAD_DIM), 1.0, 0.0).astype(BF16)
 
 
-def project_kernel(normed, a_ref, b_ref, out_ref, step_ref):
-    count = step_ref.shape[0]
-    tile = 256
-
-    def column(j, carry):
-        cols = pl.ds(pl.multiple_of(j * tile, tile), tile)
-        out_ref[:, cols] = dot(normed[...], a_ref[:, cols]).astype(BF16)
-        return carry
-
-    tiles = WIDTH_A // tile
-    lax.fori_loop(0, tiles, column, 0)
-    step_ref[...] = dot(normed[0:count, :], a_ref[:, tiles * tile : WIDTH_A])
-    out_ref[:, tiles * tile : (tiles + 1) * tile] = dot(
-        normed[...], b_ref[:, WIDTH_B - tile : WIDTH_B]
-    ).astype(BF16)
-
-
-def project(normed, count, a, b):
-    rows, width = normed.shape
-    columns = 2048
-    vmem = pl.BlockSpec(memory_space=pltpu.VMEM)
-    return pl.pallas_call(
-        project_kernel,
-        in_specs=[vmem] * 3,
-        out_specs=[vmem] * 2,
-        out_shape=[
-            jax.ShapeDtypeStruct((rows, columns), BF16),
-            jax.ShapeDtypeStruct((count, 128), F32),
-        ],
-        compiler_params=pltpu.CompilerParams(vmem_limit_bytes=12 << 20),
-        cost_estimate=pl.CostEstimate(
-            flops=2 * rows * width * (columns + 128),
-            bytes_accessed=2 * (rows * width + width * columns + rows * columns),
-            transcendentals=0,
-        ),
-        name="project",
-    )(normed, a, b)
-
-
-def conv_state_kernel(
+def conv_state(
     cin_ref, taps_x_ref, taps_b_ref, taps_c_ref, step_ref, rate_ref,
     conv_ref, col_ref, row_ref, piece_ref, etot_ref, msg_ref, win, near,
 ):
@@ -172,55 +139,12 @@
             msg_ref[e, pair, STATE:MSG, :] = tail[:, e * channels + pair * 128 : e * channels + pair * 128 + 128]
 
 
-def conv_state(proj, taps, step_raw, rate):
-    count = step_raw.shape[0]
-    width = sum(t.shape[1] for t in taps)
-    blocks = count // BLOCK
-    channels = HEADS * HEAD_DIM
-    whole = lambda shape: pl.BlockSpec(shape, lambda i: (0,) * len(shape))
-    return pl.pallas_call(
-        conv_state_kernel,
-        grid=(1,),
-        in_specs=[
-            pl.BlockSpec((proj.shape[0], width), lambda i: (0, 0)),
-            *(whole(t.shape) for t in taps),
-            whole(step_raw.shape),
-            whole(rate.shape),
-        ],
-        out_specs=[
-            whole((count, width)),
-            whole((count, 4 * HEADS)),
-            whole((blocks, 4 * HEADS, BLOCK)),
-            whole((blocks, STATE, 2 * channels)),
-            whole((blocks, 8, 2 * channels)),
-            whole((2, channels // 128, MSG, 128)),
-        ],
-        out_shape=[
-            jax.ShapeDtypeStruct((count, width), BF16),
-            jax.ShapeDtypeStruct((count, 4 * HEADS), F32),
-            jax.ShapeDtypeStruct((blocks, 4 * HEADS, BLOCK), F32),
-            jax.ShapeDtypeStruct((blocks, STATE, 2 * channels), F32),
-            jax.ShapeDtypeStruct((blocks, 8, 2 * channels), F32),
-            jax.ShapeDtypeStruct((2, channels // 128, MSG, 128), BF16),
-        ],
-        scratch_shapes=[
-            pltpu.VMEM((count + 2 * HALO, width), F32),
-            pltpu.VMEM((BLOCK + 2 * HALO, width), F32),
-        ],
-        compiler_params=pltpu.CompilerParams(vmem_limit_bytes=18 << 20),
-        cost_estimate=pl.CostEstimate(
-            flops=2 * count * STATE * 2 * channels, bytes_accessed=12 << 20, transcendentals=0
-        ),
-        name="conv_state",
-    )(proj, *taps, step_raw, rate)
-
-
-def mixer(conv_ref, col_ref, row_ref, piece_ref, etot_ref, in_ref, proj_ref, gain_ref, out_ref, held):
+def mixer(conv_ref, col_ref, row_ref, piece_ref, etot_ref, in_ref, gate_ref, gain_ref, out_ref, held):
     count = conv_ref.shape[0]
     blocks = count // BLOCK
     channels = HEADS * HEAD_DIM
     spread_m = spread_matrix()
-    gain = gain_ref[...].astype(F32)
+    gain = as_row(gain_ref)
     for e in range(2):
         state = jnp.concatenate(
             [in_ref[e, p].astype(F32) for p in range(channels // 128)], axis=1
@@ -266,7 +190,7 @@
             )
             parts.append(dot(jnp.concatenate(weights, axis=1), stacked))
         y = jnp.concatenate(parts, axis=1) + far[:, 0:channels] + far[:, channels:]
-        gate = proj_ref[rows, GATE_AT : GATE_AT + channels].astype(F32)
+        gate = gate_ref[rows, :].astype(F32)
         y = y * (gate * jax.nn.sigmoid(gate))
         y = y * lax.rsqrt(jnp.mean(y * y, axis=1, keepdims=True) + EPS)
         out_ref[rows, :] = (y * gain).astype(BF16)
@@ -275,7 +199,7 @@
 
 
 def attention(
-    count, proj_ref, before_ref, after_ref, freq_ref, sink_ref,
+    count, q_ref, kv_ref, before_ref, after_ref, freq_ref, sink_ref,
     out_ref, log_ref, keys, values, by_row, by_col,
 ):
     blocks = count // BLOCK
@@ -320,7 +244,7 @@
     def own_keys():
         def fill(i, carry):
             rows = pl.ds(pl.multiple_of(i * BLOCK, BLOCK), BLOCK)
-            store(proj_ref[rows, KV_AT : KV_AT + 256], i + 1)
+            store(kv_ref[rows, :], i + 1)
             return carry
 
         lax.fori_loop(0, blocks, fill, 0)
@@ -346,7 +270,7 @@
         for pair in range(HEADS // 2):
             group = pair // 2
             lanes = slice(pair * 128, pair * 128 + 128)
-            q = (turn(proj_ref[rows, Q_AT + pair * 128 : Q_AT + pair * 128 + 128], table).astype(F32) * HEAD_DIM ** (-0.5)).astype(BF16)
+            q = (turn(q_ref[rows, lanes], table).astype(F32) * HEAD_DIM ** (-0.5)).astype(BF16)
             zero = jnp.zeros_like(q)
             both = jnp.concatenate(
                 [jnp.where(first_half, q, zero), jnp.where(first_half, zero, q)], axis=0
@@ -452,8 +376,8 @@
     return first, order, end
 
 
-def gather_kernel(
-    lengths, tok_ref, gain_ref, step_ref, value_ref, inflow_ref, readout_ref, key_ref, vector_ref,
+def gather(
+    lengths, small_copies, enter, tok_ref, gain_ref, step_ref, value_ref, inflow_ref, readout_ref, key_ref, vector_ref,
     gate_ref, query_ref, state_ref, window_ref,
     a_ref, b_ref, normed, before, after, held, send_sem, recv_sem, core_send, core_recv, edge_sem,
     own_sem,
@@ -482,12 +406,6 @@
             SP[1]: lax.rem(index // 2, length_y),
             SP[2]: lax.rem(index, 2),
         }
-
-    peers = [{SP[2]: other}] + [towards(a, s) for a in ("z", "y") for s in (1, -1)]
-    peers += [device_at(flat + 1), device_at(flat - 1)]
-    barrier = pltpu.get_barrier_semaphore()
-    for peer in peers:
-        pl.semaphore_signal(barrier, inc=1, device_id=peer, device_id_type=mesh_id)
 
     count_rows = tok_ref.shape[0]
     half = query_ref.shape[1] // 2
@@ -509,6 +427,7 @@
     moves = [pltpu.make_async_copy(*move, own_sem.at[i]) for i, move in enumerate(moves)]
     for move in moves:
         move.start()
+    small_copies()
     step = step_ref[...].astype(F32)
     rows, cols = step.shape
     step = jnp.concatenate([step, jnp.zeros((rows, 128 - cols), F32)], axis=1)
@@ -516,7 +435,7 @@
     a_ref[z, y, c, :, WIDTH_A - 128 : WIDTH_A] = step.T[0:cols, :].astype(BF16)
     for move in moves[:-1]:
         move.wait()
-    pl.semaphore_wait(barrier, len(peers))
+    enter()
 
     sends = transfers(length_z, length_y)
     number = {s["name"]: i for i, s in enumerate(sends)}
@@ -545,7 +464,7 @@
             device_id=device_at(index), device_id_type=mesh_id,
         ))
 
-    gain = gain_ref[...].astype(F32)
+    gain = as_row(gain_ref)
 
     def norm(value):
         wide = value.astype(F32)
@@ -629,52 +548,21 @@
     ).astype(BF16)
 
 
-def gather(length_z, length_y, tokens, gain, step, *shards):
-    sends = transfers(length_z, length_y)
-    groups = length_z + length_y
-    vmem = pl.BlockSpec(memory_space=pltpu.VMEM)
-    hbm = pl.BlockSpec(memory_space=pl.ANY)
-    dma = pltpu.SemaphoreType.DMA
-    lead = (length_z, length_y, 2, 32)
-    rows, width = tokens.shape
-    edge = pltpu.VMEM((HALO, width), BF16)
-    a, b, normed = pl.pallas_call(
-        functools.partial(gather_kernel, (length_z, length_y)),
-        in_specs=[hbm, vmem, vmem] + [hbm] * len(shards),
-        out_specs=[vmem] * 3,
-        out_shape=[
-            jax.ShapeDtypeStruct((*lead, WIDTH_A), BF16),
-            jax.ShapeDtypeStruct((*lead, WIDTH_B), BF16),
-            jax.ShapeDtypeStruct((rows + 2 * HALO, width), BF16),
-        ],
-        scratch_shapes=[
-            edge, edge, pltpu.VMEM((rows, width), BF16),
-            dma((len(sends),)), dma((len(sends),)), dma((groups,)), dma((groups,)), dma((2, 2)),
-            dma((len(shards) + 2,)),
-        ],
-        compiler_params=pltpu.CompilerParams(
-            collective_id=2, has_side_effects=True, vmem_limit_bytes=28 << 20
-        ),
-        cost_estimate=pl.CostEstimate(flops=1 << 24, bytes_accessed=24 << 20, transcendentals=0),
-        name="gather",
-    )(tokens, gain, step, *shards)
-    return a.reshape(-1, WIDTH_A), b.reshape(-1, WIDTH_B), normed
-
-
-def exchange_kernel(
-    rows, msg_ref, proj_ref, freq_ref, sink_ref, out_ref, window_ref, log_ref,
-    kv_before_ref, kv_after_ref, keys, values, by_row, by_col, part, turned, by_y, summed, by_z, back, arrived, nxt, final, carry,
+def middle(
+    normed, a_ref, b_ref, taps_x_ref, taps_b_ref, taps_c_ref, rate_ref, freq_ref, sink_ref,
+    out_ref, window_ref, log_ref, gate_ref, conv_ref, col_ref, row_ref, piece_ref, etot_ref,
+    cin_ref, kv_ref, q_ref, step_ref, win, near, msg_ref,
+    kv_before_ref, kv_after_ref, keys, values, by_row, by_col, part, turned, by_y, summed, by_z,
+    back, arrived, nxt, final, carry,
     part_sem, y_sem, z_sem, back_sem, final_sem, kv_sem,
 ):
+    rows = kv_ref.shape[0]
     z, y, c = (lax.axis_index(a) for a in SP)
     length_z, length_y = lax.axis_size(SP[0]), lax.axis_size(SP[1])
     forward = c == 0
     other = 1 - c
     order_z = jnp.where(forward, z, length_z - 1 - z)
     mesh_id = pl.DeviceIdType.MESH
-    peers = [{SP[2]: other}]
-    peers += [{SP[1]: lax.rem(y + k, length_y)} for k in range(1, length_y)]
-    peers += [{SP[0]: lax.rem(z + k, length_z)} for k in range(1, length_z)]
     flat = (z * length_y + y) * 2 + c
     count = length_z * length_y * 2
 
@@ -686,11 +574,18 @@
             SP[2]: lax.rem(index, 2),
         }
 
-    peers += [device_at(flat + 1), device_at(flat - 1)]
-    barrier = pltpu.get_barrier_semaphore()
-    for peer in peers:
-        pl.semaphore_signal(barrier, inc=1, device_id=peer, device_id_type=mesh_id)
-    pl.semaphore_wait(barrier, len(peers))
+    def project(dst, count, tiles, source, first):
+        tile = 256
+
+        def column(j, carry_over):
+            cols = pl.ds(pl.multiple_of(j * tile, tile), tile)
+            from_cols = pl.ds(pl.multiple_of(first + j * tile, 128), tile)
+            dst[:, cols] = dot(normed[0:count, :], source[:, from_cols]).astype(BF16)
+            return carry_over
+
+        lax.fori_loop(0, tiles, column, 0)
+
+    project(kv_ref, rows, 1, a_ref, KV_AT)
 
     def send(src, dst, sems, peer):
         copy = pltpu.make_async_remote_copy(
@@ -715,17 +610,22 @@
         ref[(*at, slice(STATE, MSG), slice(None))] = tail.astype(BF16)
 
     pairs = msg_ref.shape[1]
-    copy = send(msg_ref.at[other], part, part_sem, {SP[2]: other})
-    kv_cols = pl.ds(KV_AT, kv_before_ref.shape[1])
     kv_copies = [
         send(
-            proj_ref.at[pl.ds(rows - WINDOW, WINDOW), kv_cols], kv_before_ref, kv_sem.at[0],
+            kv_ref.at[pl.ds(rows - WINDOW, WINDOW)], kv_before_ref, kv_sem.at[0],
             device_at(flat + 1),
         ),
-        send(proj_ref.at[pl.ds(0, WINDOW), kv_cols], kv_after_ref, kv_sem.at[1], device_at(flat - 1)),
+        send(kv_ref.at[pl.ds(0, WINDOW)], kv_after_ref, kv_sem.at[1], device_at(flat - 1)),
     ]
+    project(cin_ref, rows + 2 * HALO, 3, a_ref, 0)
+    step_ref[...] = dot(normed[0:rows, :], a_ref[:, WIDTH_A - 128 : WIDTH_A])
+    conv_state(
+        cin_ref, taps_x_ref, taps_b_ref, taps_c_ref, step_ref, rate_ref,
+        conv_ref, col_ref, row_ref, piece_ref, etot_ref, msg_ref, win, near,
+    )
+    copy = send(msg_ref.at[other], part, part_sem, {SP[2]: other})
     own_keys, edge_keys, attend = attention(
-        rows, proj_ref, kv_before_ref, kv_after_ref, freq_ref, sink_ref,
+        rows, q_ref, kv_ref, kv_before_ref, kv_after_ref, freq_ref, sink_ref,
         window_ref, log_ref, keys, values, by_row, by_col,
     )
 
@@ -752,7 +652,8 @@
         to = lax.rem(y + k, length_y)
         copies.append(send(turned.at[to], by_y.at[k], y_sem.at[k], {SP[1]: to}))
     by_y[0] = turned[y]
-    attend_blocks(1, 2)
+    project(q_ref.at[:, pl.ds(0, 256)], rows, 1, a_ref, WIDTH_A - 384)
+    project(q_ref.at[:, pl.ds(256, 256)], rows, 1, b_ref, WIDTH_B - 256)
     for copy in copies:
         copy.wait()
     before = []
@@ -773,7 +674,7 @@
             send(summed, by_z.at[k], z_sem.at[k], {SP[0]: to})
 
     carry[...] = jnp.zeros_like(carry)
-    attend_blocks(2, blocks - 1)
+    attend_blocks(1, blocks - 1)
     for distance in reversed(range(1, length_z)):
         slot = jnp.where(forward, distance, length_z - distance)
 
@@ -819,58 +720,13 @@
         ).astype(BF16)
     copy = send(nxt, final, final_sem, {SP[2]: other})
     attend(blocks - 1)
+    project(gate_ref, rows, 2, a_ref, GATE_AT)
     copy.wait()
     out_ref[other] = final[...]
 
 
-def exchange(message, proj, rows, freqs, sinks, length_z, length_y):
-    pairs = message.shape[1]
-    channels = HEADS * HEAD_DIM
-    tile = (STATE, 128)
-    full = (MSG, 128)
-    dma = pltpu.SemaphoreType.DMA
-    vmem = pl.BlockSpec(memory_space=pltpu.VMEM)
-    return pl.pallas_call(
-        functools.partial(exchange_kernel, rows),
-        in_specs=[vmem, vmem, vmem, pl.BlockSpec(memory_space=pltpu.SMEM)],
-        out_specs=[vmem] * 3,
-        out_shape=[
-            jax.ShapeDtypeStruct((2, pairs, *tile), BF16),
-            jax.ShapeDtypeStruct((rows, channels), BF16),
-            jax.ShapeDtypeStruct((HEADS, rows), F32),
-        ],
-        scratch_shapes=[
-            pltpu.VMEM((WINDOW, 256), BF16),
-            pltpu.VMEM((WINDOW, 256), BF16),
-            pltpu.VMEM((2, rows + 2 * BLOCK, 128), BF16),
-            pltpu.VMEM((128, rows + 2 * BLOCK), BF16),
-            pltpu.VMEM((2, (rows + 2 * WINDOW) // GRID_W, 128), F32),
-            pltpu.VMEM((2, GRID_W, 128), F32),
-            pltpu.VMEM((pairs, *full), BF16),
-            pltpu.VMEM((pairs, *full), BF16),
-            pltpu.VMEM((length_y, *full), BF16),
-            pltpu.VMEM(full, BF16),
-            pltpu.VMEM((length_z, *full), BF16),
-            pltpu.VMEM((length_y, *tile), BF16),
-            pltpu.VMEM((length_y, *tile), BF16),
-            pltpu.VMEM((pairs, *tile), BF16),
-            pltpu.VMEM((pairs, *tile), BF16),
-            pltpu.VMEM(tile, F32),
-            dma((2,)), dma((length_y, 2)), dma((length_z, 2)), dma((length_y, 2)), dma((2,)),
-            dma((2, 2)),
-        ],
-        compiler_params=pltpu.CompilerParams(
-            collective_id=1, has_side_effects=True, vmem_limit_bytes=16 << 20
-        ),
-        cost_estimate=pl.CostEstimate(
-            flops=4 * rows * 3 * BLOCK * channels, bytes_accessed=8 << 20, transcendentals=0
-        ),
-        name="exchange",
-    )(message, proj, freqs, sinks)
-
-
-def finish_kernel(
-    window_ref, w_ref, conv_ref, col_ref, row_ref, piece_ref, etot_ref, in_ref, proj_ref, gain_ref,
+def finish(
+    window_ref, w_ref, conv_ref, col_ref, row_ref, piece_ref, etot_ref, in_ref, gate_ref, gain_ref,
     out_ref, *refs
 ):
     state_ref, held, far_out, far_in, near_out, near_in, far_sem, near_sem = refs
@@ -880,7 +736,7 @@
     sides = (1, -1)
     count, channels = state_ref.shape
     mix = mixer(
-        conv_ref, col_ref, row_ref, piece_ref, etot_ref, in_ref, proj_ref, gain_ref, state_ref, held
+        conv_ref, col_ref, row_ref, piece_ref, etot_ref, in_ref, gate_ref, gain_ref, state_ref, held
     )
     width = w_ref.shape[0] // n
     half = width // 2
@@ -890,11 +746,6 @@
     def at(step):
         return lax.rem(me + step + n, n)
 
-    barrier = pltpu.get_barrier_semaphore()
-    for side in sides:
-        pl.semaphore_signal(barrier, inc=1, device_id={"tp": at(side)}, device_id_type=mesh_id)
-    pl.semaphore_wait(barrier, 2)
-
     def terms(rows, to):
         outs = pl.ds(pl.multiple_of(to * width, width), width)
         return dot(state_ref[rows, :], w_ref[outs, 0:channels], ((1,), (1,))) + dot(
@@ -915,13 +766,18 @@
 
     def send_far(i, carry):
         rows = pl.ds(pl.multiple_of(i * chunk, chunk), chunk)
-        mix(i)
         value = terms(rows, at(2)).astype(BF16)
         for k in range(2):
             far_out[k, i] = value[:, k * half : (k + 1) * half]
             far_copy(i, k).start()
+
+        @pl.when(i + 1 < chunks)
+        def _():
+            mix(i + 1)
+
         return carry
 
+    mix(0)
     lax.fori_loop(0, chunks, send_far, 0)
 
     def send_near(i, carry):
@@ -952,35 +808,148 @@
     lax.fori_loop(0, chunks, collect, 0)
 
 
-def finish(window, weights, mixed_from, n):
-    count, channels = window.shape
-    width = weights.shape[0] // n
-    chunk = BLOCK
-    chunks = count // chunk
-    vmem = pl.BlockSpec(memory_space=pltpu.VMEM)
+def layer_kernel(
+    lengths, tok_ref, *refs
+):
+    length_z, length_y = lengths
+    smalls_hbm, refs = refs[:8], refs[8:]
+    shards, refs = refs[:9], refs[9:]
+    sink_ref, mixed_ref, log_ref = refs[:3]
+    smalls, refs = refs[3:11], refs[11:]
+    small_sem, a_ref, b_ref, normed = refs[:4]
+    gather_refs, refs = refs[4:13], refs[13:]
+    incoming, window_ref, gate_ref = refs[:3]
+    conv_refs, refs = refs[3:8], refs[8:]
+    middle_refs, finish_refs = refs[:29], refs[29:]
+    gain_ref, step_ref, taps_x, taps_b, taps_c, rate_ref, freq_ref, group_gain_ref = smalls
+    z, y, c = (lax.axis_index(a) for a in SP)
+    t = lax.axis_index("tp")
+    n = lax.axis_size("tp")
+    flat = (z * length_y + y) * 2 + c
+    count = length_z * length_y * 2
+    peers = [{SP[2]: 1 - c}]
+    peers += [{SP[1]: lax.rem(y + k, length_y)} for k in range(1, length_y)]
+    peers += [{SP[0]: lax.rem(z + k, length_z)} for k in range(1, length_z)]
+    peers += [{"tp": lax.rem(t + k, n)} for k in (1, n - 1)]
+    for shift in (1, count - 1):
+        index = lax.rem(flat + shift, count)
+        peers.append({
+            SP[0]: index // (2 * length_y),
+            SP[1]: lax.rem(index // 2, length_y),
+            SP[2]: lax.rem(index, 2),
+        })
+    barrier = pltpu.get_barrier_semaphore()
+    for peer in peers:
+        pl.semaphore_signal(barrier, inc=1, device_id=peer, device_id_type=pl.DeviceIdType.MESH)
+    copies = [
+        pltpu.make_async_copy(src, dst, small_sem.at[i])
+        for i, (src, dst) in enumerate(zip(smalls_hbm, smalls))
+    ]
+    for copy in copies:
+        copy.start()
+
+    def small_copies():
+        for copy in copies:
+            copy.wait()
+
+    def enter():
+        pl.semaphore_wait(barrier, len(peers))
+
+    gather(
+        lengths, small_copies, enter, tok_ref, gain_ref, step_ref, *shards,
+        a_ref, b_ref, normed, *gather_refs,
+    )
+    flat_a = a_ref.reshape(length_z * length_y * 64, WIDTH_A)
+    flat_b = b_ref.reshape(length_z * length_y * 64, WIDTH_B)
+    middle(
+        normed, flat_a, flat_b, taps_x, taps_b, taps_c, rate_ref, freq_ref, sink_ref,
+        incoming, window_ref, log_ref, gate_ref, *conv_refs, *middle_refs,
+    )
+    finish(
+        window_ref, flat_b, *conv_refs, incoming, gate_ref, group_gain_ref, mixed_ref, *finish_refs
+    )
+
+
+def layer(length_z, length_y, n, tokens, smalls, shards, sinks):
+    rows, model = tokens.shape
+    channels = HEADS * HEAD_DIM
+    width = channels + 2 * STATE
+    blocks = rows // BLOCK
+    pairs = channels // 128
+    tile = (STATE, 128)
+    full = (MSG, 128)
+    lead = (length_z, length_y, 2, 32)
+    sends = len(transfers(length_z, length_y))
+    groups = length_z + length_y
+    part = model // n
     dma = pltpu.SemaphoreType.DMA
+    vmem = pltpu.VMEM
+    hbm = pl.BlockSpec(memory_space=pl.ANY)
+    scratch = [
+        *(vmem(s.shape, s.dtype) for s in smalls),
+        dma((len(smalls),)),
+        vmem((*lead, WIDTH_A), BF16),
+        vmem((*lead, WIDTH_B), BF16),
+        vmem((rows + 2 * HALO, model), BF16),
+        vmem((HALO, model), BF16), vmem((HALO, model), BF16), vmem((rows, model), BF16),
+        dma((sends,)), dma((sends,)), dma((groups,)), dma((groups,)), dma((2, 2)),
+        dma((len(shards) + 2,)),
+        vmem((2, pairs, *tile), BF16),
+        vmem((rows, channels), BF16),
+        vmem((rows, channels), BF16),
+        vmem((rows, width), BF16),
+        vmem((rows, 4 * HEADS), F32),
+        vmem((blocks, 4 * HEADS, BLOCK), F32),
+        vmem((blocks, STATE, 2 * channels), F32),
+        vmem((blocks, 8, 2 * channels), F32),
+        vmem((rows + 2 * HALO, width), BF16),
+        vmem((rows, 256), BF16),
+        vmem((rows, channels), BF16),
+        vmem((rows, 128), F32),
+        vmem((rows + 2 * HALO, width), F32),
+        vmem((BLOCK + 2 * HALO, width), F32),
+        vmem((2, pairs, *full), BF16),
+        vmem((WINDOW, 256), BF16),
+        vmem((WINDOW, 256), BF16),
+        vmem((2, rows + 2 * BLOCK, 128), BF16),
+        vmem((128, rows + 2 * BLOCK), BF16),
+        vmem((2, (rows + 2 * WINDOW) // GRID_W, 128), F32),
+        vmem((2, GRID_W, 128), F32),
+        vmem((pairs, *full), BF16),
+        vmem((pairs, *full), BF16),
+        vmem((length_y, *full), BF16),
+        vmem(full, BF16),
+        vmem((length_z, *full), BF16),
+        vmem((length_y, *tile), BF16),
+        vmem((length_y, *tile), BF16),
+        vmem((pairs, *tile), BF16),
+        vmem((pairs, *tile), BF16),
+        vmem(tile, F32),
+        dma((2,)), dma((length_y, 2)), dma((length_z, 2)), dma((length_y, 2)), dma((2,)),
+        dma((2, 2)),
+        vmem((rows, channels), BF16),
+        vmem((blocks, STATE, 2 * channels), BF16),
+        vmem((2, blocks, BLOCK, part // 2), BF16),
+        vmem((2, blocks, BLOCK, part // 2), BF16),
+        vmem((2, blocks, BLOCK, part), BF16),
+        vmem((2, blocks, BLOCK, part), BF16),
+        dma((2, blocks, 2)), dma((2, blocks, 2)),
+    ]
     return pl.pallas_call(
-        finish_kernel,
-        in_specs=[vmem] * (2 + len(mixed_from)),
-        out_specs=vmem,
-        out_shape=jax.ShapeDtypeStruct((count, width), BF16),
-        scratch_shapes=[
-            pltpu.VMEM((count, channels), BF16),
-            pltpu.VMEM((chunks, STATE, 2 * channels), BF16),
-            pltpu.VMEM((2, chunks, chunk, width // 2), BF16),
-            pltpu.VMEM((2, chunks, chunk, width // 2), BF16),
-            pltpu.VMEM((2, chunks, chunk, width), BF16),
-            pltpu.VMEM((2, chunks, chunk, width), BF16),
-            dma((2, chunks, 2)), dma((2, chunks, 2)),
+        functools.partial(layer_kernel, (length_z, length_y)),
+        in_specs=[hbm] * (1 + len(smalls) + len(shards)) + [pl.BlockSpec(memory_space=pltpu.SMEM)],
+        out_specs=[pl.BlockSpec(memory_space=pltpu.VMEM)] * 2,
+        out_shape=[
+            jax.ShapeDtypeStruct((rows, part), BF16),
+            jax.ShapeDtypeStruct((HEADS, rows), F32),
         ],
+        scratch_shapes=scratch,
         compiler_params=pltpu.CompilerParams(
-            collective_id=3, has_side_effects=True, vmem_limit_bytes=28 << 20
+            collective_id=1, has_side_effects=True, vmem_limit_bytes=65_800_000
         ),
-        cost_estimate=pl.CostEstimate(
-            flops=4 * count * channels * width * n, bytes_accessed=8 << 20, transcendentals=0
-        ),
-        name="finish",
-    )(window, weights, *mixed_from)
+        cost_estimate=pl.CostEstimate(flops=1 << 33, bytes_accessed=24 << 20, transcendentals=0),
+        name="layer",
+    )(tokens, *smalls, *shards, sinks)
 
 
 def flatten_rows(weight):
@@ -995,24 +964,23 @@
     count = tokens.shape[0]
     length_z, length_y = lax.axis_size(SP[0]), lax.axis_size(SP[1])
     quarter = HEAD_DIM // 4
-    freqs = ROPE_BASE ** (-(jnp.arange(128) % quarter).astype(F32) / quarter)
-    freqs = jnp.broadcast_to(freqs, (8, 128))
-    step_turned = step_weight.transpose(1, 2, 0).reshape(2 * HEADS, -1)
-    a, b, normed = gather(
-        length_z, length_y, tokens, input_gain[None], step_turned, value_weight,
-        flatten_rows(inflow_weight), flatten_rows(readout_weight), key_weight, vector_weight,
-        gate_weight, query_weight, state_out.T, window_out.T,
+    powers = (np.arange(128) % quarter).astype(np.float32) / np.float32(quarter)
+    freqs = np.broadcast_to(np.float32(ROPE_BASE) ** -powers, (8, 128)).astype(np.float32)
+    freqs = jnp.asarray(freqs)
+    smalls = (
+        input_gain.reshape(-1, 128),
+        step_weight.transpose(1, 2, 0).reshape(2 * HEADS, -1),
+        conv_values, flatten_rows(conv_inflow), flatten_rows(conv_readout),
+        log_rate.transpose(0, 2, 1).reshape(2 * HEADS, count),
+        freqs,
+        group_gain.reshape(-1, 128),
     )
-    proj, step_raw = project(normed, count, a, b)
-    taps = (conv_values, flatten_rows(conv_inflow), flatten_rows(conv_readout))
-    rate = log_rate.transpose(0, 2, 1).reshape(2 * HEADS, count)
-    conv, col, row, piece, etot, message = conv_state(proj, taps, step_raw, rate)
-    incoming, window, logs = exchange(
-        message, proj, count, freqs, sink_logit, length_z, length_y
+    shards_here = (
+        value_weight, flatten_rows(inflow_weight), flatten_rows(readout_weight), key_weight,
+        vector_weight, gate_weight, query_weight, state_out.T, window_out.T,
     )
-    mixed = finish(
-        window, b, (conv, col, row, piece, etot, incoming, proj, group_gain[None]),
-        lax.axis_size("tp"),
+    mixed, logs = layer(
+        length_z, length_y, lax.axis_size("tp"), tokens, smalls, shards_here, sink_logit
     )
     return mixed, logs.T
 

time: 135 us -> 123 us (0.911)
  local copies, waits for them, and re-layouts: 11.4 us -> 3.41 us
  Pallas kernels: 122 us -> 119 us
    unnamed x36 -> x2, local copies, waits for them, and re-layouts: 10.7 us -> 3.41 us
    pallas_call x5 -> x1, Pallas kernels: 122 us -> 119 us  [layer(): pl.pallas_call(functools.partial(layer_kernel, (length_z, length_y)), in_...]
where the time goes in v4:
time: 123 us
  Pallas kernels  119 us (97%)
  local copies, waits for them, and re-layouts  3.41 us (3%)
    pallas_call x1, Pallas kernels, layer(): pl.pallas_call(functools.partial(layer_kernel, (length_z, length_y)), in_...  119 us
    unnamed x2, local copies, waits for them, and re-layouts  3.41 us

profile of v4, /device:TPU:1, one launch (start us, length us, event | category | flops | bytes accessed | tf_op | source)
XLA Modules:
  0.0 122.9 jit_solution(10202516965498680877)
XLA Ops:
  0.6 118.8 %layer.1 = (bf16[768,512]{1,0:T(8,128)(2,1)}, f32[8,768]{1,0:T(8,128)}) custom-call(bf16[768,2048]{1,0:T(8,128)(2,1)} %tok_ref.1, bf16[16,128]{1,0:T(8,128)(2,1)} %bitcast.21, bf16[16,32]{1,0:T(8,128)(2,1)} %bitcast.22, bf16[5,512]{1,0:T(8,128)(2,1)} %refs_2_.1, bf16[5,128]{1,0:T(8,128)(2,1)} %bitcast.23, bf16[5,128]{1,0:T(8,128)(2,1)} %bitcast.24, ...), custom_call_target="tpu_custom_call" | custom-call | flops 8589934592 | bytes 25165824 | tf_op jit(solution)/shard_map/layer/pallas_call | solution.py:938
  119.5 2.1 %copy.23 = bf16[768,512]{1,0:T(8,128)(2,1)} copy(bf16[768,512]{1,0:T(8,128)(2,1)} %get-tuple-element.8) | data formatting | bytes 1572864
  121.5 1.3 %copy.24 = f32[768,8]{0,1:T(8,128)} copy(f32[768,8]{0,1:T(8,128)} %bitcast.15) | data formatting | bytes 49152

commit v5 on v4

--- a/solution.py
+++ b/solution.py
@@ -1,4 +1,5 @@
 import functools
+import heapq
 
 import jax
 import jax.numpy as jnp
@@ -23,8 +24,8 @@
 BF16 = jnp.bfloat16
 MSG = STATE + 16
 KV_AT = 768
-GATE_AT = 1024
-Q_AT = 1536
+Q_AT = 1024
+OUT_AT = 512
 
 
 def dot(a, b, dims=((1,), (0,)), precision=None):
@@ -62,7 +63,7 @@
 
 
 def conv_state(
-    cin_ref, taps_x_ref, taps_b_ref, taps_c_ref, step_ref, rate_ref,
+    service, cin_ref, taps_x_ref, taps_b_ref, taps_c_ref, step_ref, rate_ref,
     conv_ref, col_ref, row_ref, piece_ref, etot_ref, msg_ref, win, near,
 ):
     count = cin_ref.shape[0] - 2 * HALO
@@ -85,6 +86,7 @@
         return carry
 
     lax.fori_loop(0, blocks, fill, 0)
+    service(0.5)
 
     def one(i, total):
         start = pl.multiple_of(i * BLOCK, BLOCK)
@@ -116,7 +118,10 @@
         etot_ref[i] = spread(jnp.exp(jnp.broadcast_to(tot, (8, 2 * HEADS))), spread_m, 3)
         return total + tot
 
-    total = lax.fori_loop(0, blocks, one, jnp.zeros((1, 2 * HEADS), F32))
+    total = jnp.zeros((1, 2 * HEADS), F32)
+    for i in range(0, blocks, 2):
+        total = lax.fori_loop(i, i + 2, one, total)
+        service(1.7)
     forward = piece_ref[0, :, 0:channels]
     backward = piece_ref[blocks - 1, :, channels : 2 * channels]
     for i in range(1, blocks):
@@ -293,135 +298,187 @@
 
 
 LINKS = ("z+", "z-", "y+", "y-")
-WIDTH_A = 1920
-WIDTH_B = 1280
-
-
-def ring(kind, link_axis, other_at, length, total, cut):
+EARLY = 1664
+LATE = 1536
+ROUTES = (
+    (("A", 0, 0, 1024, 512, "z"), ("B", 0, 1024, 640, 384, "y")),
+    (("C", 1, 0, 896, 512, "z"), ("D", 1, 896, 640, 384, "y")),
+)
+RATE = 46.6e3
+HOP = 1.9
+
+
+def ring(route, axis, other, length):
+    name, array, column, total, cut, _ = route
     out = []
     for sign in (1, -1):
         previous = None
         for step in range(length // 2):
-            last = step == length // 2 - 1
-            cols = (0, total)
-            if last:
-                cols = (0, cut) if sign == 1 else (cut, total)
-            name = (kind, link_axis, other_at, sign, step)
+            cols = (column, total)
+            if step == length // 2 - 1:
+                cols = (column, cut) if sign == 1 else (column + cut, total - cut)
+            key = (name, axis, other, sign, step)
             out.append(dict(
-                name=name, kind=kind, axis=link_axis, sign=sign,
-                along=-sign * step, other=other_at, cols=cols, after=previous,
+                key=key, route=name, array=array, axis=axis, sign=sign, along=-sign * step,
+                other=other, cols=cols, needs=[previous] if previous else [],
             ))
-            previous = name
+            previous = key
     return out
 
 
-def transfers(length_z, length_y):
-    sends = []
-    for kind, first, length, second, length2, total, cut in (
-        ("A", "z", length_z, "y", length_y, WIDTH_A, 1024),
-        ("B", "y", length_y, "z", length_z, WIDTH_B, 640),
-    ):
-        sends += ring(kind, first, 0, length, total, cut)
+def transfers(routes, lengths):
+    sends, groups = [], {}
+    for route in routes:
+        name, _, _, _, _, first = route
+        second = "y" if first == "z" else "z"
+        length = lengths[first]
+        sends += ring(route, first, 0, length)
         for offset in range(-(length // 2) + 1, length // 2 + 1):
-            sends += ring(kind, second, offset, length2, total, cut)
-    for s in sends:
-        length, first = (length_z, "z") if s["kind"] == "A" else (length_y, "y")
-        s["needs"] = []
-        if s["after"] is not None:
-            s["needs"] = [s["after"]]
-        elif s["axis"] != first and s["other"] != 0:
-            d = s["other"]
-            if abs(d) == length // 2:
-                s["needs"] = [(s["kind"], first, 0, sign, length // 2 - 1) for sign in (1, -1)]
-            else:
-                s["needs"] = [(s["kind"], first, 0, -1 if d > 0 else 1, abs(d) - 1)]
-    return sends
-
-
-def arrival_order(sends):
-    import heapq
-
-    rate, hop = 46.6e3, 1.9
-    free = dict.fromkeys(LINKS, 0.0)
-    left = {s["name"]: len(s["needs"]) for s in sends}
-    followers = {}
-    for s in sends:
-        for need in s["needs"]:
-            followers.setdefault(need, []).append(s)
-    heap, order, first = [], [], []
-
-    def start(s, now):
+            one = ring(route, second, offset, lengths[second])
+            needs = []
+            if offset == length // 2:
+                needs = [(name, first, 0, sign, length // 2 - 1) for sign in (1, -1)]
+            elif offset:
+                needs = [(name, first, 0, -1 if offset > 0 else 1, abs(offset) - 1)]
+            for s in one:
+                s["needs"] = s["needs"] or needs
+            sends += one
+            groups[(name, offset)] = {s["key"] for s in one}
+    return sends, groups
+
+
+class Flow:
+    def __init__(self, number, lengths, arrays, sems):
+        self.routes = ROUTES[number]
+        self.lengths = lengths
+        self.arrays = arrays
+        self.send_sem, self.recv_sem, self.core_send, self.core_recv = sems
+        self.at = dict(zip("zy", (lax.axis_index(SP[0]), lax.axis_index(SP[1]))))
+        self.c = lax.axis_index(SP[2])
+        self.sends, self.groups = transfers(self.routes, lengths)
+        self.number = {s["key"]: i for i, s in enumerate(self.sends)}
+        self.by_key = {s["key"]: s for s in self.sends}
+        self.group_keys = list(self.groups)
+        self.left = {s["key"]: len(s["needs"]) for s in self.sends}
+        self.followers = {}
+        for s in self.sends:
+            for need in s["needs"]:
+                self.followers.setdefault(need, []).append(s)
+        self.first_axis = {route[0]: route[5] for route in self.routes}
+        self.free = dict.fromkeys(LINKS, 0.0)
+        self.heap = []
+        self.clock = 0.0
+        self.started = []
+
+    def wrap(self, axis, shift):
+        length = self.lengths[axis]
+        return lax.rem(self.at[axis] + shift + length, length)
+
+    def rank(self, s):
+        return (s["axis"] != self.first_axis[s["route"]], s["route"])
+
+    def copy_of(self, s, shift):
+        along = s["along"] - shift * s["sign"]
+        place = {s["axis"]: along, "y" if s["axis"] == "z" else "z": s["other"]}
+        ref = self.arrays[s["array"]].at[
+            self.wrap("z", place["z"]), self.wrap("y", place["y"]), self.c, :, pl.ds(*s["cols"])
+        ]
+        i = self.number[s["key"]]
+        to = {SP["zy".index(s["axis"])]: self.wrap(s["axis"], s["sign"])}
+        return pltpu.make_async_remote_copy(
+            src_ref=ref, dst_ref=ref, send_sem=self.send_sem.at[i], recv_sem=self.recv_sem.at[i],
+            device_id=to, device_id_type=pl.DeviceIdType.MESH,
+        )
+
+    def core_copy(self, key, c):
+        name, offset = key
+        i = self.group_keys.index(key)
+        route = [r for r in self.routes if r[0] == name][0]
+        ref = self.arrays[route[1]]
+        cols = pl.ds(route[2], route[3])
+        if route[5] == "z":
+            ref = ref.at[self.wrap("z", offset), :, c, :, cols]
+        else:
+            ref = ref.at[:, self.wrap("y", offset), c, :, cols]
+        return pltpu.make_async_remote_copy(
+            src_ref=ref, dst_ref=ref, send_sem=self.core_send.at[i],
+            recv_sem=self.core_recv.at[i], device_id={SP[2]: 1 - self.c},
+            device_id_type=pl.DeviceIdType.MESH,
+        )
+
+    def launch(self, s):
+        copy = self.copy_of(s, 0)
+        copy.start()
+        self.started.append(copy)
         link = s["axis"] + ("+" if s["sign"] == 1 else "-")
-        size = 32 * 2 * (s["cols"][1] - s["cols"][0])
-        free[link] = max(free[link], now) + size / rate
-        heapq.heappush(heap, (free[link] + hop, len(order), str(s["name"]), s["name"]))
-
-    def rank(s):
-        return (s["axis"] != ("z" if s["kind"] == "A" else "y"), s["kind"] != "A")
-
-    for s in sorted((s for s in sends if not s["needs"]), key=rank):
-        first.append(s)
-        start(s, 0.0)
-    end = 0.0
-    while heap:
-        now, _, _, name = heapq.heappop(heap)
-        ready = []
-        for s in sorted(followers.get(name, []), key=rank):
-            left[s["name"]] -= 1
-            if left[s["name"]] == 0:
-                ready.append(s)
-                start(s, now)
-        order.append((name, ready))
-        end = now
-    return first, order, end
+        self.free[link] = max(self.free[link], self.clock) + 64 * s["cols"][1] / RATE
+        heapq.heappush(self.heap, (self.free[link] + HOP, len(self.started), s["key"]))
+
+    def begin(self):
+        for s in sorted((s for s in self.sends if not s["needs"]), key=self.rank):
+            self.launch(s)
+
+    def handle(self):
+        _, _, key = heapq.heappop(self.heap)
+        self.copy_of(self.by_key[key], 1).wait_recv()
+        for s in sorted(self.followers.get(key, []), key=self.rank):
+            self.left[s["key"]] -= 1
+            if self.left[s["key"]] == 0:
+                self.launch(s)
+        for group, keys in self.groups.items():
+            if key in keys:
+                keys.remove(key)
+                if not keys:
+                    copy = self.core_copy(group, self.c)
+                    copy.start()
+                    self.started.append(copy)
+
+    def service(self, passed):
+        self.clock += passed
+        while self.heap and self.heap[0][0] <= self.clock:
+            self.handle()
+
+    def drain(self):
+        while self.heap:
+            self.clock = max(self.clock, self.heap[0][0])
+            self.handle()
+        for group in self.group_keys:
+            self.core_copy(group, 1 - self.c).wait_recv()
+
+    def finish(self):
+        for copy in self.started:
+            copy.wait_send()
 
 
 def gather(
-    lengths, small_copies, enter, tok_ref, gain_ref, step_ref, value_ref, inflow_ref, readout_ref, key_ref, vector_ref,
-    gate_ref, query_ref, state_ref, window_ref,
-    a_ref, b_ref, normed, before, after, held, send_sem, recv_sem, core_send, core_recv, edge_sem,
-    own_sem,
+    early, late, small_copies, enter, tok_ref, gain_ref, step_ref, value_ref, inflow_ref,
+    readout_ref, key_ref, vector_ref, gate_ref, query_ref, state_ref, window_ref,
+    normed, before, after, held, edge_sem, own_sem,
 ):
-    length_z, length_y = lengths
     z, y, c = (lax.axis_index(a) for a in SP)
-    other = 1 - c
-    mesh_id = pl.DeviceIdType.MESH
-
-    def wrap(value, length):
-        return lax.rem(value + length, length)
-
-    steps = {"z": (SP[0], z, length_z), "y": (SP[1], y, length_y)}
-
-    def towards(axis, sign):
-        name, at, length = steps[axis]
-        return {name: wrap(at + sign, length)}
-
+    length_z, length_y = early.lengths["z"], early.lengths["y"]
     flat = (z * length_y + y) * 2 + c
     count = length_z * length_y * 2
+    count_rows = tok_ref.shape[0]
+    a_ref, b_ref = early.arrays
 
     def device_at(index):
-        index = wrap(index, count)
+        index = lax.rem(index + count, count)
         return {
             SP[0]: index // (2 * length_y),
             SP[1]: lax.rem(index // 2, length_y),
             SP[2]: lax.rem(index, 2),
         }
 
-    count_rows = tok_ref.shape[0]
-    half = query_ref.shape[1] // 2
     moves = []
     for array, refs in (
-        (a_ref, (value_ref, inflow_ref, readout_ref, key_ref, vector_ref, gate_ref, query_ref)),
-        (b_ref, (state_ref, window_ref, query_ref)),
+        (a_ref, (value_ref, inflow_ref, readout_ref, key_ref, vector_ref, query_ref)),
+        (b_ref, (gate_ref, state_ref, window_ref)),
     ):
         column = 0
         for ref in refs:
             width = ref.shape[1]
-            src = ref
-            if ref is query_ref:
-                src = ref.at[:, pl.ds(0 if array is a_ref else half, half)]
-                width = half
-            moves.append((src, array.at[z, y, c, :, pl.ds(column, width)]))
+            moves.append((ref, array.at[z, y, c, :, pl.ds(column, width)]))
             column += width
     moves.append((tok_ref, held))
     moves = [pltpu.make_async_copy(*move, own_sem.at[i]) for i, move in enumerate(moves)]
@@ -432,38 +489,17 @@
     rows, cols = step.shape
     step = jnp.concatenate([step, jnp.zeros((rows, 128 - cols), F32)], axis=1)
     step = jnp.concatenate([step, jnp.zeros((128 - rows, 128), F32)], axis=0)
-    a_ref[z, y, c, :, WIDTH_A - 128 : WIDTH_A] = step.T[0:cols, :].astype(BF16)
-    for move in moves[:-1]:
+    a_ref[z, y, c, :, EARLY - 128 : EARLY] = step.T[0:cols, :].astype(BF16)
+    for move in moves[:6]:
         move.wait()
     enter()
-
-    sends = transfers(length_z, length_y)
-    number = {s["name"]: i for i, s in enumerate(sends)}
-    by_name = {s["name"]: s for s in sends}
-
-    def block(s, shift):
-        along = s["along"] - shift * s["sign"]
-        dz, dy = (along, s["other"]) if s["axis"] == "z" else (s["other"], along)
-        ref = a_ref if s["kind"] == "A" else b_ref
-        cols = pl.ds(s["cols"][0], s["cols"][1] - s["cols"][0])
-        return ref.at[wrap(z + dz, length_z), wrap(y + dy, length_y), c, :, cols]
-
-    def copy_of(s, shift):
-        i = number[s["name"]]
-        ref = block(s, shift)
-        return pltpu.make_async_remote_copy(
-            src_ref=ref, dst_ref=ref, send_sem=send_sem.at[i], recv_sem=recv_sem.at[i],
-            device_id=towards(s["axis"], s["sign"]), device_id_type=mesh_id,
-        )
-
     edge_copies = []
     for k, (index, dst) in enumerate(((flat - 1, after), (flat + 1, before))):
         edge_copies.append(pltpu.make_async_remote_copy(
             src_ref=tok_ref.at[pl.ds(k * (count_rows - HALO), HALO)], dst_ref=dst,
             send_sem=edge_sem.at[k, 0], recv_sem=edge_sem.at[k, 1],
-            device_id=device_at(index), device_id_type=mesh_id,
+            device_id=device_at(index), device_id_type=pl.DeviceIdType.MESH,
         ))
-
     gain = as_row(gain_ref)
 
     def norm(value):
@@ -471,85 +507,43 @@
         scale = lax.rsqrt(jnp.mean(wide * wide, axis=1, keepdims=True) + EPS)
         return wide * scale * gain
 
-    def norm_block(i, carry):
-        rows = pl.ds(pl.multiple_of(i * BLOCK, BLOCK), BLOCK)
-        normed[rows, :] = norm(held[rows, :]).astype(BF16)
-        return carry
-
-    first, order, _ = arrival_order(sends)
-    started = []
-    for s in first:
-        copy = copy_of(s, 0)
-        copy.start()
-        started.append(copy)
+    def norm_blocks(first, last):
+        def norm_block(i, carry):
+            rows = pl.ds(pl.multiple_of(i * BLOCK, BLOCK), BLOCK)
+            normed[rows, :] = norm(held[rows, :]).astype(BF16)
+            return carry
+
+        lax.fori_loop(first, last, norm_block, 0)
+
+    early.begin()
     for copy in edge_copies:
         copy.start()
-    moves[-1].wait()
-    lax.fori_loop(0, count_rows // BLOCK, norm_block, 0)
-
-    waiting = {}
-    for kind, first_axis, length, second in (("A", "z", length_z, "y"), ("B", "y", length_y, "z")):
-        for offset in range(-(length // 2) + 1, length // 2 + 1):
-            names = [s["name"] for s in sends
-                     if s["kind"] == kind and s["axis"] == second and s["other"] == offset]
-            waiting[(kind, offset)] = set(names)
-    keys = list(waiting)
-
-    def core_copy(key):
-        kind, offset = key
-        i = keys.index(key)
-        if kind == "A":
-            src = a_ref.at[wrap(z + offset, length_z), :, c]
-        else:
-            src = b_ref.at[:, wrap(y + offset, length_y), c]
-        return src, i
-
-    def send_core(key):
-        src, i = core_copy(key)
-        copy = pltpu.make_async_remote_copy(
-            src_ref=src, dst_ref=src, send_sem=core_send.at[i], recv_sem=core_recv.at[i],
-            device_id={SP[2]: other}, device_id_type=mesh_id,
-        )
-        copy.start()
-        started.append(copy)
-
-    def wait_core(key):
-        kind, offset = key
-        i = keys.index(key)
-        if kind == "A":
-            dst = a_ref.at[wrap(z + offset, length_z), :, other]
-        else:
-            dst = b_ref.at[:, wrap(y + offset, length_y), other]
-        pltpu.make_async_remote_copy(
-            src_ref=dst, dst_ref=dst, send_sem=core_send.at[i], recv_sem=core_recv.at[i],
-            device_id={SP[2]: other}, device_id_type=mesh_id,
-        ).wait_recv()
-
-    for name, ready in order:
-        copy_of(by_name[name], 1).wait_recv()
-        for s in ready:
-            copy = copy_of(s, 0)
-            copy.start()
-            started.append(copy)
-        for key in keys:
-            if name in waiting[key]:
-                waiting[key].remove(name)
-                if not waiting[key]:
-                    send_core(key)
-    for copy in started:
-        copy.wait_send()
-    for key in keys:
-        wait_core(key)
+    for move in moves[6:]:
+        move.wait()
+    blocks = count_rows // BLOCK
+    norm_blocks(0, blocks // 2)
+    early.service(4.5)
+    norm_blocks(blocks // 2, blocks)
+    early.service(2.0)
     for copy in edge_copies:
         copy.wait()
     normed[count_rows : count_rows + HALO, :] = jnp.where(flat > 0, norm(before[...]), 0.0).astype(BF16)
     normed[count_rows + HALO : count_rows + 2 * HALO, :] = jnp.where(
         flat < count - 1, norm(after[...]), 0.0
     ).astype(BF16)
+    early.service(1.0)
+    while sum(early.left.values()) > 0:
+        early.clock = max(early.clock, early.heap[0][0])
+        early.handle()
+    late.clock = early.clock
+    late.free = dict(early.free)
+    late.begin()
+    early.drain()
+    late.service(max(early.clock - late.clock, 0.0))
 
 
 def middle(
-    normed, a_ref, b_ref, taps_x_ref, taps_b_ref, taps_c_ref, rate_ref, freq_ref, sink_ref,
+    late, normed, a_ref, b_ref, taps_x_ref, taps_b_ref, taps_c_ref, rate_ref, freq_ref, sink_ref,
     out_ref, window_ref, log_ref, gate_ref, conv_ref, col_ref, row_ref, piece_ref, etot_ref,
     cin_ref, kv_ref, q_ref, step_ref, win, near, msg_ref,
     kv_before_ref, kv_after_ref, keys, values, by_row, by_col, part, turned, by_y, summed, by_z,
@@ -586,6 +580,7 @@
         lax.fori_loop(0, tiles, column, 0)
 
     project(kv_ref, rows, 1, a_ref, KV_AT)
+    late.service(1.1)
 
     def send(src, dst, sems, peer):
         copy = pltpu.make_async_remote_copy(
@@ -617,9 +612,13 @@
         ),
         send(kv_ref.at[pl.ds(0, WINDOW)], kv_after_ref, kv_sem.at[1], device_at(flat - 1)),
     ]
-    project(cin_ref, rows + 2 * HALO, 3, a_ref, 0)
-    step_ref[...] = dot(normed[0:rows, :], a_ref[:, WIDTH_A - 128 : WIDTH_A])
+    project(cin_ref.at[:, pl.ds(0, 256)], rows + 2 * HALO, 1, a_ref, 0)
+    late.service(1.1)
+    project(cin_ref.at[:, pl.ds(256, 512)], rows + 2 * HALO, 2, a_ref, 256)
+    step_ref[...] = dot(normed[0:rows, :], a_ref[:, EARLY - 128 : EARLY])
+    late.service(2.8)
     conv_state(
+        late.service,
         cin_ref, taps_x_ref, taps_b_ref, taps_c_ref, step_ref, rate_ref,
         conv_ref, col_ref, row_ref, piece_ref, etot_ref, msg_ref, win, near,
     )
@@ -629,15 +628,9 @@
         window_ref, log_ref, keys, values, by_row, by_col,
     )
 
-    def attend_blocks(first, last):
-        def one(i, carry):
-            attend(i)
-            return carry
-
-        lax.fori_loop(first, last, one, 0)
-
     blocks = rows // BLOCK
     own_keys()
+    late.service(1.2)
     copy.wait()
     for j in range(pairs):
         decay = decay_of(part, j)
@@ -652,8 +645,8 @@
         to = lax.rem(y + k, length_y)
         copies.append(send(turned.at[to], by_y.at[k], y_sem.at[k], {SP[1]: to}))
     by_y[0] = turned[y]
-    project(q_ref.at[:, pl.ds(0, 256)], rows, 1, a_ref, WIDTH_A - 384)
-    project(q_ref.at[:, pl.ds(256, 256)], rows, 1, b_ref, WIDTH_B - 256)
+    project(q_ref, rows, 2, a_ref, Q_AT)
+    late.service(2.4)
     for copy in copies:
         copy.wait()
     before = []
@@ -674,7 +667,9 @@
             send(summed, by_z.at[k], z_sem.at[k], {SP[0]: to})
 
     carry[...] = jnp.zeros_like(carry)
-    attend_blocks(1, blocks - 1)
+    for i in range(1, blocks - 1):
+        attend(i)
+        late.service(1.9)
     for distance in reversed(range(1, length_z)):
         slot = jnp.where(forward, distance, length_z - distance)
 
@@ -710,6 +705,7 @@
         copy.wait()
     edge_keys()
     attend(0)
+    late.service(2.2)
     for copy in copies:
         copy.wait()
     for j in range(pairs):
@@ -720,7 +716,9 @@
         ).astype(BF16)
     copy = send(nxt, final, final_sem, {SP[2]: other})
     attend(blocks - 1)
-    project(gate_ref, rows, 2, a_ref, GATE_AT)
+    late.service(2.0)
+    late.drain()
+    project(gate_ref, rows, 2, b_ref, 0)
     copy.wait()
     out_ref[other] = final[...]
 
@@ -748,8 +746,8 @@
 
     def terms(rows, to):
         outs = pl.ds(pl.multiple_of(to * width, width), width)
-        return dot(state_ref[rows, :], w_ref[outs, 0:channels], ((1,), (1,))) + dot(
-            window_ref[rows, :], w_ref[outs, channels : 2 * channels], ((1,), (1,))
+        return dot(state_ref[rows, :], w_ref[outs, OUT_AT : OUT_AT + channels], ((1,), (1,))) + dot(
+            window_ref[rows, :], w_ref[outs, OUT_AT + channels : OUT_AT + 2 * channels], ((1,), (1,))
         )
 
     def far_copy(i, k):
@@ -817,7 +815,8 @@
     sink_ref, mixed_ref, log_ref = refs[:3]
     smalls, refs = refs[3:11], refs[11:]
     small_sem, a_ref, b_ref, normed = refs[:4]
-    gather_refs, refs = refs[4:13], refs[13:]
+    gather_refs, refs = refs[4:9], refs[9:]
+    flow_sems, refs = (refs[0:4], refs[4:8]), refs[8:]
     incoming, window_ref, gate_ref = refs[:3]
     conv_refs, refs = refs[3:8], refs[8:]
     middle_refs, finish_refs = refs[:29], refs[29:]
@@ -855,19 +854,24 @@
     def enter():
         pl.semaphore_wait(barrier, len(peers))
 
+    early, late = (
+        Flow(i, {"z": length_z, "y": length_y}, (a_ref, b_ref), flow_sems[i]) for i in range(2)
+    )
     gather(
-        lengths, small_copies, enter, tok_ref, gain_ref, step_ref, *shards,
-        a_ref, b_ref, normed, *gather_refs,
-    )
-    flat_a = a_ref.reshape(length_z * length_y * 64, WIDTH_A)
-    flat_b = b_ref.reshape(length_z * length_y * 64, WIDTH_B)
+        early, late, small_copies, enter, tok_ref, gain_ref, step_ref, *shards,
+        normed, *gather_refs,
+    )
+    flat_a = a_ref.reshape(length_z * length_y * 64, EARLY)
+    flat_b = b_ref.reshape(length_z * length_y * 64, LATE)
     middle(
-        normed, flat_a, flat_b, taps_x, taps_b, taps_c, rate_ref, freq_ref, sink_ref,
+        late, normed, flat_a, flat_b, taps_x, taps_b, taps_c, rate_ref, freq_ref, sink_ref,
         incoming, window_ref, log_ref, gate_ref, *conv_refs, *middle_refs,
     )
     finish(
         window_ref, flat_b, *conv_refs, incoming, gate_ref, group_gain_ref, mixed_ref, *finish_refs
     )
+    early.finish()
+    late.finish()
 
 
 def layer(length_z, length_y, n, tokens, smalls, shards, sinks):
@@ -879,8 +883,7 @@
     tile = (STATE, 128)
     full = (MSG, 128)
     lead = (length_z, length_y, 2, 32)
-    sends = len(transfers(length_z, length_y))
-    groups = length_z + length_y
+    flows = [transfers(routes, {"z": length_z, "y": length_y}) for routes in ROUTES]
     part = model // n
     dma = pltpu.SemaphoreType.DMA
     vmem = pltpu.VMEM
@@ -888,12 +891,12 @@
     scratch = [
         *(vmem(s.shape, s.dtype) for s in smalls),
         dma((len(smalls),)),
-        vmem((*lead, WIDTH_A), BF16),
-        vmem((*lead, WIDTH_B), BF16),
+        vmem((*lead, EARLY), BF16),
+        vmem((*lead, LATE), BF16),
         vmem((rows + 2 * HALO, model), BF16),
         vmem((HALO, model), BF16), vmem((HALO, model), BF16), vmem((rows, model), BF16),
-        dma((sends,)), dma((sends,)), dma((groups,)), dma((groups,)), dma((2, 2)),
-        dma((len(shards) + 2,)),
+        dma((2, 2)), dma((len(shards) + 1,)),
+        *(dma((len(part),)) for sends, groups in flows for part in (sends, sends, groups, groups)),
         vmem((2, pairs, *tile), BF16),
         vmem((rows, channels), BF16),
         vmem((rows, channels), BF16),

time: 123 us -> 115 us (0.935)
  Pallas kernels: 119 us -> 111 us
    pallas_call x1, Pallas kernels: 119 us -> 111 us  [layer(): pl.pallas_call(functools.partial(layer_kernel, (length_z, length_y)), in_...]
where the time goes in v5:
time: 115 us
  Pallas kernels  111 us (97%)
  local copies, waits for them, and re-layouts  3.41 us (3%)
    pallas_call x1, Pallas kernels, layer(): pl.pallas_call(functools.partial(layer_kernel, (length_z, length_y)), in_...  111 us
    unnamed x2, local copies, waits for them, and re-layouts  3.41 us

profile of v5, /device:TPU:1, one launch (start us, length us, event | category | flops | bytes accessed | tf_op | source)
XLA Modules:
  0.0 114.6 jit_solution(16478281043958099802)
XLA Ops:
  0.6 110.5 %layer.1 = (bf16[768,512]{1,0:T(8,128)(2,1)}, f32[8,768]{1,0:T(8,128)}) custom-call(bf16[768,2048]{1,0:T(8,128)(2,1)} %tok_ref.1, bf16[16,128]{1,0:T(8,128)(2,1)} %bitcast.21, bf16[16,32]{1,0:T(8,128)(2,1)} %bitcast.22, bf16[5,512]{1,0:T(8,128)(2,1)} %refs_2_.1, bf16[5,128]{1,0:T(8,128)(2,1)} %bitcast.23, bf16[5,128]{1,0:T(8,128)(2,1)} %bitcast.24, ...), custom_call_target="tpu_custom_call" | custom-call | flops 8589934592 | bytes 25165824 | tf_op jit(solution)/shard_map/layer/pallas_call | solution.py:941
  111.2 2.1 %copy.23 = bf16[768,512]{1,0:T(8,128)(2,1)} copy(bf16[768,512]{1,0:T(8,128)(2,1)} %get-tuple-element.8) | data formatting | bytes 1572864
  113.2 1.3 %copy.24 = f32[768,8]{0,1:T(8,128)} copy(f32[768,8]{0,1:T(8,128)} %bitcast.15) | data formatting | bytes 49152

commit v6 on v5

--- a/solution.py
+++ b/solution.py
@@ -63,8 +63,8 @@
 
 
 def conv_state(
-    service, cin_ref, taps_x_ref, taps_b_ref, taps_c_ref, step_ref, rate_ref,
-    conv_ref, col_ref, row_ref, piece_ref, etot_ref, msg_ref, win, near,
+    traffic_service, cin_ref, taps_x_ref, taps_b_ref, taps_c_ref, step_ref, rate_ref,
+    conv_ref, col_ref, row_ref, piece_ref, etot_ref, msg_ref, win,
 ):
     count = cin_ref.shape[0] - 2 * HALO
     blocks = count // BLOCK
@@ -86,42 +86,53 @@
         return carry
 
     lax.fori_loop(0, blocks, fill, 0)
-    service(0.5)
-
-    def one(i, total):
-        start = pl.multiple_of(i * BLOCK, BLOCK)
-        rows = pl.ds(start, BLOCK)
-        near[...] = win[pl.ds(start, BLOCK + 2 * HALO), :]
-        acc = near[HALO - 2 : HALO - 2 + BLOCK, :] * taps[0:1, :]
-        for tap in range(1, 5):
-            first = HALO - 2 + tap
-            acc = acc + near[first : first + BLOCK, :] * taps[tap : tap + 1, :]
-        conv = (acc * jax.nn.sigmoid(acc)).astype(BF16)
-        conv_ref[rows, :] = conv
-        raw = step_ref[rows, 0 : 2 * HEADS]
-        step = jnp.maximum(raw, 0.0) + jnp.log1p(jnp.exp(-jnp.abs(raw)))
-        rate = jnp.concatenate([rate_ref[:, rows], jnp.zeros((BLOCK - 2 * HEADS, BLOCK), F32)], axis=0)
-        decay = -jnp.exp(rate.T[:, 0 : 2 * HEADS]) * step
-        cum = dot(tri, decay, precision=lax.Precision.HIGHEST)
-        tot = cum[BLOCK - 1 : BLOCK, :]
-        col = jnp.where(forward16, cum, cum - decay)
-        col_ref[rows, 0 : 2 * HEADS] = col
-        col_ref[rows, 2 * HEADS : 4 * HEADS] = jnp.broadcast_to(tot, (BLOCK, 2 * HEADS))
-        both = jnp.concatenate([col, step, jnp.zeros((BLOCK, 128 - 4 * HEADS), F32)], axis=1)
-        row_ref[i] = both.T[0 : 4 * HEADS, :]
-        weight = jnp.exp(jnp.where(forward16, tot - col, col)) * step
-        wide = spread(weight, spread_m, 2)
-        xs = conv[:, 0:channels].astype(F32)
-        scaled = (jnp.concatenate([xs, xs], axis=1) * wide).astype(BF16)
-        inflow = conv[:, channels : channels + STATE]
-        piece_ref[i] = dot(inflow, scaled, ((0,), (0,)))
-        etot_ref[i] = spread(jnp.exp(jnp.broadcast_to(tot, (8, 2 * HEADS))), spread_m, 3)
-        return total + tot
+    traffic_service(0.5)
+
+    def some(which):
+        spans = [slice(i * BLOCK, (i + 1) * BLOCK) for i in which]
+        steps, decays, convs = [], [], []
+        for rows in spans:
+            raw = step_ref[rows, 0 : 2 * HEADS]
+            steps.append(jnp.maximum(raw, 0.0) + jnp.log1p(jnp.exp(-jnp.abs(raw))))
+            rate = jnp.concatenate(
+                [rate_ref[:, rows], jnp.zeros((BLOCK - 2 * HEADS, BLOCK), F32)], axis=0
+            )
+            decays.append(-jnp.exp(rate.T[:, 0 : 2 * HEADS]) * steps[-1])
+        cums = [dot(tri, decay, precision=lax.Precision.HIGHEST) for decay in decays]
+        tots = [cum[BLOCK - 1 : BLOCK, :] for cum in cums]
+        cols = [jnp.where(forward16, cum, cum - decay) for cum, decay in zip(cums, decays)]
+        weights = [
+            jnp.exp(jnp.where(forward16, tot - col, col)) * step
+            for tot, col, step in zip(tots, cols, steps)
+        ]
+        wides = [spread(weight, spread_m, 2) for weight in weights]
+        etots = [spread(jnp.exp(jnp.broadcast_to(tot, (8, 2 * HEADS))), spread_m, 3) for tot in tots]
+        rests = jnp.zeros((BLOCK, 128 - 4 * HEADS), F32)
+        turned = [jnp.concatenate([col, step, rests], axis=1).T for col, step in zip(cols, steps)]
+        for rows in spans:
+            acc = 0.0
+            for tap in range(5):
+                first = rows.start + HALO - 2 + tap
+                acc = acc + win[first : first + BLOCK, :] * taps[tap : tap + 1, :]
+            convs.append((acc * jax.nn.sigmoid(acc)).astype(BF16))
+        pieces = []
+        for conv, wide in zip(convs, wides):
+            xs = conv[:, 0:channels].astype(F32)
+            scaled = (jnp.concatenate([xs, xs], axis=1) * wide).astype(BF16)
+            pieces.append(dot(conv[:, channels : channels + STATE], scaled, ((0,), (0,))))
+        for n, (i, rows) in enumerate(zip(which, spans)):
+            conv_ref[rows, :] = convs[n]
+            col_ref[rows, 0 : 2 * HEADS] = cols[n]
+            col_ref[rows, 2 * HEADS : 4 * HEADS] = jnp.broadcast_to(tots[n], (BLOCK, 2 * HEADS))
+            row_ref[i] = turned[n][0 : 4 * HEADS, :]
+            piece_ref[i] = pieces[n]
+            etot_ref[i] = etots[n]
+        return sum(tots)
 
     total = jnp.zeros((1, 2 * HEADS), F32)
     for i in range(0, blocks, 2):
-        total = lax.fori_loop(i, i + 2, one, total)
-        service(1.7)
+        total = total + some((i, i + 1))
+        traffic_service(1.6)
     forward = piece_ref[0, :, 0:channels]
     backward = piece_ref[blocks - 1, :, channels : 2 * channels]
     for i in range(1, blocks):
@@ -272,38 +283,43 @@
         valid = in_band & (here >= start_at) & (here < end_at)
         table = tables(i + 1)
         band = pl.ds(start, 3 * BLOCK)
+        qs = []
         for pair in range(HEADS // 2):
-            group = pair // 2
             lanes = slice(pair * 128, pair * 128 + 128)
             q = (turn(q_ref[rows, lanes], table).astype(F32) * HEAD_DIM ** (-0.5)).astype(BF16)
             zero = jnp.zeros_like(q)
-            both = jnp.concatenate(
+            qs.append(jnp.concatenate(
                 [jnp.where(first_half, q, zero), jnp.where(first_half, zero, q)], axis=0
-            )
-            scores = dot(keys[group, band, :], both, ((1,), (1,)))
-            scores = jnp.where(valid, scores, -1e30)
+            ))
+        scores = [dot(keys[pair // 2, band, :], q, ((1,), (1,))) for pair, q in enumerate(qs)]
+        outs = []
+        for pair in range(HEADS // 2):
+            group = pair // 2
+            mine = jnp.where(valid, scores[pair], -1e30)
             sink = jnp.where(first_row_half, sink_ref[2 * pair], sink_ref[2 * pair + 1])
-            top = jnp.maximum(jnp.max(scores, axis=0, keepdims=True), sink)
-            expo = jnp.exp(scores - top)
+            top = jnp.maximum(jnp.max(mine, axis=0, keepdims=True), sink)
+            expo = jnp.exp(mine - top)
             total = jnp.sum(expo, axis=0, keepdims=True) + jnp.exp(sink - top)
-            mine = values[group * HEAD_DIM : (group + 1) * HEAD_DIM, band]
-            o = dot(mine, expo.astype(BF16)) / total
-            turned = jnp.concatenate([o[:, 0:BLOCK], o[:, BLOCK:]], axis=0).T
-            out_ref[rows, lanes] = turned.astype(BF16)
+            value = values[group * HEAD_DIM : (group + 1) * HEAD_DIM, band]
+            outs.append(dot(value, expo.astype(BF16)) / total)
             log = top + jnp.log(total)
             log_ref[2 * pair : 2 * pair + 1, rows] = log[:, 0:BLOCK]
             log_ref[2 * pair + 1 : 2 * pair + 2, rows] = log[:, BLOCK:]
+        for pair, o in enumerate(outs):
+            turned = jnp.concatenate([o[:, 0:BLOCK], o[:, BLOCK:]], axis=0).T
+            out_ref[rows, pair * 128 : pair * 128 + 128] = turned.astype(BF16)
 
     return own_keys, edge_keys, one
 
 
 LINKS = ("z+", "z-", "y+", "y-")
-EARLY = 1664
-LATE = 1536
+WIDTHS = (1152, 512, 1536)
 ROUTES = (
-    (("A", 0, 0, 1024, 512, "z"), ("B", 0, 1024, 640, 384, "y")),
-    (("C", 1, 0, 896, 512, "z"), ("D", 1, 896, 640, 384, "y")),
+    (("A", 0, 0, 640, 384, "z"), ("B", 0, 640, 512, 256, "y")),
+    (("C", 1, 0, 256, 128, "z"), ("D", 1, 256, 256, 128, "y")),
+    (("E", 2, 0, 896, 512, "z"), ("F", 2, 896, 640, 384, "y")),
 )
+BEGIN_AFTER = (50, 60)
 RATE = 46.6e3
 HOP = 1.9
 
@@ -348,11 +364,12 @@
 
 
 class Flow:
-    def __init__(self, number, lengths, arrays, sems):
+    def __init__(self, number, lengths, arrays, sems, free):
         self.routes = ROUTES[number]
         self.lengths = lengths
         self.arrays = arrays
         self.send_sem, self.recv_sem, self.core_send, self.core_recv = sems
+        self.free = free
         self.at = dict(zip("zy", (lax.axis_index(SP[0]), lax.axis_index(SP[1]))))
         self.c = lax.axis_index(SP[2])
         self.sends, self.groups = transfers(self.routes, lengths)
@@ -365,10 +382,10 @@
             for need in s["needs"]:
                 self.followers.setdefault(need, []).append(s)
         self.first_axis = {route[0]: route[5] for route in self.routes}
-        self.free = dict.fromkeys(LINKS, 0.0)
         self.heap = []
         self.clock = 0.0
         self.started = []
+        self.launched = 0
 
     def wrap(self, axis, shift):
         length = self.lengths[axis]
@@ -410,6 +427,7 @@
         copy = self.copy_of(s, 0)
         copy.start()
         self.started.append(copy)
+        self.launched += 1
         link = s["axis"] + ("+" if s["sign"] == 1 else "-")
         self.free[link] = max(self.free[link], self.clock) + 64 * s["cols"][1] / RATE
         heapq.heappush(self.heap, (self.free[link] + HOP, len(self.started), s["key"]))
@@ -433,34 +451,65 @@
                     copy.start()
                     self.started.append(copy)
 
+    def wait_core(self):
+        for group in self.group_keys:
+            self.core_copy(group, 1 - self.c).wait_recv()
+
+
+class Traffic:
+    def __init__(self, lengths, arrays, sems):
+        free = dict.fromkeys(LINKS, 0.0)
+        self.flows = [Flow(i, lengths, arrays, s, free) for i, s in enumerate(sems)]
+        self.lengths = lengths
+        self.arrays = arrays
+        self.clock = 0.0
+        self.newest = 0
+
+    def begin(self):
+        self.flows[0].begin()
+
+    def next_arrival(self):
+        return min(((f.heap[0][0], i) for i, f in enumerate(self.flows) if f.heap), default=None)
+
+    def handle(self, index, now):
+        flow = self.flows[index]
+        flow.clock = max(flow.clock, now)
+        flow.handle()
+        if index == self.newest and index + 1 < len(self.flows):
+            if flow.launched >= BEGIN_AFTER[index]:
+                self.newest += 1
+                self.flows[self.newest].clock = flow.clock
+                self.flows[self.newest].begin()
+
     def service(self, passed):
         self.clock += passed
-        while self.heap and self.heap[0][0] <= self.clock:
-            self.handle()
-
-    def drain(self):
-        while self.heap:
-            self.clock = max(self.clock, self.heap[0][0])
-            self.handle()
-        for group in self.group_keys:
-            self.core_copy(group, 1 - self.c).wait_recv()
+        while (head := self.next_arrival()) and head[0] <= self.clock:
+            self.handle(head[1], self.clock)
+
+    def until(self, index):
+        while self.newest < index or self.flows[index].heap:
+            head = self.next_arrival()
+            self.clock = max(self.clock, head[0])
+            self.handle(head[1], self.clock)
+        self.flows[index].wait_core()
 
     def finish(self):
-        for copy in self.started:
-            copy.wait_send()
+        for flow in self.flows:
+            for copy in flow.started:
+                copy.wait_send()
 
 
 def gather(
-    early, late, small_copies, enter, tok_ref, gain_ref, step_ref, value_ref, inflow_ref,
+    traffic, small_copies, enter, tok_ref, gain_ref, step_ref, value_ref, inflow_ref,
     readout_ref, key_ref, vector_ref, gate_ref, query_ref, state_ref, window_ref,
     normed, before, after, held, edge_sem, own_sem,
 ):
     z, y, c = (lax.axis_index(a) for a in SP)
-    length_z, length_y = early.lengths["z"], early.lengths["y"]
+    length_z, length_y = traffic.lengths["z"], traffic.lengths["y"]
     flat = (z * length_y + y) * 2 + c
     count = length_z * length_y * 2
     count_rows = tok_ref.shape[0]
-    a_ref, b_ref = early.arrays
+    a_ref, q_ref, b_ref = traffic.arrays
 
     def device_at(index):
         index = lax.rem(index + count, count)
@@ -472,7 +521,8 @@
 
     moves = []
     for array, refs in (
-        (a_ref, (value_ref, inflow_ref, readout_ref, key_ref, vector_ref, query_ref)),
+        (a_ref, (value_ref, inflow_ref, readout_ref, key_ref, vector_ref)),
+        (q_ref, (query_ref,)),
         (b_ref, (gate_ref, state_ref, window_ref)),
     ):
         column = 0
@@ -489,8 +539,8 @@
     rows, cols = step.shape
     step = jnp.concatenate([step, jnp.zeros((rows, 128 - cols), F32)], axis=1)
     step = jnp.concatenate([step, jnp.zeros((128 - rows, 128), F32)], axis=0)
-    a_ref[z, y, c, :, EARLY - 128 : EARLY] = step.T[0:cols, :].astype(BF16)
-    for move in moves[:6]:
+    a_ref[z, y, c, :, WIDTHS[0] - 128 : WIDTHS[0]] = step.T[0:cols, :].astype(BF16)
+    for move in moves[:5]:
         move.wait()
     enter()
     edge_copies = []
@@ -515,35 +565,29 @@
 
         lax.fori_loop(first, last, norm_block, 0)
 
-    early.begin()
+    traffic.begin()
     for copy in edge_copies:
         copy.start()
-    for move in moves[6:]:
+    for move in moves[5:]:
         move.wait()
     blocks = count_rows // BLOCK
-    norm_blocks(0, blocks // 2)
-    early.service(4.5)
-    norm_blocks(blocks // 2, blocks)
-    early.service(2.0)
+    traffic.service(1.0)
+    for i in range(blocks):
+        norm_blocks(i, i + 1)
+        traffic.service(0.6)
     for copy in edge_copies:
         copy.wait()
     normed[count_rows : count_rows + HALO, :] = jnp.where(flat > 0, norm(before[...]), 0.0).astype(BF16)
     normed[count_rows + HALO : count_rows + 2 * HALO, :] = jnp.where(
         flat < count - 1, norm(after[...]), 0.0
     ).astype(BF16)
-    early.service(1.0)
-    while sum(early.left.values()) > 0:
-        early.clock = max(early.clock, early.heap[0][0])
-        early.handle()
-    late.clock = early.clock
-    late.free = dict(early.free)
-    late.begin()
-    early.drain()
-    late.service(max(early.clock - late.clock, 0.0))
+    traffic.service(0.3)
+    traffic.until(0)
+    traffic.service(1.5)
 
 
 def middle(
-    late, normed, a_ref, b_ref, taps_x_ref, taps_b_ref, taps_c_ref, rate_ref, freq_ref, sink_ref,
+    traffic, normed, a_ref, query_ref, b_ref, taps_x_ref, taps_b_ref, taps_c_ref, rate_ref, freq_ref, sink_ref,
     out_ref, window_ref, log_ref, gate_ref, conv_ref, col_ref, row_ref, piece_ref, etot_ref,
     cin_ref, kv_ref, q_ref, step_ref, win, near, msg_ref,
     kv_before_ref, kv_after_ref, keys, values, by_row, by_col, part, turned, by_y, summed, by_z,
@@ -570,17 +614,12 @@
 
     def project(dst, count, tiles, source, first):
         tile = 256
-
-        def column(j, carry_over):
-            cols = pl.ds(pl.multiple_of(j * tile, tile), tile)
-            from_cols = pl.ds(pl.multiple_of(first + j * tile, 128), tile)
-            dst[:, cols] = dot(normed[0:count, :], source[:, from_cols]).astype(BF16)
-            return carry_over
-
-        lax.fori_loop(0, tiles, column, 0)
+        for j in range(tiles):
+            cols = slice(first + j * tile, first + (j + 1) * tile)
+            dst[:, j * tile : (j + 1) * tile] = dot(normed[0:count, :], source[:, cols]).astype(BF16)
+            traffic.service(1.05)
 
     project(kv_ref, rows, 1, a_ref, KV_AT)
-    late.service(1.1)
 
     def send(src, dst, sems, peer):
         copy = pltpu.make_async_remote_copy(
@@ -612,15 +651,13 @@
         ),
         send(kv_ref.at[pl.ds(0, WINDOW)], kv_after_ref, kv_sem.at[1], device_at(flat - 1)),
     ]
-    project(cin_ref.at[:, pl.ds(0, 256)], rows + 2 * HALO, 1, a_ref, 0)
-    late.service(1.1)
-    project(cin_ref.at[:, pl.ds(256, 512)], rows + 2 * HALO, 2, a_ref, 256)
-    step_ref[...] = dot(normed[0:rows, :], a_ref[:, EARLY - 128 : EARLY])
-    late.service(2.8)
+    project(cin_ref, rows + 2 * HALO, 3, a_ref, 0)
+    step_ref[...] = dot(normed[0:rows, :], a_ref[:, WIDTHS[0] - 128 : WIDTHS[0]])
+    traffic.service(0.6)
     conv_state(
-        late.service,
+        traffic.service,
         cin_ref, taps_x_ref, taps_b_ref, taps_c_ref, step_ref, rate_ref,
-        conv_ref, col_ref, row_ref, piece_ref, etot_ref, msg_ref, win, near,
+        conv_ref, col_ref, row_ref, piece_ref, etot_ref, msg_ref, win,
     )
     copy = send(msg_ref.at[other], part, part_sem, {SP[2]: other})
     own_keys, edge_keys, attend = attention(
@@ -630,7 +667,7 @@
 
     blocks = rows // BLOCK
     own_keys()
-    late.service(1.2)
+    traffic.service(1.2)
     copy.wait()
     for j in range(pairs):
         decay = decay_of(part, j)
@@ -645,8 +682,10 @@
         to = lax.rem(y + k, length_y)
         copies.append(send(turned.at[to], by_y.at[k], y_sem.at[k], {SP[1]: to}))
     by_y[0] = turned[y]
-    project(q_ref, rows, 2, a_ref, Q_AT)
-    late.service(2.4)
+    traffic.until(1)
+    project(q_ref, rows, 2, query_ref, 0)
+    attend(1)
+    traffic.service(1.1)
     for copy in copies:
         copy.wait()
     before = []
@@ -667,9 +706,9 @@
             send(summed, by_z.at[k], z_sem.at[k], {SP[0]: to})
 
     carry[...] = jnp.zeros_like(carry)
-    for i in range(1, blocks - 1):
+    for i in range(2, blocks - 1):
         attend(i)
-        late.service(1.9)
+        traffic.service(1.1)
     for distance in reversed(range(1, length_z)):
         slot = jnp.where(forward, distance, length_z - distance)
 
@@ -705,7 +744,7 @@
         copy.wait()
     edge_keys()
     attend(0)
-    late.service(2.2)
+    traffic.service(1.3)
     for copy in copies:
         copy.wait()
     for j in range(pairs):
@@ -716,8 +755,8 @@
         ).astype(BF16)
     copy = send(nxt, final, final_sem, {SP[2]: other})
     attend(blocks - 1)
-    late.service(2.0)
-    late.drain()
+    traffic.service(1.1)
+    traffic.until(2)
     project(gate_ref, rows, 2, b_ref, 0)
     copy.wait()
     out_ref[other] = final[...]
@@ -814,9 +853,9 @@
     shards, refs = refs[:9], refs[9:]
     sink_ref, mixed_ref, log_ref = refs[:3]
     smalls, refs = refs[3:11], refs[11:]
-    small_sem, a_ref, b_ref, normed = refs[:4]
-    gather_refs, refs = refs[4:9], refs[9:]
-    flow_sems, refs = (refs[0:4], refs[4:8]), refs[8:]
+    small_sem, arrays, normed = refs[0], refs[1:4], refs[4]
+    gather_refs, refs = refs[5:10], refs[10:]
+    flow_sems, refs = (refs[0:4], refs[4:8], refs[8:12]), refs[12:]
     incoming, window_ref, gate_ref = refs[:3]
     conv_refs, refs = refs[3:8], refs[8:]
     middle_refs, finish_refs = refs[:29], refs[29:]
@@ -854,24 +893,21 @@
     def enter():
         pl.semaphore_wait(barrier, len(peers))
 
-    early, late = (
-        Flow(i, {"z": length_z, "y": length_y}, (a_ref, b_ref), flow_sems[i]) for i in range(2)
+    traffic = Traffic({"z": length_z, "y": length_y}, arrays, flow_sems)
+    gather(
+        traffic, small_copies, enter, tok_ref, gain_ref, step_ref, *shards, normed, *gather_refs,
     )
-    gather(
-        early, late, small_copies, enter, tok_ref, gain_ref, step_ref, *shards,
-        normed, *gather_refs,
-    )
-    flat_a = a_ref.reshape(length_z * length_y * 64, EARLY)
-    flat_b = b_ref.reshape(length_z * length_y * 64, LATE)
+    flat_refs = [
+        ref.reshape(length_z * length_y * 64, width) for ref, width in zip(arrays, WIDTHS)
+    ]
     middle(
-        late, normed, flat_a, flat_b, taps_x, taps_b, taps_c, rate_ref, freq_ref, sink_ref,
+        traffic, normed, *flat_refs, taps_x, taps_b, taps_c, rate_ref, freq_ref, sink_ref,
         incoming, window_ref, log_ref, gate_ref, *conv_refs, *middle_refs,
     )
     finish(
-        window_ref, flat_b, *conv_refs, incoming, gate_ref, group_gain_ref, mixed_ref, *finish_refs
+        window_ref, flat_refs[2], *conv_refs, incoming, gate_ref, group_gain_ref, mixed_ref, *finish_refs
     )
-    early.finish()
-    late.finish()
+    traffic.finish()
 
 
 def layer(length_z, length_y, n, tokens, smalls, shards, sinks):
@@ -891,8 +927,7 @@
     scratch = [
         *(vmem(s.shape, s.dtype) for s in smalls),
         dma((len(smalls),)),
-        vmem((*lead, EARLY), BF16),
-        vmem((*lead, LATE), BF16),
+        *(vmem((*lead, w), BF16) for w in WIDTHS),
         vmem((rows + 2 * HALO, model), BF16),
         vmem((HALO, model), BF16), vmem((HALO, model), BF16), vmem((rows, model), BF16),
         dma((2, 2)), dma((len(shards) + 1,)),

time: 115 us -> 120 us (1.043)
  Pallas kernels: 111 us -> 116 us
    pallas_call x1, Pallas kernels: 111 us -> 116 us  [layer(): pl.pallas_call(functools.partial(layer_kernel, (length_z, length_y)), in_...]
where the time goes in v6:
time: 120 us
  Pallas kernels  116 us (97%)
  local copies, waits for them, and re-layouts  3.41 us (3%)
    pallas_call x1, Pallas kernels, layer(): pl.pallas_call(functools.partial(layer_kernel, (length_z, length_y)), in_...  116 us
    unnamed x2, local copies, waits for them, and re-layouts  3.41 us

profile of v6, /device:TPU:1, one launch (start us, length us, event | category | flops | bytes accessed | tf_op | source)
XLA Modules:
  0.0 120.0 jit_solution(2807150441869071824)
XLA Ops:
  0.6 115.9 %layer.1 = (bf16[768,512]{1,0:T(8,128)(2,1)}, f32[8,768]{1,0:T(8,128)}) custom-call(bf16[768,2048]{1,0:T(8,128)(2,1)} %tok_ref.1, bf16[16,128]{1,0:T(8,128)(2,1)} %bitcast.21, bf16[16,32]{1,0:T(8,128)(2,1)} %bitcast.22, bf16[5,512]{1,0:T(8,128)(2,1)} %refs_2_.1, bf16[5,128]{1,0:T(8,128)(2,1)} %bitcast.23, bf16[5,128]{1,0:T(8,128)(2,1)} %bitcast.24, ...), custom_call_target="tpu_custom_call" | custom-call | flops 8589934592 | bytes 25165824 | tf_op jit(solution)/shard_map/layer/pallas_call | solution.py:976
  116.6 2.1 %copy.23 = bf16[768,512]{1,0:T(8,128)(2,1)} copy(bf16[768,512]{1,0:T(8,128)(2,1)} %get-tuple-element.8) | data formatting | bytes 1572864
  118.7 1.3 %copy.24 = f32[768,8]{0,1:T(8,128)} copy(f32[768,8]{0,1:T(8,128)} %bitcast.15) | data formatting | bytes 49152

commit v7 on v6

--- a/solution.py
+++ b/solution.py
@@ -313,15 +313,14 @@
 
 
 LINKS = ("z+", "z-", "y+", "y-")
-WIDTHS = (1152, 512, 1536)
+WIDTHS = (1664, 1536)
 ROUTES = (
-    (("A", 0, 0, 640, 384, "z"), ("B", 0, 640, 512, 256, "y")),
-    (("C", 1, 0, 256, 128, "z"), ("D", 1, 256, 256, 128, "y")),
-    (("E", 2, 0, 896, 512, "z"), ("F", 2, 896, 640, 384, "y")),
+    (("A", 0, 0, 1024, 512, "z"), ("B", 0, 1024, 640, 384, "y")),
+    (("C", 1, 0, 896, 512, "z"), ("D", 1, 896, 640, 384, "y")),
 )
-BEGIN_AFTER = (50, 60)
-RATE = 46.6e3
-HOP = 1.9
+BEGIN_AFTER = (76,)
+RATE = 42.0e3
+HOP = 2.6
 
 
 def ring(route, axis, other, length):
@@ -509,7 +508,7 @@
     flat = (z * length_y + y) * 2 + c
     count = length_z * length_y * 2
     count_rows = tok_ref.shape[0]
-    a_ref, q_ref, b_ref = traffic.arrays
+    a_ref, b_ref = traffic.arrays
 
     def device_at(index):
         index = lax.rem(index + count, count)
@@ -521,8 +520,7 @@
 
     moves = []
     for array, refs in (
-        (a_ref, (value_ref, inflow_ref, readout_ref, key_ref, vector_ref)),
-        (q_ref, (query_ref,)),
+        (a_ref, (value_ref, inflow_ref, readout_ref, key_ref, vector_ref, query_ref)),
         (b_ref, (gate_ref, state_ref, window_ref)),
     ):
         column = 0
@@ -540,7 +538,7 @@
     step = jnp.concatenate([step, jnp.zeros((rows, 128 - cols), F32)], axis=1)
     step = jnp.concatenate([step, jnp.zeros((128 - rows, 128), F32)], axis=0)
     a_ref[z, y, c, :, WIDTHS[0] - 128 : WIDTHS[0]] = step.T[0:cols, :].astype(BF16)
-    for move in moves[:5]:
+    for move in moves[:6]:
         move.wait()
     enter()
     edge_copies = []
@@ -568,7 +566,7 @@
     traffic.begin()
     for copy in edge_copies:
         copy.start()
-    for move in moves[5:]:
+    for move in moves[6:]:
         move.wait()
     blocks = count_rows // BLOCK
     traffic.service(1.0)
@@ -583,11 +581,11 @@
     ).astype(BF16)
     traffic.service(0.3)
     traffic.until(0)
-    traffic.service(1.5)
+    traffic.service(0.5)
 
 
 def middle(
-    traffic, normed, a_ref, query_ref, b_ref, taps_x_ref, taps_b_ref, taps_c_ref, rate_ref, freq_ref, sink_ref,
+    traffic, normed, a_ref, b_ref, taps_x_ref, taps_b_ref, taps_c_ref, rate_ref, freq_ref, sink_ref,
     out_ref, window_ref, log_ref, gate_ref, conv_ref, col_ref, row_ref, piece_ref, etot_ref,
     cin_ref, kv_ref, q_ref, step_ref, win, near, msg_ref,
     kv_before_ref, kv_after_ref, keys, values, by_row, by_col, part, turned, by_y, summed, by_z,
@@ -682,8 +680,7 @@
         to = lax.rem(y + k, length_y)
         copies.append(send(turned.at[to], by_y.at[k], y_sem.at[k], {SP[1]: to}))
     by_y[0] = turned[y]
-    traffic.until(1)
-    project(q_ref, rows, 2, query_ref, 0)
+    project(q_ref, rows, 2, a_ref, Q_AT)
     attend(1)
     traffic.service(1.1)
     for copy in copies:
@@ -756,7 +753,7 @@
     copy = send(nxt, final, final_sem, {SP[2]: other})
     attend(blocks - 1)
     traffic.service(1.1)
-    traffic.until(2)
+    traffic.until(1)
     project(gate_ref, rows, 2, b_ref, 0)
     copy.wait()
     out_ref[other] = final[...]
@@ -853,9 +850,9 @@
     shards, refs = refs[:9], refs[9:]
     sink_ref, mixed_ref, log_ref = refs[:3]
     smalls, refs = refs[3:11], refs[11:]
-    small_sem, arrays, normed = refs[0], refs[1:4], refs[4]
-    gather_refs, refs = refs[5:10], refs[10:]
-    flow_sems, refs = (refs[0:4], refs[4:8], refs[8:12]), refs[12:]
+    small_sem, arrays, normed = refs[0], refs[1:3], refs[3]
+    gather_refs, refs = refs[4:9], refs[9:]
+    flow_sems, refs = (refs[0:4], refs[4:8]), refs[8:]
     incoming, window_ref, gate_ref = refs[:3]
     conv_refs, refs = refs[3:8], refs[8:]
     middle_refs, finish_refs = refs[:29], refs[29:]
@@ -905,7 +902,7 @@
         incoming, window_ref, log_ref, gate_ref, *conv_refs, *middle_refs,
     )
     finish(
-        window_ref, flat_refs[2], *conv_refs, incoming, gate_ref, group_gain_ref, mixed_ref, *finish_refs
+        window_ref, flat_refs[1], *conv_refs, incoming, gate_ref, group_gain_ref, mixed_ref, *finish_refs
     )
     traffic.finish()
 

time: 120 us -> 117 us (0.975)
  Pallas kernels: 116 us -> 113 us
    pallas_call x1, Pallas kernels: 116 us -> 113 us  [layer(): pl.pallas_call(functools.partial(layer_kernel, (length_z, length_y)), in_...]
where the time goes in v7:
time: 117 us
  Pallas kernels  113 us (97%)
  local copies, waits for them, and re-layouts  3.41 us (3%)
    pallas_call x1, Pallas kernels, layer(): pl.pallas_call(functools.partial(layer_kernel, (length_z, length_y)), in_...  113 us
    unnamed x2, local copies, waits for them, and re-layouts  3.41 us

profile of v7, /device:TPU:1, one launch (start us, length us, event | category | flops | bytes accessed | tf_op | source)
XLA Modules:
  0.0 117.1 jit_solution(17940181706334307646)
XLA Ops:
  0.6 113.1 %layer.1 = (bf16[768,512]{1,0:T(8,128)(2,1)}, f32[8,768]{1,0:T(8,128)}) custom-call(bf16[768,2048]{1,0:T(8,128)(2,1)} %tok_ref.1, bf16[16,128]{1,0:T(8,128)(2,1)} %bitcast.21, bf16[16,32]{1,0:T(8,128)(2,1)} %bitcast.22, bf16[5,512]{1,0:T(8,128)(2,1)} %refs_2_.1, bf16[5,128]{1,0:T(8,128)(2,1)} %bitcast.23, bf16[5,128]{1,0:T(8,128)(2,1)} %bitcast.24, ...), custom_call_target="tpu_custom_call" | custom-call | flops 8589934592 | bytes 25165824 | tf_op jit(solution)/shard_map/layer/pallas_call | solution.py:973
  113.7 2.1 %copy.23 = bf16[768,512]{1,0:T(8,128)(2,1)} copy(bf16[768,512]{1,0:T(8,128)(2,1)} %get-tuple-element.8) | data formatting | bytes 1572864
  115.8 1.3 %copy.24 = f32[768,8]{0,1:T(8,128)} copy(f32[768,8]{0,1:T(8,128)} %bitcast.15) | data formatting | bytes 49152

commit v8 on v5

--- a/solution.py
+++ b/solution.py
@@ -63,8 +63,8 @@
 
 
 def conv_state(
-    service, cin_ref, taps_x_ref, taps_b_ref, taps_c_ref, step_ref, rate_ref,
-    conv_ref, col_ref, row_ref, piece_ref, etot_ref, msg_ref, win, near,
+    traffic_service, cin_ref, taps_x_ref, taps_b_ref, taps_c_ref, step_ref, rate_ref,
+    conv_ref, col_ref, row_ref, piece_ref, etot_ref, msg_ref, win,
 ):
     count = cin_ref.shape[0] - 2 * HALO
     blocks = count // BLOCK
@@ -86,42 +86,53 @@
         return carry
 
     lax.fori_loop(0, blocks, fill, 0)
-    service(0.5)
-
-    def one(i, total):
-        start = pl.multiple_of(i * BLOCK, BLOCK)
-        rows = pl.ds(start, BLOCK)
-        near[...] = win[pl.ds(start, BLOCK + 2 * HALO), :]
-        acc = near[HALO - 2 : HALO - 2 + BLOCK, :] * taps[0:1, :]
-        for tap in range(1, 5):
-            first = HALO - 2 + tap
-            acc = acc + near[first : first + BLOCK, :] * taps[tap : tap + 1, :]
-        conv = (acc * jax.nn.sigmoid(acc)).astype(BF16)
-        conv_ref[rows, :] = conv
-        raw = step_ref[rows, 0 : 2 * HEADS]
-        step = jnp.maximum(raw, 0.0) + jnp.log1p(jnp.exp(-jnp.abs(raw)))
-        rate = jnp.concatenate([rate_ref[:, rows], jnp.zeros((BLOCK - 2 * HEADS, BLOCK), F32)], axis=0)
-        decay = -jnp.exp(rate.T[:, 0 : 2 * HEADS]) * step
-        cum = dot(tri, decay, precision=lax.Precision.HIGHEST)
-        tot = cum[BLOCK - 1 : BLOCK, :]
-        col = jnp.where(forward16, cum, cum - decay)
-        col_ref[rows, 0 : 2 * HEADS] = col
-        col_ref[rows, 2 * HEADS : 4 * HEADS] = jnp.broadcast_to(tot, (BLOCK, 2 * HEADS))
-        both = jnp.concatenate([col, step, jnp.zeros((BLOCK, 128 - 4 * HEADS), F32)], axis=1)
-        row_ref[i] = both.T[0 : 4 * HEADS, :]
-        weight = jnp.exp(jnp.where(forward16, tot - col, col)) * step
-        wide = spread(weight, spread_m, 2)
-        xs = conv[:, 0:channels].astype(F32)
-        scaled = (jnp.concatenate([xs, xs], axis=1) * wide).astype(BF16)
-        inflow = conv[:, channels : channels + STATE]
-        piece_ref[i] = dot(inflow, scaled, ((0,), (0,)))
-        etot_ref[i] = spread(jnp.exp(jnp.broadcast_to(tot, (8, 2 * HEADS))), spread_m, 3)
-        return total + tot
+    traffic_service(0.5)
+
+    def some(which):
+        spans = [slice(i * BLOCK, (i + 1) * BLOCK) for i in which]
+        steps, decays, convs = [], [], []
+        for rows in spans:
+            raw = step_ref[rows, 0 : 2 * HEADS]
+            steps.append(jnp.maximum(raw, 0.0) + jnp.log1p(jnp.exp(-jnp.abs(raw))))
+            rate = jnp.concatenate(
+                [rate_ref[:, rows], jnp.zeros((BLOCK - 2 * HEADS, BLOCK), F32)], axis=0
+            )
+            decays.append(-jnp.exp(rate.T[:, 0 : 2 * HEADS]) * steps[-1])
+        cums = [dot(tri, decay, precision=lax.Precision.HIGHEST) for decay in decays]
+        tots = [cum[BLOCK - 1 : BLOCK, :] for cum in cums]
+        cols = [jnp.where(forward16, cum, cum - decay) for cum, decay in zip(cums, decays)]
+        weights = [
+            jnp.exp(jnp.where(forward16, tot - col, col)) * step
+            for tot, col, step in zip(tots, cols, steps)
+        ]
+        wides = [spread(weight, spread_m, 2) for weight in weights]
+        etots = [spread(jnp.exp(jnp.broadcast_to(tot, (8, 2 * HEADS))), spread_m, 3) for tot in tots]
+        rests = jnp.zeros((BLOCK, 128 - 4 * HEADS), F32)
+        turned = [jnp.concatenate([col, step, rests], axis=1).T for col, step in zip(cols, steps)]
+        for rows in spans:
+            acc = 0.0
+            for tap in range(5):
+                first = rows.start + HALO - 2 + tap
+                acc = acc + win[first : first + BLOCK, :] * taps[tap : tap + 1, :]
+            convs.append((acc * jax.nn.sigmoid(acc)).astype(BF16))
+        pieces = []
+        for conv, wide in zip(convs, wides):
+            xs = conv[:, 0:channels].astype(F32)
+            scaled = (jnp.concatenate([xs, xs], axis=1) * wide).astype(BF16)
+            pieces.append(dot(conv[:, channels : channels + STATE], scaled, ((0,), (0,))))
+        for n, (i, rows) in enumerate(zip(which, spans)):
+            conv_ref[rows, :] = convs[n]
+            col_ref[rows, 0 : 2 * HEADS] = cols[n]
+            col_ref[rows, 2 * HEADS : 4 * HEADS] = jnp.broadcast_to(tots[n], (BLOCK, 2 * HEADS))
+            row_ref[i] = turned[n][0 : 4 * HEADS, :]
+            piece_ref[i] = pieces[n]
+            etot_ref[i] = etots[n]
+        return sum(tots)
 
     total = jnp.zeros((1, 2 * HEADS), F32)
     for i in range(0, blocks, 2):
-        total = lax.fori_loop(i, i + 2, one, total)
-        service(1.7)
+        total = total + some((i, i + 1))
+        traffic_service(1.6)
     forward = piece_ref[0, :, 0:channels]
     backward = piece_ref[blocks - 1, :, channels : 2 * channels]
     for i in range(1, blocks):
@@ -272,27 +283,31 @@
         valid = in_band & (here >= start_at) & (here < end_at)
         table = tables(i + 1)
         band = pl.ds(start, 3 * BLOCK)
+        qs = []
         for pair in range(HEADS // 2):
-            group = pair // 2
             lanes = slice(pair * 128, pair * 128 + 128)
             q = (turn(q_ref[rows, lanes], table).astype(F32) * HEAD_DIM ** (-0.5)).astype(BF16)
             zero = jnp.zeros_like(q)
-            both = jnp.concatenate(
+            qs.append(jnp.concatenate(
                 [jnp.where(first_half, q, zero), jnp.where(first_half, zero, q)], axis=0
-            )
-            scores = dot(keys[group, band, :], both, ((1,), (1,)))
-            scores = jnp.where(valid, scores, -1e30)
+            ))
+        scores = [dot(keys[pair // 2, band, :], q, ((1,), (1,))) for pair, q in enumerate(qs)]
+        outs = []
+        for pair in range(HEADS // 2):
+            group = pair // 2
+            mine = jnp.where(valid, scores[pair], -1e30)
             sink = jnp.where(first_row_half, sink_ref[2 * pair], sink_ref[2 * pair + 1])
-            top = jnp.maximum(jnp.max(scores, axis=0, keepdims=True), sink)
-            expo = jnp.exp(scores - top)
+            top = jnp.maximum(jnp.max(mine, axis=0, keepdims=True), sink)
+            expo = jnp.exp(mine - top)
             total = jnp.sum(expo, axis=0, keepdims=True) + jnp.exp(sink - top)
-            mine = values[group * HEAD_DIM : (group + 1) * HEAD_DIM, band]
-            o = dot(mine, expo.astype(BF16)) / total
-            turned = jnp.concatenate([o[:, 0:BLOCK], o[:, BLOCK:]], axis=0).T
-            out_ref[rows, lanes] = turned.astype(BF16)
+            value = values[group * HEAD_DIM : (group + 1) * HEAD_DIM, band]
+            outs.append(dot(value, expo.astype(BF16)) / total)
             log = top + jnp.log(total)
             log_ref[2 * pair : 2 * pair + 1, rows] = log[:, 0:BLOCK]
             log_ref[2 * pair + 1 : 2 * pair + 2, rows] = log[:, BLOCK:]
+        for pair, o in enumerate(outs):
+            turned = jnp.concatenate([o[:, 0:BLOCK], o[:, BLOCK:]], axis=0).T
+            out_ref[rows, pair * 128 : pair * 128 + 128] = turned.astype(BF16)
 
     return own_keys, edge_keys, one
 
@@ -620,7 +635,7 @@
     conv_state(
         late.service,
         cin_ref, taps_x_ref, taps_b_ref, taps_c_ref, step_ref, rate_ref,
-        conv_ref, col_ref, row_ref, piece_ref, etot_ref, msg_ref, win, near,
+        conv_ref, col_ref, row_ref, piece_ref, etot_ref, msg_ref, win,
     )
     copy = send(msg_ref.at[other], part, part_sem, {SP[2]: other})
     own_keys, edge_keys, attend = attention(
@@ -647,6 +662,8 @@
     by_y[0] = turned[y]
     project(q_ref, rows, 2, a_ref, Q_AT)
     late.service(2.4)
+    attend(1)
+    late.service(1.4)
     for copy in copies:
         copy.wait()
     before = []
@@ -667,9 +684,9 @@
             send(summed, by_z.at[k], z_sem.at[k], {SP[0]: to})
 
     carry[...] = jnp.zeros_like(carry)
-    for i in range(1, blocks - 1):
+    for i in range(2, blocks - 1):
         attend(i)
-        late.service(1.9)
+        late.service(1.5)
     for distance in reversed(range(1, length_z)):
         slot = jnp.where(forward, distance, length_z - distance)
 
@@ -705,7 +722,7 @@
         copy.wait()
     edge_keys()
     attend(0)
-    late.service(2.2)
+    late.service(1.7)
     for copy in copies:
         copy.wait()
     for j in range(pairs):
@@ -716,7 +733,7 @@
         ).astype(BF16)
     copy = send(nxt, final, final_sem, {SP[2]: other})
     attend(blocks - 1)
-    late.service(2.0)
+    late.service(1.5)
     late.drain()
     project(gate_ref, rows, 2, b_ref, 0)
     copy.wait()

time: 115 us -> 113 us (0.983)
  Pallas kernels: 111 us -> 109 us
    pallas_call x1, Pallas kernels: 111 us -> 109 us  [layer(): pl.pallas_call(functools.partial(layer_kernel, (length_z, length_y)), in_...]
where the time goes in v8:
time: 113 us
  Pallas kernels  109 us (96%)
  local copies, waits for them, and re-layouts  3.41 us (3%)
    pallas_call x1, Pallas kernels, layer(): pl.pallas_call(functools.partial(layer_kernel, (length_z, length_y)), in_...  109 us
    unnamed x2, local copies, waits for them, and re-layouts  3.41 us

profile of v8, /device:TPU:1, one launch (start us, length us, event | category | flops | bytes accessed | tf_op | source)
XLA Modules:
  0.0 112.7 jit_solution(12149201720866101236)
XLA Ops:
  0.6 108.7 %layer.1 = (bf16[768,512]{1,0:T(8,128)(2,1)}, f32[8,768]{1,0:T(8,128)}) custom-call(bf16[768,2048]{1,0:T(8,128)(2,1)} %tok_ref.1, bf16[16,128]{1,0:T(8,128)(2,1)} %bitcast.21, bf16[16,32]{1,0:T(8,128)(2,1)} %bitcast.22, bf16[5,512]{1,0:T(8,128)(2,1)} %refs_2_.1, bf16[5,128]{1,0:T(8,128)(2,1)} %bitcast.23, bf16[5,128]{1,0:T(8,128)(2,1)} %bitcast.24, ...), custom_call_target="tpu_custom_call" | custom-call | flops 8589934592 | bytes 25165824 | tf_op jit(solution)/shard_map/layer/pallas_call | solution.py:958
  109.3 2.1 %copy.23 = bf16[768,512]{1,0:T(8,128)(2,1)} copy(bf16[768,512]{1,0:T(8,128)(2,1)} %get-tuple-element.8) | data formatting | bytes 1572864
  111.4 1.3 %copy.24 = f32[768,8]{0,1:T(8,128)} copy(f32[768,8]{0,1:T(8,128)} %bitcast.15) | data formatting | bytes 49152
